TPU v7x, 32 devices: a whole 2x2x4 slice. The times are simulated.
32 devices in a mesh: sp: 8 (over z, y), tp: 4 (over x, core).
Axes of the slice: x: 2, y: 2, z: 4, core: 2. Of those that a mesh axis runs over, the one named last changes fastest.
Arguments:
- inputs: bfloat16 [8192, 2048], P(('sp', 'tp')), may hold values from -90 to 90
- in_gain: float32 [2048], replicated, may hold values from 0.1 to 1.9
- w_query: bfloat16 [2048, 1024], replicated, may hold values from -2 to 2
- w_key: bfloat16 [2048, 128], replicated, may hold values from -2 to 2
- w_value: bfloat16 [2048, 128], replicated, may hold values from -0.125 to 0.125
- query_gain: float32 [64], replicated, may hold values from 0 to 8, as said below
- key_gain: float32 [64], replicated, may hold values from 0 to 8, as said below
- decay_sums: float32 [8192, 16], P('sp', 'tp'), may hold values from -1173 to 0, as said below
- w_out: bfloat16 [1024, 2048], replicated, may hold values from -0.1875 to 0.1875
Outputs:
- result: bfloat16 [8192, 2048], P(('sp', 'tp'))
Inputs may be any that keep to these rules, and one draw needn't show every extreme that they name: `decay_sums`: along positions, each head's entries never rise. `query_gain`: every entry is positive. `key_gain`: every entry is positive.
All inputs are finite; a program needn't handle non-finite values.
Results may differ from a plain program's by a relative error of at most 0.015.
The roundings to bfloat16 on the way count: a program that leaves them out, or rounds other values in their place, can miss the bound.
Values may be sent and summed in bfloat16 or wider, within the bound.
A program may use at most 64 MiB of HBM per device.

v0:
```python
import math

import jax
import jax.numpy as jnp
from jax import lax
from jax.experimental import pallas as pl
from jax.experimental.pallas import tpu as pltpu
from jax.sharding import Mesh, PartitionSpec as P

epsilon = 1e-06
LOG2E = math.log2(math.e)
ALL = ("sp", "kv", "half")
HEADS_PER_DOT = 2
KEY_BLOCK = 512
SMALL = 60.0


def rms_norm(vector, gain_vec):
    return (
        vector * lax.rsqrt(jnp.mean(vector * vector, axis=-1, keepdims=True) + epsilon) * gain_vec
    )


def exchange_kernel(
    kv_ref, q_ref, decay_ref, kv_out, q_out, decay_out, own_sems, kv_send, kv_recv, kv_relay,
    decay_send, decay_recv, decay_relay, q_send, q_recv, *, rows, sizes
):
    sp_count, kv_heads, half_count = sizes
    sp, group, half = lax.axis_index("sp"), lax.axis_index("kv"), lax.axis_index("half")
    core, chips = half % 2, half_count // 2
    partner = (sp, group, half + 1 - 2 * core)

    def device_of(chip):
        return (chip // (kv_heads * chips), (chip // chips) % kv_heads, (chip % chips) * 2 + core)

    def block_of(place):
        return (place[0] * kv_heads + place[1]) * half_count + place[2]

    def kv_copy(source, block, send, device):
        return pltpu.make_async_remote_copy(
            src_ref=source, dst_ref=kv_out.at[pl.ds(pl.multiple_of(block * rows, rows), rows)],
            send_sem=send, recv_sem=kv_recv.at[block], device_id=device,
            device_id_type=pl.DeviceIdType.MESH,
        )

    def decay_copy(source, member, send, device):
        return pltpu.make_async_remote_copy(
            src_ref=source, dst_ref=decay_out.at[member], send_sem=send,
            recv_sem=decay_recv.at[member], device_id=device,
            device_id_type=pl.DeviceIdType.MESH,
        )

    me = block_of((sp, group, half))
    chip = (sp * kv_heads + group) * chips + half // 2
    total = sp_count * kv_heads * chips
    member = sp * half_count + half
    cluster = sp * chips + half // 2
    clusters = sp_count * chips
    started = []
    for k in range(1, total):
        place = device_of((chip + k) % total)
        started.append(kv_copy(kv_ref.at[place[1]], me, kv_send.at[k], place))
        started[-1].start()
    for k in range(1, clusters):
        other = (cluster + k) % clusters
        place = (other // chips, group, (other % chips) * 2 + core)
        started.append(decay_copy(decay_ref, member, decay_send.at[k], place))
        started[-1].start()
    q_copy = pltpu.make_async_remote_copy(
        src_ref=q_ref, dst_ref=q_out, send_sem=q_send, recv_sem=q_recv,
        device_id=(sp_count - 1 - sp, kv_heads - 1 - group, half_count - 1 - half),
        device_id_type=pl.DeviceIdType.MESH,
    )
    q_copy.start()
    started.append(kv_copy(kv_ref.at[group], me, kv_relay.at[0], partner))
    started[-1].start()
    started.append(decay_copy(decay_ref, member, decay_relay.at[0], partner))
    started[-1].start()
    own_kv = pltpu.make_async_copy(
        kv_ref.at[group], kv_out.at[pl.ds(pl.multiple_of(me * rows, rows), rows)], own_sems.at[0]
    )
    own_kv.start()
    own_decay = pltpu.make_async_copy(decay_ref, decay_out.at[member], own_sems.at[1])
    own_decay.start()
    for k in range(1, clusters):
        other = (cluster + clusters - k) % clusters
        which = (other // chips) * half_count + (other % chips) * 2 + core
        landed = decay_out.at[which]
        relay = decay_copy(landed, which, decay_relay.at[k], partner)
        relay.wait_recv()
        relay.start()
        started.append(relay)
    for k in range(1, total):
        block = block_of(device_of((chip + total - k) % total))
        landed = kv_out.at[pl.ds(pl.multiple_of(block * rows, rows), rows)]
        relay = kv_copy(landed, block, kv_relay.at[k], partner)
        relay.wait_recv()
        relay.start()
        started.append(relay)
    for k in range(clusters):
        other = (cluster + clusters - k) % clusters
        which = (other // chips) * half_count + (other % chips) * 2 + 1 - core
        decay_copy(decay_out.at[which], which, decay_relay.at[k], partner).wait_recv()
    for k in range(total):
        place = device_of((chip + total - k) % total)
        block = block_of((place[0], place[1], place[2] + 1 - 2 * core))
        landed = kv_out.at[pl.ds(pl.multiple_of(block * rows, rows), rows)]
        kv_copy(landed, block, kv_relay.at[k], partner).wait_recv()
    for copy in started:
        copy.wait_send()
    own_kv.wait()
    own_decay.wait()
    q_copy.wait()


def attend_kernel(
    place_ref, near_ref, far_ref, row_ref, decay_ref, kv_ref, out_ref, ones_ref, q_ref, peak_ref,
    acc_ref, *, rows, heads, key_block, small
):
    lane = lax.broadcasted_iota(jnp.int32, (rows, 128), 1)
    low = lane < 64
    for r, ref in enumerate((near_ref, far_ref)):
        for pair in range(heads // 2):
            both = ref[:, pair * 128 : (pair + 1) * 128].astype(jnp.float32)
            even = jnp.where(low, both, 0.0)
            odd = jnp.where(low, pltpu.roll(both, 64, 1), 0.0)
            q_ref[r, (2 * pair) * rows : (2 * pair + 1) * rows] = even.astype(jnp.bfloat16)
            q_ref[r, (2 * pair + 1) * rows : (2 * pair + 2) * rows] = odd.astype(jnp.bfloat16)

    def fill(i, carry):
        at = pl.ds(pl.multiple_of(i * key_block, key_block), key_block)
        wide = lax.broadcasted_iota(jnp.int32, (key_block, 128), 1) < 64
        ones_ref[at] = jnp.where(wide, 1.0, kv_ref[at].astype(jnp.float32)).astype(jnp.bfloat16)
        return carry

    lax.fori_loop(0, kv_ref.shape[0] // key_block, fill, 0)
    span = HEADS_PER_DOT * rows

    for r in range(2):
        first = place_ref[r]
        for head in range(heads):
            part = pl.ds(head * rows, rows)
            if small:
                peak_ref[part] = jnp.broadcast_to(row_ref[r, :, head : head + 1], (rows, 128))
            else:
                peak_ref[part] = jnp.full((rows, 128), -1e30, jnp.float32)
        acc_ref[...] = jnp.zeros_like(acc_ref)

        def step(index, masked):
            at = pl.ds(pl.multiple_of(index * key_block, key_block), key_block)
            keys = kv_ref[at]
            values = ones_ref[at]
            for start in range(0, heads, HEADS_PER_DOT):
                part = pl.ds(start * rows, span)
                before = peak_ref[part]
                scores = lax.dot_general(
                    q_ref[r, part], keys, (((1,), (1,)), ((), ())),
                    preferred_element_type=jnp.float32,
                )
                if small:
                    scores = scores + jnp.concatenate([before] * (key_block // 128), axis=1)
                scores = scores.reshape(HEADS_PER_DOT, rows, key_block)
                scores = scores - decay_ref[index, start : start + HEADS_PER_DOT][:, None, :]
                if masked:
                    row = first + lax.broadcasted_iota(jnp.int32, (rows, key_block), 0)
                    col = index * key_block + lax.broadcasted_iota(
                        jnp.int32, (rows, key_block), 1
                    )
                    scores = jnp.where((col <= row)[None], scores, -1e30)
                scores = scores.reshape(span, key_block)
                if small:
                    weights = jnp.exp2(scores).astype(jnp.bfloat16)
                    acc_ref[part] += jnp.dot(weights, values, preferred_element_type=jnp.float32)
                else:
                    after = jnp.maximum(before, jnp.max(scores, axis=1, keepdims=True))
                    weights = jnp.exp2(scores - after[:, :1]).astype(jnp.bfloat16)
                    acc_ref[part] = acc_ref[part] * jnp.exp2(before - after) + jnp.dot(
                        weights, values, preferred_element_type=jnp.float32
                    )
                    peak_ref[part] = after

        full = first // key_block

        def body(index, carry):
            step(index, False)
            return carry

        lax.fori_loop(0, full, body, 0)
        step(full, True)
        for pair in range(heads // 2):
            even = acc_ref[(2 * pair) * rows : (2 * pair + 1) * rows]
            odd = acc_ref[(2 * pair + 1) * rows : (2 * pair + 2) * rows]
            done = jnp.where(low, pltpu.roll(even, 64, 1), odd) / jnp.where(
                low, even, pltpu.roll(odd, 64, 1)
            )
            out_ref[r, :, pair * 128 : (pair + 1) * 128] = done.astype(jnp.bfloat16)


def attend(place, near, far, row_decay, decays, kv, small):
    length = kv.shape[0]
    rows, width = near.shape
    heads, key_block = decays.shape[1:]
    vmem = pl.BlockSpec(memory_space=pltpu.VMEM)
    return pl.pallas_call(
        lambda *refs: attend_kernel(
            *refs, rows=rows, heads=heads, key_block=key_block, small=small
        ),
        out_shape=jax.ShapeDtypeStruct((2, rows, width), jnp.bfloat16),
        in_specs=[pl.BlockSpec(memory_space=pltpu.SMEM)] + [vmem] * 5,
        out_specs=vmem,
        scratch_shapes=[
            pltpu.VMEM((length, 128), jnp.bfloat16),
            pltpu.VMEM((2, heads * rows, 128), jnp.bfloat16),
            pltpu.VMEM((heads * rows, 128), jnp.float32),
            pltpu.VMEM((heads * rows, 128), jnp.float32),
        ],
        compiler_params=pltpu.CompilerParams(vmem_limit_bytes=40 * 1024 * 1024),
        name="attend_small" if small else "attend_any",
    )(place, near, far, row_decay, decays, kv)


def per_device(inputs, in_gain, w_query, w_key, w_value, query_gain, key_gain, decay_sums, w_out):
    sp_count = lax.axis_size("sp")
    kv_heads = lax.axis_size("kv")
    half_count = lax.axis_size("half")
    tp_count = kv_heads * half_count
    group = lax.axis_index("kv")
    me = (lax.axis_index("sp") * kv_heads + group) * half_count + lax.axis_index("half")
    count = sp_count * tp_count
    mirror = [(i, count - 1 - i) for i in range(count)]
    head_size = query_gain.shape[0]
    rows = inputs.shape[0]
    length = rows * count
    all_heads = w_query.shape[1] // head_size
    heads = all_heads // kv_heads
    width = heads * head_size
    members = sp_count * half_count
    key_block = math.gcd(length, KEY_BLOCK)

    def choose(a, b):
        return jnp.where(group == 0, a, b)

    normed = rms_norm(inputs.astype(jnp.float32), in_gain).astype(jnp.bfloat16)
    keys = rms_norm(
        jnp.dot(normed, w_key, preferred_element_type=jnp.float32).reshape(
            rows, kv_heads, head_size
        ),
        key_gain,
    ).astype(jnp.bfloat16)
    values = (
        jnp.dot(normed, w_value, preferred_element_type=jnp.float32)
        .astype(jnp.bfloat16)
        .reshape(rows, kv_heads, head_size)
    )
    pairs = jnp.concatenate([keys, values], axis=2)
    kv_blocks = pairs.transpose(1, 0, 2)
    decay_rows = (decay_sums.T * LOG2E).reshape(-1, 128)

    queries = rms_norm(
        jnp.dot(normed, w_query, preferred_element_type=jnp.float32).reshape(
            rows, all_heads, head_size
        ),
        query_gain * (LOG2E * head_size ** (-0.5)),
    ).astype(jnp.bfloat16).reshape(rows, kv_heads * width)
    own_q = choose(queries[:, :width], queries[:, width:])
    sent_q = choose(queries[:, width:], queries[:, :width])
    vmem = pl.BlockSpec(memory_space=pltpu.VMEM)
    chips = count // 2
    dma = pltpu.SemaphoreType.DMA
    kv, far_q, decay_all = pl.pallas_call(
        lambda *refs: exchange_kernel(
            *refs, rows=rows, sizes=(sp_count, kv_heads, half_count)
        ),
        out_shape=(
            jax.ShapeDtypeStruct((length, 128), jnp.bfloat16),
            jax.ShapeDtypeStruct((rows, width), jnp.bfloat16),
            jax.ShapeDtypeStruct((members, *decay_rows.shape), jnp.float32),
        ),
        in_specs=[vmem] * 3,
        out_specs=(vmem,) * 3,
        scratch_shapes=[
            dma((2,)), dma((chips,)), dma((count,)), dma((chips,)), dma((members // 2,)),
            dma((members,)), dma((members // 2,)), dma, dma,
        ],
        compiler_params=pltpu.CompilerParams(has_side_effects=True),
        name="exchange",
    )(kv_blocks, sent_q, decay_rows)
    decay_all = decay_all.reshape(sp_count, heads, -1, key_block)
    decay_all = decay_all.transpose(0, 2, 1, 3).reshape(length // key_block, heads, key_block)
    firsts = (me * rows, (count - 1 - me) * rows)
    place = jnp.stack(firsts).astype(jnp.int32)
    row_decay = jnp.stack(
        [
            lax.dynamic_slice(
                decay_all, (first // key_block, 0, first % key_block), (1, heads, rows)
            )[0].T
            for first in firsts
        ]
    )
    bound = head_size**0.5 * LOG2E * jnp.max(query_gain) * jnp.max(key_gain)
    attended = lax.cond(
        bound <= SMALL,
        lambda *given: attend(*given, True),
        lambda *given: attend(*given, False),
        place, own_q, far_q, row_decay, decay_all, kv,
    )
    back = lax.ppermute(attended[1], ALL, mirror)
    whole = choose(
        jnp.concatenate([attended[0], back], axis=1), jnp.concatenate([back, attended[0]], axis=1)
    )
    return jnp.dot(whole, w_out, preferred_element_type=jnp.float32).astype(jnp.bfloat16)


def solution(mesh):
    sp_count, tp_count = mesh.devices.shape
    split = Mesh(mesh.devices.reshape(sp_count, 2, tp_count // 2), ALL)
    placed = (P(ALL, None), P(), P(), P(), P(), P(), P(), P("sp", ("kv", "half")), P())
    return jax.shard_map(
        per_device, mesh=split, in_specs=placed, out_specs=P(ALL, None), check_vma=False
    )
```

profile of v0, /device:TPU:9, one launch (start us, length us, event | category | flops | bytes accessed | tf_op | source)
XLA Modules:
  0.0 139.4 jit_solution(17819943625331422007)
XLA Ops:
  0.1 1.6 %fusion = f32[256]{0:T(256)S(1)} fusion(bf16[256,2048]{1,0:T(8,128)(2,1)} %param.11), kind=kLoop, calls=%fused_computation.5 | loop fusion | flops 1572608 | bytes 1049600 | tf_op jit(solution)/shard_map/reduce_sum | solution.py:20
  1.7 1.3 broadcast_multiply_fusion
  3.0 1.3 reduce_max.19
  5.5 0.7 multiply_bitcast_fusion
  6.2 0.6 reshape.49.refs_2_
  6.9 1.9 %convolution_convert_fusion.1 = bf16[256,128]{0,1:T(8,128)(2,1)S(1)} fusion(bf16[2048,128]{1,0:T(8,128)(2,1)} %param.15, bf16[256,2048]{1,0:T(8,128)(2,1)} %param.11, f32[2048]{0:T(1024)} %param.12, f32[256]{0:T(256)S(1)} %add_rsqrt_fusion.2), kind=kOutput, calls=%fused_computation.8 | convolution fusion | flops 136347648 | bytes 1647616 | tf_op jit(solution)/shard_map/dot_general | solution.py:251
  9.0 0.6 multiply_reduce_fusion
  9.6 0.1 copy.11
  9.7 4.5 %fusion.16 = (f32[256,1024]{1,0:T(8,128)S(1)}, f32[256,1024]{1,0:T(8,128)}) fusion(bf16[2048,1024]{1,0:T(8,128)(2,1)} %param.13, bf16[256,2048]{1,0:T(8,128)(2,1)S(1)} %copy-done.1, f32[2048]{0:T(1024)S(1)} %copy-done.3, f32[256]{0:T(256)S(1)} %add_rsqrt_fusion.2), kind=kOutput, calls=%fused_computation.37 | convolution fusion | flops 1076101120 | bytes 7349248 | tf_op jit(solution)/shard_map/dot_general | solution.py:260
  14.2 0.3 copy.13
  14.7 0.3 copy.14
  15.2 0.1 multiply_convert_fusion.1
  15.3 0.8 maximum_bitcast_fusion.refs_0_
  16.1 1.4 %multiply_convert_fusion = bf16[256,1024]{1,0:T(8,128)(2,1)S(1)} fusion(f32[256,1024]{1,0:T(8,128)} %get-tuple-element.84, f32[256,1024]{1,0:T(8,128)S(1)} %copy.14, f32[1024]{0:T(1024)S(1)} %mul.116), kind=kLoop, calls=%fused_computation.10 | loop fusion | flops 786432 | bytes 2625536 | tf_op jit(solution)/shard_map/convert_element_type | solution.py:264
  17.5 0.8 fusion.15
  18.3 50.9 %exchange.1 = (bf16[8192,128]{1,0:T(8,128)(2,1)S(1)}, bf16[256,512]{1,0:T(8,128)(2,1)}, f32[16,32,128]{2,1,0:T(8,128)}) custom-call(bf16[2,256,128]{2,1,0:T(8,128)(2,1)} %maximum_bitcast_fusion.refs_0_, bf16[256,512]{1,0:T(8,128)(2,1)} %get-tuple-element.77.refs_1_, f32[32,128]{1,0:T(8,128)} %reshape.49.refs_2_), custom_call_target="tpu_custom_call" | custom-call | tf_op jit(solution)/shard_map/exchange/pallas_call | solution.py:270
  69.3 1.1 reshape.50
  70.5 49.9 %conditional.1 = (bf16[2,256,512]{2,1,0:T(8,128)(2,1)}) conditional(s32[]{:T(128)} %convert_element_type.22, (s32[2]{0:T(128)S(1)}, pred[]{:T(512)}, bf16[256,512]{1,0:T(8,128)(2,1)}, f32[2,256,8]{1,2,0:T(8,128)S(1)}, f32[16,8,512]{2,1,0:T(8,128)S(1)}, /*index=5*/bf16[8192,128]{1,0:T(8,128)(2,1)S(1)}, bf16[256,512]{1,0:T(8,128)(2,1)}, ...), branch_computations={%region_5.6_spmd, %region_6.7_spmd} | conditional | flops 131072 | bytes 819209 | solution.py:301
  70.5 1.0 broadcast_select_fusion.refs_1_
  71.5 0.1 copy.16.refs_3_
  71.6 48.8 %attend_any.1 = bf16[2,256,512]{2,1,0:T(8,128)(2,1)} custom-call(s32[2]{0:T(128)S(1)} %get-tuple-element.32.refs_0_, bf16[256,512]{1,0:T(8,128)(2,1)S(1)} %broadcast_select_fusion.refs_1_, bf16[256,512]{1,0:T(8,128)(2,1)} %get-tuple-element.34.refs_2_, f32[2,256,8]{2,1,0:T(8,128)S(1)} %copy.16.refs_3_, f32[16,8,512]{2,1,0:T(8,128)S(1)} %get-tuple-element.36.refs_4_, ...), custom_call_target="tpu_custom_call" | custom-call | tf_op jit(solution)/shard_map/cond/branch_0_fun/attend_any/pallas_call | solution.py:204
  120.5 1.1 slice_bitcast_fusion.1
  121.6 13.4 %collective-permute-done = bf16[256,512]{1,0:T(8,128)(2,1)S(1)} collective-permute-done((bf16[256,512]{1,0:T(8,128)(2,1)S(1)}, bf16[256,512]{1,0:T(8,128)(2,1)S(1)}, u32[]{:S(2)}, u32[]{:S(2)}) %collective-permute-start) | collective-permute-done | bytes 262176 | tf_op jit(solution)/shard_map/ppermute | solution.py:307
  135.0 4.4 %convolution_convert_fusion = bf16[256,2048]{1,0:T(8,128)(2,1)} fusion(bf16[1024,2048]{1,0:T(8,128)(2,1)} %param.19, bf16[256,512]{1,0:T(8,128)(2,1)S(1)} %collective-permute-done, bf16[256,512]{1,0:T(8,128)(2,1)S(1)} %get-tuple-element.74, pred[]{:T(512)} %eq.8), kind=kOutput, calls=%fused_computation.4 | convolution fusion | flops 1076625408 | bytes 5767169 | tf_op jit(solution)/shard_map/dot_general | solution.py:311
  (21 shorter events, 0.7 us)
Async XLA Ops:
  0.0 8.9 %copy-start = (bf16[2048,128]{1,0:T(8,128)(2,1)S(1)}, bf16[2048,128]{1,0:T(8,128)(2,1)}, u32[]{:S(2)}) copy-start(bf16[2048,128]{1,0:T(8,128)(2,1)} %param.14) | copy-start | bytes 1572868
  0.0 8.9 %copy-start.1 = (bf16[256,2048]{1,0:T(8,128)(2,1)S(1)}, bf16[256,2048]{1,0:T(8,128)(2,1)}, u32[]{:S(2)}) copy-start(bf16[256,2048]{1,0:T(8,128)(2,1)} %param.11) | copy-start | bytes 3145732
  0.0 8.9 %copy-start.3 = (f32[2048]{0:T(1024)S(1)}, f32[2048]{0:T(1024)}, u32[]{:S(2)}) copy-start(f32[2048]{0:T(1024)} %param.12) | copy-start | bytes 24580
  14.5 0.7 copy-start.2
  121.5 13.5 %collective-permute-start = (bf16[256,512]{1,0:T(8,128)(2,1)S(1)}, bf16[256,512]{1,0:T(8,128)(2,1)S(1)}, u32[]{:S(2)}, u32[]{:S(2)}) collective-permute-start(bf16[256,512]{1,0:T(8,128)(2,1)S(1)} %get-tuple-element.75), channel_id=1, source_target_pairs={{0,31},{1,30},{2,29},{3,28},{4,27},{5,26},{6,25},{7,24},{8,23},{9,... | collective-permute-start | bytes 786440 | tf_op jit(solution)/shard_map/ppermute | solution.py:307
where the time goes:
time: 140 us; the launch traced here: 139 us
  Pallas kernels  99.8 us (71%)
  waiting for transfers between devices  13.4 us (10%)
  matrix products  11.4 us (8%)
  other arithmetic  9.2 us (7%)
  local copies, waits for them, and re-layouts  4.11 us (3%)
  between operations  1.47 us (1%)
    pallas_call x1, Pallas kernels, per_device(): pl.pallas_call(lambda *refs: exchange_kernel(*refs, rows=rows, sizes=(sp_...  50.9 us
    pallas_call x1, Pallas kernels, attend(): pl.pallas_call(lambda *refs: attend_kernel(*refs, rows=rows, heads=heads,...  48.8 us
    ppermute x1, waiting for transfers between devices, per_device(): back = lax.ppermute(attended[1], ALL, mirror)  13.4 us
    dot_general x1, matrix products, per_device(): jnp.dot(normed, w_query, preferred_element_type=jnp.float32)  4.46 us
    dot_general x1, matrix products, per_device(): jnp.dot(whole, w_out, preferred_element_type=jnp.float32)  4.43 us
  transfers between devices with their start and end apart: 1, of which 1 were waited for; matrix products, arithmetic and copies ran while one was open for 0% of the time, Pallas kernels for 0%

commit v1 on v0

--- a/solution.py
+++ b/solution.py
@@ -219,58 +219,461 @@
     )(place, near, far, row_decay, decays, kv)
 
 
-def per_device(inputs, in_gain, w_query, w_key, w_value, query_gain, key_gain, decay_sums, w_out):
-    sp_count = lax.axis_size("sp")
-    kv_heads = lax.axis_size("kv")
-    half_count = lax.axis_size("half")
-    tp_count = kv_heads * half_count
+def stream_kernel(
+    kv_ref, query_ref, decay_ref, out_ref, kv_all, decay_all, far_decay, far_q, q_ref, peak_ref,
+    acc_ref, res_ref, kv_recv, decay_recv, x_send, own_send, round_send, far_send, far_recv,
+    q_send, q_recv, back_send, back_recv, *, sizes, lines, rows, heads, key_block
+):
+    sp_count, kv_heads, half_count = sizes
+    zs, ys = lines
+    pairs = heads // 2
+    width = heads * 64
+    local, chunk_rows = decay_ref.shape
+    blocks = chunk_rows // key_block
+    s, g, j = lax.axis_index("sp"), lax.axis_index("kv"), lax.axis_index("half")
+    z, y = s // ys, s % ys
+    mirror = (sp_count - 1 - s, kv_heads - 1 - g, half_count - 1 - j)
+    offset = (g * half_count + j) * rows
+    far_offset = (mirror[1] * half_count + mirror[2]) * rows
+
+    def block_at(s_, x_, j_):
+        return (s_ * kv_heads + x_) * half_count + j_
+
+    def rows_of(block):
+        return pl.ds(pl.multiple_of(block * rows, rows), rows)
+
+    def remote(source, target, send, recv, device):
+        return pltpu.make_async_remote_copy(
+            src_ref=source, dst_ref=target, send_sem=send, recv_sem=recv, device_id=device,
+            device_id_type=pl.DeviceIdType.MESH,
+        )
+
+    def kv_copy(source, block, send, device):
+        return remote(source, kv_all.at[rows_of(block)], send, kv_recv.at[block], device)
+
+    def decay_copy(source, member, send, device):
+        return remote(source, decay_all.at[member], send, decay_recv.at[member], device)
+
+    here = (s, g, j)
+
+    def package(s_, j_, base, device, sems):
+        copies = []
+        for x_ in range(kv_heads):
+            block = block_at(s_, x_, j_)
+            copies.append(
+                kv_copy(kv_all.at[rows_of(block)], block, sems.at[base + x_], device)
+            )
+        member = s_ * half_count + j_
+        copies.append(
+            decay_copy(decay_all.at[member], member, sems.at[base + kv_heads], device)
+        )
+        return copies
+
+    each = kv_heads + 1
+    per = 1 + (ys - 1) + (half_count - 1) + (ys - 1) * (half_count - 1)
+
+    def arrived(s_, j_):
+        for copy in package(s_, j_, 0, here, own_send):
+            copy.wait_recv()
+
+    def start_all(copies):
+        for copy in copies:
+            copy.start()
+
+    def drain_all(copies):
+        for copy in copies:
+            copy.wait_send()
+
+    def inside(z_):
+        return (z_ >= 0) & (z_ < zs)
+
+    def round_of(k, go):
+        act = start_all if go else drain_all
+        for d, way in enumerate((1, -1)):
+            base = ((k - 1) * 2 + d) * per * each
+
+            @pl.when(inside(z - way * k))
+            def _():
+                s_ = (z - way * k) * ys + y
+                if go:
+                    arrived(s_, j)
+
+                @pl.when(inside(z + way))
+                def _():
+                    act(package(s_, j, base, ((z + way) * ys + y, g, j), round_send))
+
+                slot = 1
+                for n in range(1, ys):
+                    to = (z * ys + (y + n) % ys, g, j)
+                    act(package(s_, j, base + slot * each, to, round_send))
+                    slot += 1
+                for n in range(1, half_count):
+                    to = (s, g, (j + n) % half_count)
+                    act(package(s_, j, base + slot * each, to, round_send))
+                    slot += 1
+
+            reach = inside(z - way * (k - 1))
+            if way < 0:
+                reach = reach & (k != 1)
+
+            @pl.when(reach)
+            def _():
+                slot = ys + half_count - 1
+                for m in range(1, ys):
+                    s_ = (z - way * (k - 1)) * ys + (y + m) % ys
+                    if go:
+                        arrived(s_, j)
+                    for n in range(1, half_count):
+                        to = (s, g, (j + n) % half_count)
+                        act(package(s_, j, base + slot * each, to, round_send))
+                        slot += 1
+
+    def lanes_of(k):
+        for way in (1, -1):
+
+            @pl.when(inside(z - way * k))
+            def _():
+                for n in range(1, half_count):
+                    arrived((z - way * k) * ys + y, (j + n) % half_count)
+
+            reach = inside(z - way * (k - 1))
+            if way < 0:
+                reach = reach & (k != 1)
+
+            @pl.when(reach)
+            def _():
+                for m in range(1, ys):
+                    for n in range(1, half_count):
+                        arrived(
+                            (z - way * (k - 1)) * ys + (y + m) % ys, (j + n) % half_count
+                        )
+
+    def q_lanes(group, pair):
+        return pl.ds(pl.multiple_of(group * width + pair * 128, 128), 128)
+
+    own_block = block_at(s, g, j)
+    other_block = block_at(s, 1 - g, j)
+    member = s * half_count + j
+    x_copy = kv_copy(kv_ref.at[1 - g], own_block, x_send, (s, 1 - g, j))
+    x_copy.start()
+
+    def own_to(act):
+        slot = 0
+        targets = []
+        for n in range(1, half_count):
+            targets.append((None, (s, g, (j + n) % half_count)))
+        for way in (1, -1):
+            targets.append((inside(z + way), ((z + way) * ys + y, g, j)))
+        for n in range(1, ys):
+            targets.append((None, (z * ys + (y + n) % ys, g, j)))
+        for condition, device in targets:
+            base = slot * each
+
+            def run():
+                act(base, device)
+
+            if condition is None:
+                run()
+            else:
+                pl.when(condition)(run)
+            slot += 1
+
+    def own_first(base, device):
+        kv_copy(kv_ref.at[g], own_block, own_send.at[base], device).start()
+        decay_copy(decay_ref, member, own_send.at[base + 1], device).start()
+
+    def own_second(base, device):
+        landed = kv_all.at[rows_of(other_block)]
+        kv_copy(landed, other_block, own_send.at[base + 2], device).start()
+
+    def own_drain(base, device):
+        kv_copy(kv_ref.at[g], own_block, own_send.at[base], device).wait_send()
+        decay_copy(decay_ref, member, own_send.at[base + 1], device).wait_send()
+        landed = kv_all.at[rows_of(other_block)]
+        kv_copy(landed, other_block, own_send.at[base + 2], device).wait_send()
+
+    own_to(own_first)
+
+    def far_copy(n):
+        source = decay_ref.at[
+            :, pl.ds(pl.multiple_of(((1 - g) * half_count + half_count - 1 - n) * rows, rows), rows)
+        ]
+        return remote(
+            source, far_decay.at[j], far_send.at[n], far_recv.at[j], (mirror[0], g, n)
+        )
+
+    for n in range(half_count):
+        far_copy(n).start()
+
+    def q_copy(pair):
+        return remote(
+            query_ref.at[:, q_lanes(1 - g, pair)], far_q.at[pair], q_send.at[pair],
+            q_recv.at[pair], mirror,
+        )
+
+    q_copy(0).start()
+
+    kv_all[rows_of(own_block)] = kv_ref[g]
+    decay_all[member] = decay_ref[...]
+    acc_ref[...] = jnp.zeros_like(acc_ref)
+    low = lax.broadcasted_iota(jnp.int32, (rows, 128), 1) < 64
+
+    def unpack(r, pair, both):
+        both = both.astype(jnp.float32)
+        even = jnp.where(low, both, 0.0)
+        odd = jnp.where(low, pltpu.roll(both, 64, 1), 0.0)
+        q_ref[r, (2 * pair) * rows : (2 * pair + 1) * rows] = even.astype(jnp.bfloat16)
+        q_ref[r, (2 * pair + 1) * rows : (2 * pair + 2) * rows] = odd.astype(jnp.bfloat16)
+
+    def shifts(r, pair, values):
+        turned = values.T
+        for n in range(2):
+            part = pl.ds((2 * pair + n) * rows, rows)
+            peak_ref[r, part] = jnp.broadcast_to(turned[:, n : n + 1], (rows, 128))
+
+    def eight(two):
+        return jnp.concatenate([two, two, two, two], axis=0)
+
+    for pair in range(pairs):
+        unpack(0, pair, query_ref[:, q_lanes(g, pair)])
+
+    kv_copy(kv_ref.at[g], other_block, x_send, here).wait_recv()
+    own_to(own_second)
+    for pair in range(1, pairs):
+        q_copy(pair).start()
+    for n in range(1, half_count):
+        arrived(s, (j + n) % half_count)
+
+    for pair in range(pairs):
+        first = (2 * pair) % local
+        span = pl.ds(pl.multiple_of(offset, rows), rows)
+        two = decay_all[s * half_count + (2 * pair) // local, first : first + 2, span]
+        shifts(0, pair, eight(two))
+
+    def pair_step(r, chunk, block, pair, masked, start):
+        at = pl.ds(pl.multiple_of((chunk * blocks + block) * key_block, key_block), key_block)
+        keys = kv_all[at]
+        upper = lax.broadcasted_iota(jnp.int32, (key_block, 128), 1) >= 64
+        pick = jnp.where(upper, 1.0, 0.0).astype(jnp.bfloat16)
+        ones = jnp.where(upper, 0.0, 1.0).astype(jnp.bfloat16)
+        values = keys * pick + ones
+        part = pl.ds(pair * 2 * rows, 2 * rows)
+        if not isinstance(pair, int):
+            part = pl.ds(pl.multiple_of(pair * 2 * rows, 2 * rows), 2 * rows)
+        scores = lax.dot_general(
+            q_ref[r, part], keys, (((1,), (1,)), ((), ())), preferred_element_type=jnp.float32
+        )
+        before = peak_ref[r, part]
+        scores = scores + jnp.concatenate([before] * (key_block // 128), axis=1)
+        first = (2 * pair) % local
+        lanes = pl.ds(pl.multiple_of(block * key_block, key_block), key_block)
+        decays = decay_all[chunk * half_count + (2 * pair) // local, pl.ds(first, 2), lanes]
+        scores = scores.reshape(2, rows, key_block) - decays[:, None, :]
+        if masked:
+            row = start + lax.broadcasted_iota(jnp.int32, (rows, key_block), 0)
+            col = block * key_block + lax.broadcasted_iota(jnp.int32, (rows, key_block), 1)
+            scores = jnp.where((col <= row)[None], scores, -1e30)
+        weights = jnp.exp2(scores.reshape(2 * rows, key_block)).astype(jnp.bfloat16)
+        acc_ref[r, part] += jnp.dot(weights, values, preferred_element_type=jnp.float32)
+
+    def diagonal(r, chunk, some, start):
+        full = start // key_block
+
+        def whole(block, carry):
+            for pair in some:
+                pair_step(r, chunk, block, pair, False, start)
+            return carry
+
+        lax.fori_loop(0, full, whole, 0)
+        for pair in some:
+            pair_step(r, chunk, full, pair, True, start)
+
+    def finished(r, pair):
+        at = 2 * pair * rows
+        even = acc_ref[r, pl.ds(at, rows)]
+        odd = acc_ref[r, pl.ds(at + rows, rows)]
+        done = jnp.where(low, pltpu.roll(even, 64, 1), odd) / jnp.where(
+            low, even, pltpu.roll(odd, 64, 1)
+        )
+        return done.astype(jnp.bfloat16)
+
+    def prepare(some):
+        for pair in some:
+            remote(
+                query_ref.at[:, q_lanes(1 - g, pair)], far_q.at[pair], q_send.at[pair],
+                q_recv.at[pair], here,
+            ).wait_recv()
+            unpack(1, pair, far_q[pair])
+            first = (2 * pair) % local
+            two = far_decay[(2 * pair) // local, first : first + 2]
+            shifts(1, pair, eight(two))
+
+    def far_ready():
+        for n in range(half_count):
+            remote(
+                decay_ref.at[:, pl.ds(0, rows)], far_decay.at[n], far_send.at[n],
+                far_recv.at[n], here,
+            ).wait_recv()
+
+    halves = (tuple(range(pairs // 2)), tuple(range(pairs // 2, pairs)))
+    diagonal(0, s, halves[0], offset)
+    round_of(1, True)
+    diagonal(0, s, halves[1], offset)
+
+    def item(k, carry):
+        lanes_of(k)
+        far = k > s
+        r = jnp.where(far, 1, 0)
+        back = jnp.where(y == 0, jnp.where(k == 1, ys, jnp.where(k == ys, 1, k)), k)
+        chunk = jnp.where(far, k - s - 1, s - back)
+
+        @pl.when(k == s + 1)
+        def _():
+            far_ready()
+            prepare(halves[0])
+
+        for block in range(blocks):
+            for pair in halves[0]:
+                pair_step(r, chunk, block, pair, False, 0)
+
+        @pl.when(k < zs)
+        def _():
+            round_of(k + 1, True)
+
+        @pl.when(k == s + 1)
+        def _():
+            prepare(halves[1])
+
+        for block in range(blocks):
+            for pair in halves[1]:
+                pair_step(r, chunk, block, pair, False, 0)
+        return carry
+
+    lax.fori_loop(1, zs + 1, item, 0)
+
+    @pl.when(s >= zs)
+    def _():
+        far_ready()
+        prepare(range(pairs))
+
+    far_chunk = sp_count - 1 - s
+
+    def back_copy(pair, device):
+        return remote(
+            res_ref.at[pair], out_ref.at[:, q_lanes(g, pair)], back_send.at[pair],
+            back_recv.at[pair], device,
+        )
+
+    for pair in range(pairs):
+
+        def far_item(chunk, carry):
+            for block in range(blocks):
+                pair_step(1, chunk, block, pair, False, 0)
+            return carry
+
+        lax.fori_loop(jnp.maximum(zs - s, 0), far_chunk, far_item, 0)
+        diagonal(1, far_chunk, (pair,), far_offset)
+        res_ref[pair] = finished(1, pair)
+        back_copy(pair, mirror).start()
+
+    def last_item(index, carry):
+        for pair in range(pairs):
+            pair_step(0, index // blocks, index % blocks, pair, False, 0)
+        return carry
+
+    lax.fori_loop(0, jnp.maximum(s - zs, 0) * blocks, last_item, 0)
+    for pair in range(pairs):
+        out_ref[:, q_lanes(g, pair)] = finished(0, pair)
+
+    x_copy.wait_send()
+    own_to(own_drain)
+
+    def drain(k, carry):
+        round_of(k, False)
+        return carry
+
+    lax.fori_loop(1, zs + 1, drain, 0)
+    for n in range(half_count):
+        far_copy(n).wait_send()
+    for pair in range(pairs):
+        q_copy(pair).wait_send()
+        back_copy(pair, mirror).wait_send()
+        remote(
+            res_ref.at[pair], out_ref.at[:, q_lanes(1 - g, pair)], back_send.at[pair],
+            back_recv.at[pair], here,
+        ).wait_recv()
+
+
+def lines_of(sp_count):
+    ys = 1 << ((sp_count.bit_length() - 1) // 2)
+    return sp_count // ys, ys
+
+
+def stream(queries, kv_blocks, decays, sizes):
+    sp_count, kv_heads, half_count = sizes
+    rows = queries.shape[0]
+    heads = queries.shape[1] // 64 // kv_heads
+    local, chunk_rows = decays.shape
+    zs, ys = lines_of(sp_count)
+    pairs = heads // 2
+    count = sp_count * kv_heads * half_count
+    members = sp_count * half_count
+    per = 1 + (ys - 1) + (half_count - 1) + (ys - 1) * (half_count - 1)
+    each = kv_heads + 1
+    vmem = pl.BlockSpec(memory_space=pltpu.VMEM)
+    dma = pltpu.SemaphoreType.DMA
+    return pl.pallas_call(
+        lambda *refs: stream_kernel(
+            *refs, sizes=sizes, lines=(zs, ys), rows=rows, heads=heads,
+            key_block=math.gcd(chunk_rows, KEY_BLOCK),
+        ),
+        out_shape=jax.ShapeDtypeStruct(queries.shape, jnp.bfloat16),
+        in_specs=[vmem] * 3,
+        out_specs=vmem,
+        scratch_shapes=[
+            pltpu.VMEM((rows * count, 128), jnp.bfloat16),
+            pltpu.VMEM((members, local, chunk_rows), jnp.float32),
+            pltpu.VMEM((half_count, local, rows), jnp.float32),
+            pltpu.VMEM((pairs, rows, 128), jnp.bfloat16),
+            pltpu.VMEM((2, heads * rows, 128), jnp.bfloat16),
+            pltpu.VMEM((2, heads * rows, 128), jnp.float32),
+            pltpu.VMEM((2, heads * rows, 128), jnp.float32),
+            pltpu.VMEM((pairs, rows, 128), jnp.bfloat16),
+            dma((count,)), dma((members,)), dma, dma(((ys + half_count) * each,)),
+            dma((zs * 2 * per * each,)), dma((half_count,)), dma((half_count,)),
+            dma((pairs,)), dma((pairs,)), dma((pairs,)), dma((pairs,)),
+        ],
+        compiler_params=pltpu.CompilerParams(
+            has_side_effects=True, vmem_limit_bytes=44 * 1024 * 1024
+        ),
+        name="stream",
+    )(kv_blocks, queries, decays)
+
+
+def any_scores(queries, kv_blocks, decays, sizes):
+    sp_count, kv_heads, half_count = sizes
     group = lax.axis_index("kv")
     me = (lax.axis_index("sp") * kv_heads + group) * half_count + lax.axis_index("half")
-    count = sp_count * tp_count
+    count = sp_count * kv_heads * half_count
     mirror = [(i, count - 1 - i) for i in range(count)]
-    head_size = query_gain.shape[0]
-    rows = inputs.shape[0]
+    rows = queries.shape[0]
     length = rows * count
-    all_heads = w_query.shape[1] // head_size
-    heads = all_heads // kv_heads
-    width = heads * head_size
+    heads = queries.shape[1] // 64 // kv_heads
+    width = heads * 64
     members = sp_count * half_count
     key_block = math.gcd(length, KEY_BLOCK)
 
     def choose(a, b):
         return jnp.where(group == 0, a, b)
 
-    normed = rms_norm(inputs.astype(jnp.float32), in_gain).astype(jnp.bfloat16)
-    keys = rms_norm(
-        jnp.dot(normed, w_key, preferred_element_type=jnp.float32).reshape(
-            rows, kv_heads, head_size
-        ),
-        key_gain,
-    ).astype(jnp.bfloat16)
-    values = (
-        jnp.dot(normed, w_value, preferred_element_type=jnp.float32)
-        .astype(jnp.bfloat16)
-        .reshape(rows, kv_heads, head_size)
-    )
-    pairs = jnp.concatenate([keys, values], axis=2)
-    kv_blocks = pairs.transpose(1, 0, 2)
-    decay_rows = (decay_sums.T * LOG2E).reshape(-1, 128)
-
-    queries = rms_norm(
-        jnp.dot(normed, w_query, preferred_element_type=jnp.float32).reshape(
-            rows, all_heads, head_size
-        ),
-        query_gain * (LOG2E * head_size ** (-0.5)),
-    ).astype(jnp.bfloat16).reshape(rows, kv_heads * width)
+    decay_rows = decays.reshape(-1, 128)
     own_q = choose(queries[:, :width], queries[:, width:])
     sent_q = choose(queries[:, width:], queries[:, :width])
     vmem = pl.BlockSpec(memory_space=pltpu.VMEM)
     chips = count // 2
     dma = pltpu.SemaphoreType.DMA
     kv, far_q, decay_all = pl.pallas_call(
-        lambda *refs: exchange_kernel(
-            *refs, rows=rows, sizes=(sp_count, kv_heads, half_count)
-        ),
+        lambda *refs: exchange_kernel(*refs, rows=rows, sizes=sizes),
         out_shape=(
             jax.ShapeDtypeStruct((length, 128), jnp.bfloat16),
             jax.ShapeDtypeStruct((rows, width), jnp.bfloat16),
@@ -297,16 +700,48 @@
             for first in firsts
         ]
     )
+    attended = attend(place, own_q, far_q, row_decay, decay_all, kv, False)
+    back = lax.ppermute(attended[1], ALL, mirror)
+    return choose(
+        jnp.concatenate([attended[0], back], axis=1), jnp.concatenate([back, attended[0]], axis=1)
+    )
+
+
+def per_device(inputs, in_gain, w_query, w_key, w_value, query_gain, key_gain, decay_sums, w_out):
+    kv_heads = lax.axis_size("kv")
+    sizes = (lax.axis_size("sp"), kv_heads, lax.axis_size("half"))
+    head_size = query_gain.shape[0]
+    rows = inputs.shape[0]
+    all_heads = w_query.shape[1] // head_size
+
+    normed = rms_norm(inputs.astype(jnp.float32), in_gain).astype(jnp.bfloat16)
+    keys = rms_norm(
+        jnp.dot(normed, w_key, preferred_element_type=jnp.float32).reshape(
+            rows, kv_heads, head_size
+        ),
+        key_gain,
+    ).astype(jnp.bfloat16)
+    values = (
+        jnp.dot(normed, w_value, preferred_element_type=jnp.float32)
+        .astype(jnp.bfloat16)
+        .reshape(rows, kv_heads, head_size)
+    )
+    pairs = jnp.concatenate([keys, values], axis=2)
+    kv_blocks = pairs.transpose(1, 0, 2)
+    decays = decay_sums.T * LOG2E
+
+    queries = rms_norm(
+        jnp.dot(normed, w_query, preferred_element_type=jnp.float32).reshape(
+            rows, all_heads, head_size
+        ),
+        query_gain * (LOG2E * head_size ** (-0.5)),
+    ).astype(jnp.bfloat16).reshape(rows, all_heads * head_size)
     bound = head_size**0.5 * LOG2E * jnp.max(query_gain) * jnp.max(key_gain)
-    attended = lax.cond(
+    whole = lax.cond(
         bound <= SMALL,
-        lambda *given: attend(*given, True),
-        lambda *given: attend(*given, False),
-        place, own_q, far_q, row_decay, decay_all, kv,
-    )
-    back = lax.ppermute(attended[1], ALL, mirror)
-    whole = choose(
-        jnp.concatenate([attended[0], back], axis=1), jnp.concatenate([back, attended[0]], axis=1)
+        lambda *given: stream(*given, sizes),
+        lambda *given: any_scores(*given, sizes),
+        queries, kv_blocks, decays,
     )
     return jnp.dot(whole, w_out, preferred_element_type=jnp.float32).astype(jnp.bfloat16)
 

time: 140 us -> 140 us (level)
  other arithmetic: 9.2 us -> 7.68 us
  local copies, waits for them, and re-layouts: 4.11 us -> 5.53 us
    cond x0 -> x4, local copies, waits for them, and re-layouts: none -> 2.54 us
where the time goes in v1:
time: 140 us; the launch traced here: 139 us
  Pallas kernels  99.2 us (71%)
  waiting for transfers between devices  13.4 us (10%)
  matrix products  11.4 us (8%)
  other arithmetic  7.68 us (5%)
  local copies, waits for them, and re-layouts  5.53 us (4%)
  between operations  1.43 us (1%)
    pallas_call x1, Pallas kernels, any_scores(): pl.pallas_call(lambda *refs: exchange_kernel(*refs, rows=rows, sizes=size...  51.6 us
    pallas_call x1, Pallas kernels, attend(): pl.pallas_call(lambda *refs: attend_kernel(*refs, rows=rows, heads=heads,...  47.6 us
    ppermute x1, waiting for transfers between devices, any_scores(): back = lax.ppermute(attended[1], ALL, mirror)  13.4 us
    dot_general x1, matrix products, per_device(): jnp.dot(normed, w_query, preferred_element_type=jnp.float32)  4.47 us
    dot_general x1, matrix products, per_device(): jnp.dot(whole, w_out, preferred_element_type=jnp.float32)  4.41 us
  transfers between devices with their start and end apart: 1, of which 1 were waited for; matrix products, arithmetic and copies ran while one was open for 0% of the time, Pallas kernels for 0%

profile of v1, /device:TPU:9, one launch (start us, length us, event | category | flops | bytes accessed | tf_op | source)
XLA Modules:
  0.0 139.5 jit_solution(17228516531441728476)
XLA Ops:
  0.0 1.4 %reduce_max.19 = f32[]{:T(128)} reduce(f32[64]{0:T(128)} %param.17, f32[]{:T(128)} %constant.73.clone.1), dimensions={0}, to_apply=%region_1.0 | reduce | flops 63 | bytes 264 | tf_op jit(solution)/shard_map/reduce_max | solution.py:739
  1.5 1.5 %fusion = f32[256]{0:T(256)S(1)} fusion(bf16[256,2048]{1,0:T(8,128)(2,1)} %param.11), kind=kLoop, calls=%fused_computation.12 | loop fusion | flops 1572608 | bytes 1049600 | tf_op jit(solution)/shard_map/reduce_sum | solution.py:20
  3.0 1.3 broadcast_multiply_fusion
  5.6 0.7 multiply_bitcast_fusion
  6.3 2.0 %convolution_convert_fusion.1 = bf16[256,128]{0,1:T(8,128)(2,1)S(1)} fusion(bf16[2048,128]{1,0:T(8,128)(2,1)} %param.15, bf16[256,2048]{1,0:T(8,128)(2,1)} %param.11, f32[2048]{0:T(1024)} %param.12, f32[256]{0:T(256)S(1)} %add_rsqrt_fusion.2), kind=kOutput, calls=%fused_computation.15 | convolution fusion | flops 136347648 | bytes 1647616 | tf_op jit(solution)/shard_map/dot_general | solution.py:725
  8.3 0.1 copy.25
  8.5 0.6 multiply_reduce_fusion
  9.1 0.1 copy.24
  9.2 0.1 multiply_convert_fusion.1
  9.5 4.5 %fusion.8 = (f32[256,1024]{1,0:T(8,128)S(1)}, f32[256,1024]{1,0:T(8,128)}) fusion(bf16[2048,1024]{1,0:T(8,128)(2,1)} %param.13, bf16[256,2048]{1,0:T(8,128)(2,1)S(1)} %copy-done.3, f32[2048]{0:T(1024)S(1)} %copy-done.5, f32[256]{0:T(256)S(1)} %add_rsqrt_fusion.2), kind=kOutput, calls=%fused_computation.28 | convolution fusion | flops 1076101120 | bytes 7349248 | tf_op jit(solution)/shard_map/dot_general | solution.py:734
  13.9 0.3 copy.22
  14.5 0.3 copy.23
  14.8 1.4 %multiply_convert_fusion = bf16[256,1024]{1,0:T(8,128)(2,1)S(1)} fusion(f32[256,1024]{1,0:T(8,128)} %get-tuple-element.38, f32[256,1024]{1,0:T(8,128)S(1)} %copy.23, f32[1024]{0:T(1024)S(1)} %mul.112), kind=kLoop, calls=%fused_computation.17 | loop fusion | flops 786432 | bytes 2625536 | tf_op jit(solution)/shard_map/convert_element_type | solution.py:738
  16.2 118.8 %conditional.1 = (bf16[256,1024]{1,0:T(8,128)(2,1)S(1)}) conditional(s32[]{:T(128)} %convert_element_type.22, (bf16[256,1024]{1,0:T(8,128)(2,1)S(1)}, f32[4,1024]{1,0:T(4,128)S(1)}, bf16[2,256,128]{2,1,0:T(8,128)(2,1)S(1)}) %tuple.11, (bf16[2,256,128]{2,1,0:T(8,128)(2,1)S(1)}, bf16[256,1024]{1,0:T(8,128)(2,1)S(1)}, f32[4,1024]{1,0:T(4,128)S(1)}) %tuple.12), branch_computations={%region_5.6_spmd, %region_6.7_spmd} | conditional | flops 2625604 | bytes 14811961 | solution.py:740
  16.3 0.6 reshape.42.refs_2_
  16.9 0.7 broadcast_select_fusion
  17.7 51.6 %exchange.1 = (bf16[8192,128]{1,0:T(8,128)(2,1)}, bf16[256,512]{1,0:T(8,128)(2,1)}, f32[16,32,128]{2,1,0:T(8,128)}) custom-call(bf16[2,256,128]{2,1,0:T(8,128)(2,1)S(1)} %get-tuple-element.21.refs_0_, bf16[256,512]{1,0:T(8,128)(2,1)} %get-tuple-element.31.refs_1_, f32[32,128]{1,0:T(8,128)} %reshape.42.refs_2_), custom_call_target="tpu_custom_call" | custom-call | tf_op jit(solution)/shard_map/cond/branch_0_fun/exchange/pallas_call | solution.py:675
  69.3 1.1 reshape.43
  70.7 1.6 %copy-done.1 = bf16[8192,128]{1,0:T(8,128)(2,1)S(1)} copy-done((bf16[8192,128]{1,0:T(8,128)(2,1)S(1)}, bf16[8192,128]{1,0:T(8,128)(2,1)}, u32[]{:S(2)}) %copy-start.1) | copy-done | bytes 2097176 | tf_op jit(solution)/shard_map/cond
  72.3 0.9 copy-done.2
  73.2 47.6 %attend_any.1 = bf16[2,256,512]{2,1,0:T(8,128)(2,1)S(1)} custom-call(s32[2]{0:T(128)S(1)} %pad_add_fusion.refs_0_, bf16[256,512]{1,0:T(8,128)(2,1)S(1)} %get-tuple-element.32.refs_1_, bf16[256,512]{1,0:T(8,128)(2,1)S(1)} %copy-done.2, f32[2,256,8]{2,1,0:T(8,128)S(1)} %copy.21.refs_3_, f32[16,8,512]{2,1,0:T(8,128)S(1)} %bitcast.37, ...), custom_call_target="tpu_custom_call" | custom-call | tf_op jit(solution)/shard_map/cond/branch_0_fun/attend_any/pallas_call | solution.py:204
  121.0 13.4 %collective-permute-done = bf16[256,512]{1,0:T(8,128)(2,1)S(1)} collective-permute-done((bf16[256,512]{1,0:T(8,128)(2,1)S(1)}, bf16[256,512]{1,0:T(8,128)(2,1)S(1)}, u32[]{:S(2)}, u32[]{:S(2)}) %collective-permute-start) | collective-permute-done | bytes 262176 | tf_op jit(solution)/shard_map/cond/branch_0_fun/ppermute | solution.py:704
  134.4 0.1 maximum_select_fusion
  135.0 4.4 %convolution_convert_fusion = bf16[256,2048]{1,0:T(8,128)(2,1)} fusion(bf16[256,1024]{1,0:T(8,128)(2,1)S(1)} %get-tuple-element.41, bf16[1024,2048]{1,0:T(8,128)(2,1)} %param.19), kind=kOutput, calls=%fused_computation.11 | convolution fusion | flops 1074266112 | bytes 5767168 | tf_op jit(solution)/shard_map/dot_general | solution.py:746
  (25 shorter events, 0.8 us)
Async XLA Ops:
  0.0 8.4 %copy-start = (bf16[2048,128]{1,0:T(8,128)(2,1)S(1)}, bf16[2048,128]{1,0:T(8,128)(2,1)}, u32[]{:S(2)}) copy-start(bf16[2048,128]{1,0:T(8,128)(2,1)} %param.14) | copy-start | bytes 1572868
  0.0 8.4 %copy-start.3 = (bf16[256,2048]{1,0:T(8,128)(2,1)S(1)}, bf16[256,2048]{1,0:T(8,128)(2,1)}, u32[]{:S(2)}) copy-start(bf16[256,2048]{1,0:T(8,128)(2,1)} %param.11) | copy-start | bytes 3145732
  0.0 8.4 %copy-start.5 = (f32[2048]{0:T(1024)S(1)}, f32[2048]{0:T(1024)}, u32[]{:S(2)}) copy-start(f32[2048]{0:T(1024)} %param.12) | copy-start | bytes 24580
  6.3 2.9 %copy-start.4 = (f32[64]{0:T(128)S(1)}, f32[64]{0:T(128)}, u32[]{:S(2)}) copy-start(f32[64]{0:T(128)} %param.17) | copy-start | bytes 772
  70.7 1.6 %copy-start.1 = (bf16[8192,128]{1,0:T(8,128)(2,1)S(1)}, bf16[8192,128]{1,0:T(8,128)(2,1)}, u32[]{:S(2)}) copy-start(bf16[8192,128]{1,0:T(8,128)(2,1)} %get-tuple-element.25.refs_5_) | copy-start | bytes 6291460 | tf_op jit(solution)/shard_map/cond
  72.3 0.9 copy-start.2
  120.9 13.5 %collective-permute-start = (bf16[256,512]{1,0:T(8,128)(2,1)S(1)}, bf16[256,512]{1,0:T(8,128)(2,1)S(1)}, u32[]{:S(2)}, u32[]{:S(2)}) collective-permute-start(bf16[256,512]{1,0:T(8,128)(2,1)S(1)} %get-tuple-element.30), channel_id=1, source_target_pairs={{0,31},{1,30},{2,29},{3,28},{4,27},{5,26},{6,25},{7,24},{8,23},{9,... | collective-permute-start | bytes 786440 | tf_op jit(solution)/shard_map/cond/branch_0_fun/ppermute | solution.py:704

commit v2 on v0

--- a/solution.py
+++ b/solution.py
@@ -219,58 +219,709 @@
     )(place, near, far, row_decay, decays, kv)
 
 
-def per_device(inputs, in_gain, w_query, w_key, w_value, query_gain, key_gain, decay_sums, w_out):
-    sp_count = lax.axis_size("sp")
-    kv_heads = lax.axis_size("kv")
-    half_count = lax.axis_size("half")
-    tp_count = kv_heads * half_count
+def stream_kernel(
+    kvt_ref, query_ref, decay_ref, out_ref, kvt_all, decay_all, far_decay, in_q, qt_ref, acc_ref,
+    kp_all, vt_all, res_ref, kv_recv, decay_recv, x_send, own_send, round_send, late_send,
+    far_send, far_recv, q_send, q_recv, back_send, back_recv, *, sizes, lines, rows, heads
+):
+    sp_count, kv_heads, half_count = sizes
+    zs, ys = lines
+    zh = zs // 2
+    upper = sp_count // 2
+    pairs = heads // 2
+    units = pairs * kv_heads
+    width = heads * 64
+    span = 2 * rows
+    local, chunk_rows = decay_ref.shape
+    s, g, j = lax.axis_index("sp"), lax.axis_index("kv"), lax.axis_index("half")
+    z, y = s // ys, s % ys
+    partner_x = 1 - g
+    s_far = sp_count - 1 - s
+    is_high = s >= upper
+
+    def share(s_):
+        return (2 * units * (2 * s_ + 1 - sp_count) + 2 * s_ + 1) // (2 * (2 * s_ + 1))
+
+    given = jnp.where(is_high, share(jnp.maximum(s, upper)), 0)
+    taken = jnp.where(is_high, 0, share(jnp.maximum(s_far, upper)))
+
+    def kept_from(x_):
+        return (jnp.maximum(given - x_, 0) + kv_heads - 1) // kv_heads
+
+    def block_at(s_, x_, j_):
+        return (s_ * kv_heads + x_) * half_count + j_
+
+    def remote(source, target, send, recv, device):
+        return pltpu.make_async_remote_copy(
+            src_ref=source, dst_ref=target, send_sem=send, recv_sem=recv, device_id=device,
+            device_id_type=pl.DeviceIdType.MESH,
+        )
+
+    def kv_copy(source, block, send, device):
+        return remote(source, kvt_all.at[block], send, kv_recv.at[block], device)
+
+    def decay_copy(source, member, send, device):
+        return remote(source, decay_all.at[member], send, decay_recv.at[member], device)
+
+    here = (s, g, j)
+    each = kv_heads + 1
+
+    def package(s_, j_, base, device, sems):
+        copies = []
+        for x_ in range(kv_heads):
+            block = block_at(s_, x_, j_)
+            copies.append(kv_copy(kvt_all.at[block], block, sems.at[base + x_], device))
+        member = s_ * half_count + j_
+        copies.append(
+            decay_copy(decay_all.at[member], member, sems.at[base + kv_heads], device)
+        )
+        return copies
+
+    def arrived(s_, j_):
+        for copy in package(s_, j_, 0, here, own_send):
+            copy.wait_recv()
+
+    def start_all(copies):
+        for copy in copies:
+            copy.start()
+
+    def drain_all(copies):
+        for copy in copies:
+            copy.wait_send()
+
+    def inside(z_):
+        return (z_ >= 0) & (z_ < zs)
+
+    def others(s_, base, sems, act, z_=None):
+        slot = 0
+        if z_ is None:
+            for n in range(1, ys):
+                to = (z * ys + (y + n) % ys, g, j)
+                act(package(s_, j, base + slot * each, to, sems))
+                slot += 1
+        for n in range(1, half_count):
+            to = (s, g, (j + n) % half_count)
+            act(package(s_, j, base + slot * each, to, sems))
+            slot += 1
+
+    per = 1 + (ys - 1) + (half_count - 1) + (ys - 1) * (half_count - 1)
+
+    def near_from(z_, way):
+        return inside(z_) if way > 0 else inside(z_) & (z_ < zh)
+
+    def round_of(k, go):
+        act = start_all if go else drain_all
+        for d, way in enumerate((1, -1)):
+            base = ((k - 1) * 2 + d) * per * each
+
+            @pl.when(near_from(z - way * k, way))
+            def _():
+                s_ = (z - way * k) * ys + y
+                if go:
+                    arrived(s_, j)
+
+                @pl.when(inside(z + way))
+                def _():
+                    act(package(s_, j, base, ((z + way) * ys + y, g, j), round_send))
+
+                others(s_, base + each, round_send, act)
+
+            reach = near_from(z - way * (k - 1), way)
+            if way < 0:
+                reach = reach & (k != 1)
+
+            @pl.when(reach)
+            def _():
+                for m in range(1, ys):
+                    s_ = (z - way * (k - 1)) * ys + (y + m) % ys
+                    if go:
+                        arrived(s_, j)
+                    slot = ys + half_count - 1 + (m - 1) * (half_count - 1)
+                    others(s_, base + slot * each, round_send, act, z)
+
+    def late(zo, go):
+        act = start_all if go else drain_all
+        base = (zo - zh) * per * each
+
+        @pl.when((zo > z) & (zo < zs))
+        def _():
+            s_ = zo * ys + y
+            if go:
+                arrived(s_, j)
+
+            @pl.when(z > 0)
+            def _():
+                act(package(s_, j, base, ((z - 1) * ys + y, g, j), late_send))
+
+            @pl.when(zo <= zs - 1 - z)
+            def _():
+                others(s_, base + each, late_send, act)
+
+    def late_across(zo, go):
+        act = start_all if go else drain_all
+        base = (zo - zh) * per * each
+
+        @pl.when((zo > z) & (zo <= zs - 1 - z))
+        def _():
+            for m in range(1, ys):
+                s_ = zo * ys + (y + m) % ys
+                if go:
+                    arrived(s_, j)
+                slot = ys + half_count - 1 + (m - 1) * (half_count - 1)
+                others(s_, base + slot * each, late_send, act, z)
+
+    def build(s_):
+        for x_ in range(kv_heads):
+            for j_ in range(half_count):
+                block = block_at(s_, x_, j_)
+                place = (x_ * half_count + j_) * rows
+                decays = jnp.concatenate(
+                    [
+                        decay_all[s_ * half_count + n, :, pl.ds(place, rows)]
+                        for n in range(half_count)
+                    ],
+                    axis=0,
+                )
+                decays = -decays
+                high = decays.astype(jnp.bfloat16).astype(jnp.float32)
+                rest = decays - high
+                middle = rest.astype(jnp.bfloat16).astype(jnp.float32)
+                parts = jnp.concatenate(
+                    [high, middle, rest - middle, jnp.ones((8, rows), jnp.float32)], axis=0
+                ).astype(jnp.bfloat16)
+                wide = jnp.concatenate(
+                    [kvt_all[block, 0:64], parts, jnp.zeros((32, rows), jnp.bfloat16)], axis=0
+                )
+                kp_all[s_, pl.ds(place, rows)] = wide.T
+                vt_all[s_, 0:64, pl.ds(place, rows)] = kvt_all[block, 64:128]
+
+    def build_if(s_):
+        @pl.when(s_ <= jnp.where(is_high, s, s_far))
+        def _():
+            build(s_)
+
+    def lanes_of(k):
+        for way in (1, -1):
+
+            @pl.when(near_from(z - way * k, way))
+            def _():
+                s_ = (z - way * k) * ys + y
+                for n in range(1, half_count):
+                    arrived(s_, (j + n) % half_count)
+                build_if(s_)
+
+            reach = near_from(z - way * (k - 1), way)
+            if way < 0:
+                reach = reach & (k != 1)
+
+            @pl.when(reach)
+            def _():
+                for m in range(1, ys):
+                    s_ = (z - way * (k - 1)) * ys + (y + m) % ys
+                    for n in range(1, half_count):
+                        arrived(s_, (j + n) % half_count)
+                    build_if(s_)
+
+    def late_lanes(zo):
+        @pl.when((zo > z) & (zo <= zs - 1 - z))
+        def _():
+            for m in range(ys):
+                s_ = zo * ys + (y + m) % ys
+                for n in range(1, half_count):
+                    arrived(s_, (j + n) % half_count)
+                build_if(s_)
+
+    def q_lanes(group, pair):
+        return pl.ds(pl.multiple_of(group * width + pair * 128, 128), 128)
+
+    def far_q_copy(group, pair):
+        unit = kv_heads * pair + g
+        slot = jnp.minimum(pairs + unit, 2 * pairs - 1)
+        return remote(
+            query_ref.at[:, q_lanes(group, pair)], in_q.at[slot],
+            q_send.at[group * pairs + pair], q_recv.at[slot], (s_far, group, j),
+        )
+
+    def near_q_copy(pair):
+        return remote(
+            query_ref.at[:, q_lanes(partner_x, pair)], in_q.at[pair],
+            q_send.at[partner_x * pairs + pair], q_recv.at[pair], (s, partner_x, j),
+        )
+
+    def q_arrived(slot):
+        remote(
+            query_ref.at[:, pl.ds(0, 128)], in_q.at[slot], q_send.at[0], q_recv.at[slot], here
+        ).wait_recv()
+
+    def is_given(pair, x_):
+        return kv_heads * pair + x_ < given
+
+    def far_sends(act):
+        for pair in range(pairs):
+            for group in range(kv_heads):
+
+                @pl.when(is_given(pair, g))
+                def _():
+                    act([far_q_copy(group, pair)])
+
+    def near_sends(act):
+        for pair in range(pairs):
+
+            @pl.when(jnp.logical_not(is_given(pair, g)))
+            def _():
+                act([near_q_copy(pair)])
+
+    def far_decay_copies():
+        copies = []
+        for x_ in range(kv_heads):
+            for n in range(half_count):
+                source = decay_ref.at[:, pl.ds((x_ * half_count + n) * rows, rows)]
+                at = x_ * half_count + n
+                copies.append(
+                    remote(
+                        source, far_decay.at[x_ * half_count + j], far_send.at[at],
+                        far_recv.at[x_ * half_count + j], (s_far, g, n),
+                    )
+                )
+        return copies
+
+    own_block = block_at(s, g, j)
+    other_block = block_at(s, partner_x, j)
+    member = s * half_count + j
+
+    def side_targets():
+        targets = [(None, (s, g, (j + n) % half_count)) for n in range(1, half_count)]
+        targets.append((inside(z + 1), ((z + 1) * ys + y, g, j)))
+        targets += [(None, (z * ys + (y + n) % ys, g, j)) for n in range(1, ys)]
+        return targets
+
+    down = (jnp.maximum(z - 1, 0) * ys + y, g, j)
+    down_base = (ys + half_count - 1) * each
+
+    def each_side(act):
+        for slot, (condition, device) in enumerate(side_targets()):
+            if condition is None:
+                act(slot * each, device)
+            else:
+
+                @pl.when(condition)
+                def _():
+                    act(slot * each, device)
+
+    def own_copies(base, device):
+        return [
+            kv_copy(kvt_ref.at[g], own_block, own_send.at[base], device),
+            decay_copy(decay_ref, member, own_send.at[base + 1], device),
+        ]
+
+    def other_copies(base, device):
+        return [kv_copy(kvt_all.at[other_block], other_block, own_send.at[base + 2], device)]
+
+    x_copy = kv_copy(kvt_ref.at[partner_x], own_block, x_send, (s, partner_x, j))
+    x_copy.start()
+    each_side(lambda base, device: start_all(own_copies(base, device)))
+
+    @pl.when(is_high)
+    def _():
+        far_sends(start_all)
+        start_all(far_decay_copies())
+
+    @pl.when(z > 0)
+    def _():
+        start_all(own_copies(down_base, down))
+
+    near_sends(start_all)
+    kvt_all[own_block] = kvt_ref[g]
+    decay_all[member] = decay_ref[...]
+    acc_ref[...] = jnp.zeros_like(acc_ref)
+    vt_all[:, 64:80] = jnp.ones((sp_count, 16, chunk_rows), jnp.bfloat16)
+
+    def prepare(t, slot, source, pair, decays):
+        turned = source.astype(jnp.float32).T.astype(jnp.bfloat16)
+        high = decays.astype(jnp.bfloat16).astype(jnp.float32)
+        rest = decays - high
+        middle = rest.astype(jnp.bfloat16).astype(jnp.float32)
+        rest = rest - middle
+        row = lax.broadcasted_iota(jnp.int32, (64, rows), 0)
+        for n in range(2):
+            head = 2 * pair + n
+            lanes = pl.ds(slot * span + n * rows, rows)
+            picked = (row == head) | (row == 8 + head) | (row == 16 + head)
+            extra = jnp.where(picked, 1.0, 0.0)
+            for at, part in ((24, high), (25, middle), (26, rest)):
+                extra = jnp.where(row == at, part[n : n + 1], extra)
+            qt_ref[t, 0:64, lanes] = turned[n * 64 : (n + 1) * 64]
+            qt_ref[t, 64:128, lanes] = extra.astype(jnp.bfloat16)
+
+    def own_decays(pair, x_):
+        first = (2 * pair) % local
+        at = pl.ds(pl.multiple_of((x_ * half_count + j) * rows, rows), rows)
+        return decay_all[s * half_count + (2 * pair) // local, first : first + 2, at]
+
+    def far_decays(slot):
+        pair, x_ = slot // kv_heads, slot % kv_heads
+        first = (2 * pair) % local
+        return far_decay[x_ * half_count + (2 * pair) // local, first : first + 2]
+
+    def work(t, at, lanes, chunk, start, size, step, limit=None):
+        at = pl.ds(pl.multiple_of(at, span), lanes)
+        q = qt_ref[t, :, at]
+        total = acc_ref[t, :, at]
+        for b in range(size // step):
+            where = pl.ds(pl.multiple_of(start + b * step, step), step)
+            scores = jnp.dot(kp_all[chunk, where], q, preferred_element_type=jnp.float32)
+            if limit is not None:
+                key = lax.broadcasted_iota(jnp.int32, (step, lanes), 0)
+                row = lax.broadcasted_iota(jnp.int32, (step, lanes), 1) % rows
+                scores = jnp.where(key <= row, scores, -1e30)
+            weights = jnp.exp2(scores).astype(jnp.bfloat16)
+            total = total + jnp.dot(
+                vt_all[chunk, :, where], weights, preferred_element_type=jnp.float32
+            )
+        acc_ref[t, :, at] = total
+
+    def whole(t, at, lanes, chunk):
+        work(t, at, lanes, chunk, 0, chunk_rows, chunk_rows if lanes == span else chunk_rows // 2)
+
+    def sweep(t, at, lanes, low, high):
+        def body(chunk, carry):
+            whole(t, at, lanes, chunk)
+            return carry
+
+        lax.fori_loop(low, high, body, 0)
+
+    def diagonal(t, at, lanes, chunk, offset):
+        def body(i, carry):
+            work(t, at, lanes, chunk, i * rows, rows, rows)
+            return carry
+
+        lax.fori_loop(0, offset // rows, body, 0)
+        work(t, at, lanes, chunk, offset, rows, rows, True)
+
+    def finished(t, slot):
+        out = []
+        for n in range(2):
+            lanes = pl.ds(slot * span + n * rows, rows)
+            out.append(acc_ref[t, 0:64, lanes] / acc_ref[t, 64:65, lanes])
+        return jnp.concatenate(out, axis=0).T.astype(jnp.bfloat16)
+
+    def back_copy(slot, pair, device):
+        return remote(
+            res_ref.at[slot], out_ref.at[:, q_lanes(g, pair)], back_send.at[slot],
+            back_recv.at[g * pairs + pair], device,
+        )
+
+    def back_arrived(group, pair):
+        remote(
+            res_ref.at[0], out_ref.at[:, q_lanes(group, pair)], back_send.at[0],
+            back_recv.at[group * pairs + pair], here,
+        ).wait_recv()
+
+    def kept_groups(first, act):
+        def body(i, carry):
+            @pl.when(first <= 2 * i)
+            def _():
+                act(i * 2 * span, 2 * span)
+
+            @pl.when(first == 2 * i + 1)
+            def _():
+                act((2 * i + 1) * span, span)
+
+            return carry
+
+        lax.fori_loop(0, pairs // 2, body, 0)
+
+    def taken_groups(act):
+        def body(i, carry):
+            @pl.when(taken >= 2 * i + 2)
+            def _():
+                act(i * 2 * span, 2 * span)
+
+            @pl.when(taken == 2 * i + 1)
+            def _():
+                act(i * 2 * span, span)
+
+            return carry
+
+        lax.fori_loop(0, pairs // 2, body, 0)
+
+    my_first = kept_from(g)
+    partner_first = kept_from(partner_x)
+    offset = (g * half_count + j) * rows
+    partner_offset = (partner_x * half_count + j) * rows
+
+    kv_copy(kvt_ref.at[g], other_block, x_send, here).wait_recv()
+    each_side(lambda base, device: start_all(other_copies(base, device)))
+
+    @pl.when(z > 0)
+    def _():
+        start_all(other_copies(down_base, down))
+
+    for n in range(1, half_count):
+        arrived(s, (j + n) % half_count)
+    build(s)
+    for pair in range(pairs):
+        prepare(0, pair, query_ref[:, q_lanes(g, pair)], pair, own_decays(pair, g))
+    kept_groups(my_first, lambda at, lanes: diagonal(0, at, lanes, s, offset))
+    round_of(1, True)
+
+    def item(k, carry):
+        lanes_of(k)
+
+        @pl.when(k < zs)
+        def _():
+            round_of(k + 1, True)
+
+        back = jnp.where(y == 0, jnp.where(k == 1, ys, jnp.where(k == ys, 1, k)), k)
+
+        @pl.when(k <= s)
+        def _():
+            kept_groups(my_first, lambda at, lanes: whole(0, at, lanes, s - back))
+
+        return carry
+
+    lax.fori_loop(1, zs + 1, item, 0)
+
+    @pl.when(z >= zh)
+    def _():
+        for extra in range(zs - zh):
+            late(jnp.maximum(z + 1, zh) + extra, True)
+
+    first_late = jnp.maximum(z + 1, zh)
+
+    def partner_phase():
+        def body(i, carry):
+            for n in range(pairs):
+
+                @pl.when((i == n // 2) & (partner_first <= n))
+                def _():
+                    q_arrived(n)
+                    prepare(1, n, in_q[n], n, own_decays(n, partner_x))
+
+            def run(at, lanes):
+                diagonal(1, at, lanes, s, partner_offset)
+                sweep(1, at, lanes, 0, s)
+
+            @pl.when(partner_first <= 2 * i)
+            def _():
+                run(i * 2 * span, 2 * span)
+
+            @pl.when(partner_first == 2 * i + 1)
+            def _():
+                run((2 * i + 1) * span, span)
+
+            for n in range(pairs):
+
+                @pl.when((i == n // 2) & (partner_first <= n))
+                def _():
+                    res_ref[n] = finished(1, n)
+                    back_copy(n, n, (s, partner_x, j)).start()
+
+            @pl.when((i == 0) & (z < zh))
+            def _():
+                late(first_late, True)
+                late_across(first_late, True)
+
+            return carry
+
+        lax.fori_loop(0, pairs // 2, body, 0)
+
+        @pl.when((z > 0) & (z < zh))
+        def _():
+            for extra in range(1, zs - zh):
+                late(first_late + extra, True)
+                late_across(first_late + extra, True)
+
+    def far_phase():
+        for n in range(kv_heads * half_count):
+            remote(
+                decay_ref.at[:, pl.ds(0, rows)], far_decay.at[n], far_send.at[n],
+                far_recv.at[n], here,
+            ).wait_recv()
+
+        for n in range(pairs):
+
+            @pl.when(n < taken)
+            def _():
+                q_arrived(pairs + n)
+                prepare(2, n, in_q[pairs + n], n // kv_heads, far_decays(n))
+
+        taken_groups(lambda at, lanes: sweep(2, at, lanes, 0, upper))
+
+    def turn(i, carry):
+        @pl.when((i == 0) == (z > 0))
+        def _():
+            partner_phase()
+
+        @pl.when(((i == 0) == (z == 0)) & (z < zh))
+        def _():
+            far_phase()
+
+        return carry
+
+    lax.fori_loop(0, 2, turn, 0)
+
+    @pl.when(z < zh)
+    def _():
+        def zone(zo, carry):
+            @pl.when((z == 0) & (zo > first_late))
+            def _():
+                late(zo, True)
+                late_across(zo, True)
+
+            late_lanes(zo)
+
+            @pl.when(zo < zs - 1 - z)
+            def _():
+                taken_groups(lambda at, lanes: sweep(2, at, lanes, zo * ys, zo * ys + ys))
+
+            return carry
+
+        lax.fori_loop(zh, zs - z, zone, 0)
+        last = (zs - 1 - z) * ys
+        taken_groups(lambda at, lanes: sweep(2, at, lanes, last, s_far))
+
+        def close(n, carry):
+            unit_x = n % kv_heads
+            diagonal(2, n * span, span, s_far, (unit_x * half_count + j) * rows)
+            for m in range(pairs):
+
+                @pl.when(n == m)
+                def _():
+                    res_ref[pairs + m] = finished(2, m)
+                    back_copy(
+                        pairs + m, m // kv_heads, (s_far, m % kv_heads, j)
+                    ).start()
+
+            return carry
+
+        lax.fori_loop(0, taken, close, 0)
+
+    kept_groups(my_first, lambda at, lanes: sweep(0, at, lanes, 0, jnp.maximum(s - zs, 0)))
+    for pair in range(pairs):
+
+        @pl.when(pair >= my_first)
+        def _():
+            out_ref[:, q_lanes(g, pair)] = finished(0, pair)
+
+    x_copy.wait_send()
+    each_side(
+        lambda base, device: drain_all(own_copies(base, device) + other_copies(base, device))
+    )
+
+    @pl.when(z > 0)
+    def _():
+        drain_all(own_copies(down_base, down) + other_copies(down_base, down))
+
+    def drain(k, carry):
+        round_of(k, False)
+        return carry
+
+    lax.fori_loop(1, zs + 1, drain, 0)
+
+    def drain_late(zo, carry):
+        late(zo, False)
+        late_across(zo, False)
+        return carry
+
+    lax.fori_loop(zh, zs, drain_late, 0)
+
+    @pl.when(is_high)
+    def _():
+        far_sends(drain_all)
+        drain_all(far_decay_copies())
+
+    near_sends(drain_all)
+    for pair in range(pairs):
+
+        @pl.when(partner_first <= pair)
+        def _():
+            back_copy(pair, pair, (s, partner_x, j)).wait_send()
+
+        @pl.when(pair < taken)
+        def _():
+            back_copy(
+                pairs + pair, pair // kv_heads, (s_far, pair % kv_heads, j)
+            ).wait_send()
+
+        back_arrived(partner_x, pair)
+
+        @pl.when(pair < my_first)
+        def _():
+            back_arrived(g, pair)
+
+
+def lines_of(sp_count):
+    ys = 1 << ((sp_count.bit_length() - 1) // 2)
+    return sp_count // ys, ys
+
+
+def stream(queries, kvt, decays, sizes):
+    sp_count, kv_heads, half_count = sizes
+    rows = queries.shape[0]
+    heads = queries.shape[1] // 64 // kv_heads
+    local, chunk_rows = decays.shape
+    zs, ys = lines_of(sp_count)
+    pairs = heads // 2
+    count = sp_count * kv_heads * half_count
+    members = sp_count * half_count
+    per = 1 + (ys - 1) + (half_count - 1) + (ys - 1) * (half_count - 1)
+    each = kv_heads + 1
+    vmem = pl.BlockSpec(memory_space=pltpu.VMEM)
+    dma = pltpu.SemaphoreType.DMA
+    return pl.pallas_call(
+        lambda *refs: stream_kernel(
+            *refs, sizes=sizes, lines=(zs, ys), rows=rows, heads=heads
+        ),
+        out_shape=jax.ShapeDtypeStruct(queries.shape, jnp.bfloat16),
+        in_specs=[vmem] * 3,
+        out_specs=vmem,
+        scratch_shapes=[
+            pltpu.VMEM((count, 128, rows), jnp.bfloat16),
+            pltpu.VMEM((members, local, chunk_rows), jnp.float32),
+            pltpu.VMEM((kv_heads * half_count, local, rows), jnp.float32),
+            pltpu.VMEM((2 * pairs, rows, 128), jnp.bfloat16),
+            pltpu.VMEM((3, 128, heads * rows), jnp.bfloat16),
+            pltpu.VMEM((3, 80, heads * rows), jnp.float32),
+            pltpu.VMEM((sp_count, chunk_rows, 128), jnp.bfloat16),
+            pltpu.VMEM((sp_count, 80, chunk_rows), jnp.bfloat16),
+            pltpu.VMEM((2 * pairs, rows, 128), jnp.bfloat16),
+            dma((count,)), dma((members,)), dma, dma(((ys + half_count) * each,)),
+            dma((zs * 2 * per * each,)), dma(((zs - zs // 2) * per * each,)),
+            dma((kv_heads * half_count,)), dma((kv_heads * half_count,)),
+            dma((2 * pairs,)), dma((2 * pairs,)), dma((2 * pairs,)), dma((2 * pairs,)),
+        ],
+        compiler_params=pltpu.CompilerParams(
+            has_side_effects=True, vmem_limit_bytes=44 * 1024 * 1024
+        ),
+        name="stream",
+    )(kvt, queries, decays)
+
+
+def any_scores(queries, kv_blocks, decays, sizes):
+    sp_count, kv_heads, half_count = sizes
     group = lax.axis_index("kv")
     me = (lax.axis_index("sp") * kv_heads + group) * half_count + lax.axis_index("half")
-    count = sp_count * tp_count
+    count = sp_count * kv_heads * half_count
     mirror = [(i, count - 1 - i) for i in range(count)]
-    head_size = query_gain.shape[0]
-    rows = inputs.shape[0]
+    rows = queries.shape[0]
     length = rows * count
-    all_heads = w_query.shape[1] // head_size
-    heads = all_heads // kv_heads
-    width = heads * head_size
+    heads = queries.shape[1] // 64 // kv_heads
+    width = heads * 64
     members = sp_count * half_count
     key_block = math.gcd(length, KEY_BLOCK)
 
     def choose(a, b):
         return jnp.where(group == 0, a, b)
 
-    normed = rms_norm(inputs.astype(jnp.float32), in_gain).astype(jnp.bfloat16)
-    keys = rms_norm(
-        jnp.dot(normed, w_key, preferred_element_type=jnp.float32).reshape(
-            rows, kv_heads, head_size
-        ),
-        key_gain,
-    ).astype(jnp.bfloat16)
-    values = (
-        jnp.dot(normed, w_value, preferred_element_type=jnp.float32)
-        .astype(jnp.bfloat16)
-        .reshape(rows, kv_heads, head_size)
-    )
-    pairs = jnp.concatenate([keys, values], axis=2)
-    kv_blocks = pairs.transpose(1, 0, 2)
-    decay_rows = (decay_sums.T * LOG2E).reshape(-1, 128)
-
-    queries = rms_norm(
-        jnp.dot(normed, w_query, preferred_element_type=jnp.float32).reshape(
-            rows, all_heads, head_size
-        ),
-        query_gain * (LOG2E * head_size ** (-0.5)),
-    ).astype(jnp.bfloat16).reshape(rows, kv_heads * width)
+    decay_rows = decays.reshape(-1, 128)
     own_q = choose(queries[:, :width], queries[:, width:])
     sent_q = choose(queries[:, width:], queries[:, :width])
     vmem = pl.BlockSpec(memory_space=pltpu.VMEM)
     chips = count // 2
     dma = pltpu.SemaphoreType.DMA
     kv, far_q, decay_all = pl.pallas_call(
-        lambda *refs: exchange_kernel(
-            *refs, rows=rows, sizes=(sp_count, kv_heads, half_count)
-        ),
+        lambda *refs: exchange_kernel(*refs, rows=rows, sizes=sizes),
         out_shape=(
             jax.ShapeDtypeStruct((length, 128), jnp.bfloat16),
             jax.ShapeDtypeStruct((rows, width), jnp.bfloat16),
@@ -297,16 +948,50 @@
             for first in firsts
         ]
     )
+    attended = attend(place, own_q, far_q, row_decay, decay_all, kv, False)
+    back = lax.ppermute(attended[1], ALL, mirror)
+    return choose(
+        jnp.concatenate([attended[0], back], axis=1), jnp.concatenate([back, attended[0]], axis=1)
+    )
+
+
+def per_device(inputs, in_gain, w_query, w_key, w_value, query_gain, key_gain, decay_sums, w_out):
+    kv_heads = lax.axis_size("kv")
+    sizes = (lax.axis_size("sp"), kv_heads, lax.axis_size("half"))
+    head_size = query_gain.shape[0]
+    rows = inputs.shape[0]
+    all_heads = w_query.shape[1] // head_size
+
+    normed = rms_norm(inputs.astype(jnp.float32), in_gain).astype(jnp.bfloat16)
+    keys = rms_norm(
+        jnp.dot(normed, w_key, preferred_element_type=jnp.float32).reshape(
+            rows, kv_heads, head_size
+        ),
+        key_gain,
+    ).astype(jnp.bfloat16)
+    values = (
+        jnp.dot(normed, w_value, preferred_element_type=jnp.float32)
+        .astype(jnp.bfloat16)
+        .reshape(rows, kv_heads, head_size)
+    )
+    pairs = jnp.concatenate([keys, values], axis=2)
+    kvt = pairs.transpose(1, 2, 0)
+    decays = decay_sums.T * LOG2E
+
+    queries = rms_norm(
+        jnp.dot(normed, w_query, preferred_element_type=jnp.float32).reshape(
+            rows, all_heads, head_size
+        ),
+        query_gain * (LOG2E * head_size ** (-0.5)),
+    ).astype(jnp.bfloat16).reshape(rows, all_heads * head_size)
     bound = head_size**0.5 * LOG2E * jnp.max(query_gain) * jnp.max(key_gain)
-    attended = lax.cond(
+    whole = lax.cond(
         bound <= SMALL,
-        lambda *given: attend(*given, True),
-        lambda *given: attend(*given, False),
-        place, own_q, far_q, row_decay, decay_all, kv,
-    )
-    back = lax.ppermute(attended[1], ALL, mirror)
-    whole = choose(
-        jnp.concatenate([attended[0], back], axis=1), jnp.concatenate([back, attended[0]], axis=1)
+        lambda queries, kvt, decays: stream(queries, kvt, decays, sizes),
+        lambda queries, kvt, decays: any_scores(
+            queries, kvt.transpose(0, 2, 1), decays, sizes
+        ),
+        queries, kvt, decays,
     )
     return jnp.dot(whole, w_out, preferred_element_type=jnp.float32).astype(jnp.bfloat16)
 

time: 140 us -> 138 us (0.986)
  matrix products: 11.4 us -> 9.42 us
  local copies, waits for them, and re-layouts: 4.11 us -> 6.05 us
  other arithmetic: 9.2 us -> 7.48 us
    cond x0 -> x4, local copies, waits for them, and re-layouts: none -> 2.54 us
    dot_general x1, matrix products: 4.46 us -> 2.32 us  [per_device(): jnp.dot(normed, w_query, preferred_element_type=jnp.float32)]
where the time goes in v2:
time: 138 us; the launch traced here: 137 us
  Pallas kernels  99.2 us (72%)
  waiting for transfers between devices  13.4 us (10%)
  matrix products  9.42 us (7%)
  other arithmetic  7.48 us (5%)
  local copies, waits for them, and re-layouts  6.05 us (4%)
  between operations  1.42 us (1%)
    pallas_call x1, Pallas kernels, any_scores(): pl.pallas_call(lambda *refs: exchange_kernel(*refs, rows=rows, sizes=size...  51.6 us
    pallas_call x1, Pallas kernels, attend(): pl.pallas_call(lambda *refs: attend_kernel(*refs, rows=rows, heads=heads,...  47.6 us
    ppermute x1, waiting for transfers between devices, any_scores(): back = lax.ppermute(attended[1], ALL, mirror)  13.4 us
    dot_general x1, matrix products, per_device(): jnp.dot(whole, w_out, preferred_element_type=jnp.float32)  4.41 us
  transfers between devices with their start and end apart: 1, of which 1 were waited for; matrix products, arithmetic and copies ran while one was open for 0% of the time, Pallas kernels for 0%

profile of v2, /device:TPU:9, one launch (start us, length us, event | category | flops | bytes accessed | tf_op | source)
XLA Modules:
  0.0 137.5 jit_solution(6266190338186142948)
XLA Ops:
  0.0 1.4 %reduce_max.19 = f32[]{:T(128)} reduce(f32[64]{0:T(128)} %param.17, f32[]{:T(128)} %constant.73.clone.1), dimensions={0}, to_apply=%region_1.0 | reduce | flops 63 | bytes 264 | tf_op jit(solution)/shard_map/reduce_max | solution.py:987
  1.4 1.5 %fusion = f32[256]{0:T(256)S(1)} fusion(bf16[256,2048]{1,0:T(8,128)(2,1)} %param.11), kind=kLoop, calls=%fused_computation.12 | loop fusion | flops 1572608 | bytes 1049600 | tf_op jit(solution)/shard_map/reduce_sum | solution.py:20
  2.9 1.3 broadcast_multiply_fusion
  5.5 0.7 multiply_bitcast_fusion
  6.3 2.1 %convolution_convert_fusion.1 = bf16[256,128]{0,1:T(8,128)(2,1)S(1)} fusion(bf16[2048,128]{1,0:T(8,128)(2,1)} %param.15, bf16[256,2048]{1,0:T(8,128)(2,1)} %param.11, f32[2048]{0:T(1024)} %param.12, f32[256]{0:T(256)S(1)} %add_rsqrt_fusion.2), kind=kOutput, calls=%fused_computation.15 | convolution fusion | flops 136347648 | bytes 1647616 | tf_op jit(solution)/shard_map/dot_general | solution.py:973
  8.4 0.6 multiply_reduce_fusion
  9.1 2.3 %fusion.9 = (f32[256,1024]{1,0:T(8,128)S(1)}, f32[256,1024]{1,0:T(8,128)}) fusion(bf16[2048,1024]{1,0:T(8,128)(2,1)S(1)} %copy-done.5, bf16[256,2048]{1,0:T(8,128)(2,1)S(1)} %copy-done.3, f32[2048]{0:T(1024)S(1)} %copy-done.6, f32[256]{0:T(256)S(1)} %add_rsqrt_fusion.2), kind=kOutput, calls=%fused_computation.29 | convolution fusion | flops 1076101120 | bytes 7349248 | tf_op jit(solution)/shard_map/dot_general | solution.py:982
  11.5 0.3 copy.20
  11.8 0.1 bitcast_reduce_fusion
  12.0 0.3 copy.21
  12.3 1.4 %multiply_convert_fusion = bf16[256,1024]{1,0:T(8,128)(2,1)S(1)} fusion(f32[256,1024]{1,0:T(8,128)} %get-tuple-element.49, f32[256,1024]{1,0:T(8,128)S(1)} %copy.21, f32[1024]{0:T(1024)S(1)} %mul.112), kind=kLoop, calls=%fused_computation.17 | loop fusion | flops 786432 | bytes 2625536 | tf_op jit(solution)/shard_map/convert_element_type | solution.py:986
  13.8 119.3 %conditional.1 = (bf16[256,1024]{1,0:T(8,128)(2,1)S(1)}) conditional(s32[]{:T(128)} %convert_element_type.22, (bf16[256,1024]{1,0:T(8,128)(2,1)S(1)}, bf16[256,2,128]{0,2,1:T(8,128)(2,1)S(1)}, f32[4,1024]{1,0:T(4,128)S(1)}) %tuple.11, (bf16[2,128,256]{2,1,0:T(8,128)(2,1)S(1)}, bf16[256,1024]{1,0:T(8,128)(2,1)S(1)}, f32[4,1024]{1,0:T(4,128)S(1)}) %tuple.12), branch_computations={%region_5.6_spmd, %region_6.7_spmd} | conditional | flops 2625604 | bytes 15074105 | solution.py:988
  13.8 0.6 reshape.42.refs_2_
  14.5 0.8 copy.22
  15.2 0.7 broadcast_select_fusion
  16.0 51.6 %exchange.1 = (bf16[8192,128]{1,0:T(8,128)(2,1)}, bf16[256,512]{1,0:T(8,128)(2,1)}, f32[16,32,128]{2,1,0:T(8,128)}) custom-call(bf16[2,256,128]{2,1,0:T(8,128)(2,1)} %bitcast.41, bf16[256,512]{1,0:T(8,128)(2,1)} %get-tuple-element.40.refs_1_, f32[32,128]{1,0:T(8,128)} %reshape.42.refs_2_), custom_call_target="tpu_custom_call" | custom-call | tf_op jit(solution)/shard_map/cond/branch_0_fun/exchange/pallas_call | solution.py:923
  67.6 1.1 reshape.43
  68.8 0.1 copy.19.refs_3_
  69.0 1.6 %copy-done.1 = bf16[8192,128]{1,0:T(8,128)(2,1)S(1)} copy-done((bf16[8192,128]{1,0:T(8,128)(2,1)S(1)}, bf16[8192,128]{1,0:T(8,128)(2,1)}, u32[]{:S(2)}) %copy-start.1) | copy-done | bytes 2097176 | tf_op jit(solution)/shard_map/cond
  70.6 0.9 copy-done.2
  71.6 47.6 %attend_any.1 = bf16[2,256,512]{2,1,0:T(8,128)(2,1)S(1)} custom-call(s32[2]{0:T(128)S(1)} %pad_add_fusion.refs_0_, bf16[256,512]{1,0:T(8,128)(2,1)S(1)} %get-tuple-element.41.refs_1_, bf16[256,512]{1,0:T(8,128)(2,1)S(1)} %copy-done.2, f32[2,256,8]{2,1,0:T(8,128)S(1)} %copy.19.refs_3_, f32[16,8,512]{2,1,0:T(8,128)S(1)} %bitcast.39, ...), custom_call_target="tpu_custom_call" | custom-call | tf_op jit(solution)/shard_map/cond/branch_0_fun/attend_any/pallas_call | solution.py:204
  119.3 13.4 %collective-permute-done = bf16[256,512]{1,0:T(8,128)(2,1)S(1)} collective-permute-done((bf16[256,512]{1,0:T(8,128)(2,1)S(1)}, bf16[256,512]{1,0:T(8,128)(2,1)S(1)}, u32[]{:S(2)}, u32[]{:S(2)}) %collective-permute-start) | collective-permute-done | bytes 262176 | tf_op jit(solution)/shard_map/cond/branch_0_fun/ppermute | solution.py:952
  132.7 0.1 maximum_select_fusion
  133.0 4.4 %convolution_convert_fusion = bf16[256,2048]{1,0:T(8,128)(2,1)} fusion(bf16[256,1024]{1,0:T(8,128)(2,1)S(1)} %get-tuple-element.52, bf16[1024,2048]{1,0:T(8,128)(2,1)} %param.19), kind=kOutput, calls=%fused_computation.11 | convolution fusion | flops 1074266112 | bytes 5767168 | tf_op jit(solution)/shard_map/dot_general | solution.py:996
  (26 shorter events, 0.5 us)
Async XLA Ops:
  0.0 8.4 %copy-start = (bf16[2048,128]{1,0:T(8,128)(2,1)S(1)}, bf16[2048,128]{1,0:T(8,128)(2,1)}, u32[]{:S(2)}) copy-start(bf16[2048,128]{1,0:T(8,128)(2,1)} %param.14) | copy-start | bytes 1572868
  0.0 8.4 %copy-start.3 = (bf16[256,2048]{1,0:T(8,128)(2,1)S(1)}, bf16[256,2048]{1,0:T(8,128)(2,1)}, u32[]{:S(2)}) copy-start(bf16[256,2048]{1,0:T(8,128)(2,1)} %param.11) | copy-start | bytes 3145732
  0.0 8.4 %copy-start.6 = (f32[2048]{0:T(1024)S(1)}, f32[2048]{0:T(1024)}, u32[]{:S(2)}) copy-start(f32[2048]{0:T(1024)} %param.12) | copy-start | bytes 24580
  6.3 2.7 %copy-start.4 = (f32[64]{0:T(128)S(1)}, f32[64]{0:T(128)}, u32[]{:S(2)}) copy-start(f32[64]{0:T(128)} %param.17) | copy-start | bytes 772
  6.3 2.9 %copy-start.5 = (bf16[2048,1024]{1,0:T(8,128)(2,1)S(1)}, bf16[2048,1024]{1,0:T(8,128)(2,1)}, u32[]{:S(2)}) copy-start(bf16[2048,1024]{1,0:T(8,128)(2,1)} %param.13) | copy-start | bytes 12582916
  69.0 1.6 %copy-start.1 = (bf16[8192,128]{1,0:T(8,128)(2,1)S(1)}, bf16[8192,128]{1,0:T(8,128)(2,1)}, u32[]{:S(2)}) copy-start(bf16[8192,128]{1,0:T(8,128)(2,1)} %get-tuple-element.25.refs_5_) | copy-start | bytes 6291460 | tf_op jit(solution)/shard_map/cond
  70.6 0.9 copy-start.2
  119.2 13.5 %collective-permute-start = (bf16[256,512]{1,0:T(8,128)(2,1)S(1)}, bf16[256,512]{1,0:T(8,128)(2,1)S(1)}, u32[]{:S(2)}, u32[]{:S(2)}) collective-permute-start(bf16[256,512]{1,0:T(8,128)(2,1)S(1)} %get-tuple-element.39), channel_id=1, source_target_pairs={{0,31},{1,30},{2,29},{3,28},{4,27},{5,26},{6,25},{7,24},{8,23},{9,... | collective-permute-start | bytes 786440 | tf_op jit(solution)/shard_map/cond/branch_0_fun/ppermute | solution.py:952

commit v3 on v2

--- a/solution.py
+++ b/solution.py
@@ -220,9 +220,11 @@
 
 
 def stream_kernel(
-    kvt_ref, query_ref, decay_ref, out_ref, kvt_all, decay_all, far_decay, in_q, qt_ref, acc_ref,
-    kp_all, vt_all, res_ref, kv_recv, decay_recv, x_send, own_send, round_send, late_send,
-    far_send, far_recv, q_send, q_recv, back_send, back_recv, *, sizes, lines, rows, heads
+    x_hbm, in_gain, wq_hbm, wk_hbm, wv_hbm, query_gain, key_gain, sums_hbm, wo_hbm, out_ref,
+    x_ref, wkv_ref, wq_ref, sums_ref, wo_ref, normed_ref, kvt_ref, query_ref, decay_ref, att_ref,
+    kvt_all, decay_all, far_decay, in_q, qt_ref, acc_ref, kp_all, vt_all, res_ref, loads, kv_recv,
+    decay_recv, x_send, own_send, round_send, late_send, far_send, far_recv, q_send, q_recv,
+    back_send, back_recv, *, sizes, lines, rows, heads
 ):
     sp_count, kv_heads, half_count = sizes
     zs, ys = lines
@@ -266,20 +268,16 @@
     here = (s, g, j)
     each = kv_heads + 1
 
-    def package(s_, j_, base, device, sems):
-        copies = []
-        for x_ in range(kv_heads):
-            block = block_at(s_, x_, j_)
-            copies.append(kv_copy(kvt_all.at[block], block, sems.at[base + x_], device))
-        member = s_ * half_count + j_
-        copies.append(
-            decay_copy(decay_all.at[member], member, sems.at[base + kv_heads], device)
-        )
-        return copies
+    def one_piece(s_, j_, piece, base, device, sems):
+        if piece == kv_heads:
+            member = s_ * half_count + j_
+            return decay_copy(decay_all.at[member], member, sems.at[base + piece], device)
+        block = block_at(s_, piece, j_)
+        return kv_copy(kvt_all.at[block], block, sems.at[base + piece], device)
 
     def arrived(s_, j_):
-        for copy in package(s_, j_, 0, here, own_send):
-            copy.wait_recv()
+        for piece in range(each):
+            one_piece(s_, j_, piece, 0, here, own_send).wait_recv()
 
     def start_all(copies):
         for copy in copies:
@@ -292,39 +290,54 @@
     def inside(z_):
         return (z_ >= 0) & (z_ < zs)
 
-    def others(s_, base, sems, act, z_=None):
-        slot = 0
-        if z_ is None:
-            for n in range(1, ys):
-                to = (z * ys + (y + n) % ys, g, j)
-                act(package(s_, j, base + slot * each, to, sems))
-                slot += 1
-        for n in range(1, half_count):
-            to = (s, g, (j + n) % half_count)
-            act(package(s_, j, base + slot * each, to, sems))
-            slot += 1
+    def to_rows(base):
+        return [
+            (None, base + (n - 1) * each, (z * ys + (y + n) % ys, g, j)) for n in range(1, ys)
+        ]
+
+    def to_lanes(base):
+        return [
+            (None, base + (n - 1) * each, (s, g, (j + n) % half_count))
+            for n in range(1, half_count)
+        ]
+
+    def relay(s_, routes, sems, go):
+        for piece in range(each):
+            if go:
+                one_piece(s_, j, piece, 0, here, own_send).wait_recv()
+            for condition, base, device in routes:
+                copy = one_piece(s_, j, piece, base, device, sems)
+                act = copy.start if go else copy.wait_send
+                if condition is None:
+                    act()
+                else:
+                    pl.when(condition)(act)
 
     per = 1 + (ys - 1) + (half_count - 1) + (ys - 1) * (half_count - 1)
+
+    def spread(s_, base, condition, device, sems, go):
+        routes = [(condition, base, device)]
+        routes += to_rows(base + each) + to_lanes(base + ys * each)
+        relay(s_, routes, sems, go)
+
+    def across(zo, base, sems, go):
+        for m in range(1, ys):
+            slot = ys + half_count - 1 + (m - 1) * (half_count - 1)
+            relay(zo * ys + (y + m) % ys, to_lanes(base + slot * each), sems, go)
 
     def near_from(z_, way):
         return inside(z_) if way > 0 else inside(z_) & (z_ < zh)
 
     def round_of(k, go):
-        act = start_all if go else drain_all
         for d, way in enumerate((1, -1)):
             base = ((k - 1) * 2 + d) * per * each
 
             @pl.when(near_from(z - way * k, way))
             def _():
-                s_ = (z - way * k) * ys + y
-                if go:
-                    arrived(s_, j)
-
-                @pl.when(inside(z + way))
-                def _():
-                    act(package(s_, j, base, ((z + way) * ys + y, g, j), round_send))
-
-                others(s_, base + each, round_send, act)
+                spread(
+                    (z - way * k) * ys + y, base, inside(z + way), ((z + way) * ys + y, g, j),
+                    round_send, go,
+                )
 
             reach = near_from(z - way * (k - 1), way)
             if way < 0:
@@ -332,43 +345,18 @@
 
             @pl.when(reach)
             def _():
-                for m in range(1, ys):
-                    s_ = (z - way * (k - 1)) * ys + (y + m) % ys
-                    if go:
-                        arrived(s_, j)
-                    slot = ys + half_count - 1 + (m - 1) * (half_count - 1)
-                    others(s_, base + slot * each, round_send, act, z)
+                across(z - way * (k - 1), base, round_send, go)
 
     def late(zo, go):
-        act = start_all if go else drain_all
-        base = (zo - zh) * per * each
-
-        @pl.when((zo > z) & (zo < zs))
-        def _():
-            s_ = zo * ys + y
-            if go:
-                arrived(s_, j)
-
-            @pl.when(z > 0)
-            def _():
-                act(package(s_, j, base, ((z - 1) * ys + y, g, j), late_send))
-
-            @pl.when(zo <= zs - 1 - z)
-            def _():
-                others(s_, base + each, late_send, act)
+        @pl.when(zo <= zs - 1 - z)
+        def _():
+            base = (zo - zh) * per * each
+            spread(zo * ys + y, base, z > 0, ((z - 1) * ys + y, g, j), late_send, go)
 
     def late_across(zo, go):
-        act = start_all if go else drain_all
-        base = (zo - zh) * per * each
-
-        @pl.when((zo > z) & (zo <= zs - 1 - z))
-        def _():
-            for m in range(1, ys):
-                s_ = zo * ys + (y + m) % ys
-                if go:
-                    arrived(s_, j)
-                slot = ys + half_count - 1 + (m - 1) * (half_count - 1)
-                others(s_, base + slot * each, late_send, act, z)
+        @pl.when(zo <= zs - 1 - z)
+        def _():
+            across(zo, (zo - zh) * per * each, late_send, go)
 
     def build(s_):
         for x_ in range(kv_heads):
@@ -423,7 +411,7 @@
                     build_if(s_)
 
     def late_lanes(zo):
-        @pl.when((zo > z) & (zo <= zs - 1 - z))
+        @pl.when(zo <= zs - 1 - z)
         def _():
             for m in range(ys):
                 s_ = zo * ys + (y + m) % ys
@@ -434,23 +422,90 @@
     def q_lanes(group, pair):
         return pl.ds(pl.multiple_of(group * width + pair * 128, 128), 128)
 
+    fetches = [
+        pltpu.make_async_copy(source, target, loads.at[n])
+        for n, (source, target) in enumerate(
+            (
+                (x_hbm, x_ref), (wk_hbm, wkv_ref.at[:, 0:128]), (wv_hbm, wkv_ref.at[:, 128:256]),
+                (sums_hbm, sums_ref), (wq_hbm, wq_ref), (wo_hbm, wo_ref),
+            )
+        )
+    ]
+    for fetch in fetches:
+        fetch.start()
+
+    barrier = pltpu.get_barrier_semaphore()
+
+    def greet(device):
+        pl.semaphore_signal(
+            barrier, inc=1, device_id=device, device_id_type=pl.DeviceIdType.MESH
+        )
+
+    greeted = 0
+    for n in range(1, half_count):
+        greet((s, g, (j + n) % half_count))
+        greeted += 1
+    greet((s, partner_x, j))
+    greet(((zs - 1 - z) * ys + y, g, j))
+    greeted += 2
+    for n in range(1, ys):
+        greet((z * ys + (y + n) % ys, g, j))
+        greeted += 1
+    for x_ in range(kv_heads):
+        for n in range(half_count):
+            greet((s_far, x_, n))
+            greeted += 1
+    for way in (1, -1):
+
+        @pl.when(inside(z + way))
+        def _():
+            greet(((z + way) * ys + y, g, j))
+
+        greeted = greeted + jnp.where(inside(z + way), 1, 0)
+
+    def columns(gain):
+        wide = jnp.broadcast_to(gain.reshape(1, 64), (64, 64))
+        wide = jnp.concatenate([wide, wide], axis=1)
+        wide = jnp.concatenate([wide, wide], axis=0).T
+        return jnp.concatenate([wide[0:64]] * (rows // 128), axis=1)
+
+    def per_head(turned, gain):
+        many = turned.reshape(turned.shape[0] // 64, 64, rows)
+        mean = jnp.mean(many * many, axis=1, keepdims=True)
+        return (many * lax.rsqrt(mean + epsilon) * gain[None]).reshape(turned.shape)
+
+    fetches[0].wait()
+    x = x_ref[...].astype(jnp.float32)
+    scale = lax.rsqrt(jnp.mean(x * x, axis=1, keepdims=True) + epsilon)
+    normed_ref[...] = (x * scale * in_gain[...].reshape(1, -1)).astype(jnp.bfloat16)
+    fetches[1].wait()
+    fetches[2].wait()
+    both = jnp.dot(normed_ref[...], wkv_ref[...], preferred_element_type=jnp.float32).T
+    turned_keys = per_head(both[0:128], columns(key_gain[...])).astype(jnp.bfloat16)
+    turned_values = both[128:256].astype(jnp.bfloat16)
+    for n in range(kv_heads):
+        kvt_ref[n, 0:64] = turned_keys[n * 64 : (n + 1) * 64]
+        kvt_ref[n, 64:128] = turned_values[n * 64 : (n + 1) * 64]
+    fetches[3].wait()
+    decay_ref[...] = sums_ref[...].T * LOG2E
+
     def far_q_copy(group, pair):
         unit = kv_heads * pair + g
         slot = jnp.minimum(pairs + unit, 2 * pairs - 1)
         return remote(
-            query_ref.at[:, q_lanes(group, pair)], in_q.at[slot],
+            query_ref.at[q_lanes(group, pair)], in_q.at[slot],
             q_send.at[group * pairs + pair], q_recv.at[slot], (s_far, group, j),
         )
 
     def near_q_copy(pair):
         return remote(
-            query_ref.at[:, q_lanes(partner_x, pair)], in_q.at[pair],
+            query_ref.at[q_lanes(partner_x, pair)], in_q.at[pair],
             q_send.at[partner_x * pairs + pair], q_recv.at[pair], (s, partner_x, j),
         )
 
     def q_arrived(slot):
         remote(
-            query_ref.at[:, pl.ds(0, 128)], in_q.at[slot], q_send.at[0], q_recv.at[slot], here
+            query_ref.at[pl.ds(0, 128)], in_q.at[slot], q_send.at[0], q_recv.at[slot], here
         ).wait_recv()
 
     def is_given(pair, x_):
@@ -495,7 +550,7 @@
         targets += [(None, (z * ys + (y + n) % ys, g, j)) for n in range(1, ys)]
         return targets
 
-    down = (jnp.maximum(z - 1, 0) * ys + y, g, j)
+    down = (jnp.where(is_high, zs - 1 - z, jnp.maximum(z - 1, 0)) * ys + y, g, j)
     down_base = (ys + half_count - 1) * each
 
     def each_side(act):
@@ -518,15 +573,32 @@
         return [kv_copy(kvt_all.at[other_block], other_block, own_send.at[base + 2], device)]
 
     x_copy = kv_copy(kvt_ref.at[partner_x], own_block, x_send, (s, partner_x, j))
+    pl.semaphore_wait(barrier, greeted)
     x_copy.start()
     each_side(lambda base, device: start_all(own_copies(base, device)))
 
-    @pl.when(is_high)
+    @pl.when((z > 0) & jnp.logical_not(is_high))
+    def _():
+        start_all(own_copies(down_base, down))
+
+    fetches[4].wait()
+    query_columns = columns(query_gain[...] * (LOG2E * 64 ** (-0.5)))
+
+    def project(n, carry):
+        at = pl.ds(pl.multiple_of(n * 256, 256), 256)
+        turned = jnp.dot(
+            normed_ref[...], wq_ref[:, at], preferred_element_type=jnp.float32
+        ).T
+        query_ref[at] = per_head(turned, query_columns).astype(jnp.bfloat16)
+        return carry
+
+    lax.fori_loop(0, query_ref.shape[0] // 256, project, 0)
+
+    @pl.when(z > zh)
     def _():
         far_sends(start_all)
-        start_all(far_decay_copies())
-
-    @pl.when(z > 0)
+
+    @pl.when(is_high)
     def _():
         start_all(own_copies(down_base, down))
 
@@ -537,7 +609,7 @@
     vt_all[:, 64:80] = jnp.ones((sp_count, 16, chunk_rows), jnp.bfloat16)
 
     def prepare(t, slot, source, pair, decays):
-        turned = source.astype(jnp.float32).T.astype(jnp.bfloat16)
+        turned = source
         high = decays.astype(jnp.bfloat16).astype(jnp.float32)
         rest = decays - high
         middle = rest.astype(jnp.bfloat16).astype(jnp.float32)
@@ -607,13 +679,13 @@
 
     def back_copy(slot, pair, device):
         return remote(
-            res_ref.at[slot], out_ref.at[:, q_lanes(g, pair)], back_send.at[slot],
+            res_ref.at[slot], att_ref.at[:, q_lanes(g, pair)], back_send.at[slot],
             back_recv.at[g * pairs + pair], device,
         )
 
     def back_arrived(group, pair):
         remote(
-            res_ref.at[0], out_ref.at[:, q_lanes(group, pair)], back_send.at[0],
+            res_ref.at[0], att_ref.at[:, q_lanes(group, pair)], back_send.at[0],
             back_recv.at[group * pairs + pair], here,
         ).wait_recv()
 
@@ -657,11 +729,19 @@
     def _():
         start_all(other_copies(down_base, down))
 
+    @pl.when(z == zh)
+    def _():
+        far_sends(start_all)
+
+    @pl.when(is_high)
+    def _():
+        start_all(far_decay_copies())
+
     for n in range(1, half_count):
         arrived(s, (j + n) % half_count)
     build(s)
     for pair in range(pairs):
-        prepare(0, pair, query_ref[:, q_lanes(g, pair)], pair, own_decays(pair, g))
+        prepare(0, pair, query_ref[q_lanes(g, pair)], pair, own_decays(pair, g))
     kept_groups(my_first, lambda at, lanes: diagonal(0, at, lanes, s, offset))
     round_of(1, True)
 
@@ -682,12 +762,9 @@
 
     lax.fori_loop(1, zs + 1, item, 0)
 
-    @pl.when(z >= zh)
+    @pl.when((z > 0) & (z < zh))
     def _():
-        for extra in range(zs - zh):
-            late(jnp.maximum(z + 1, zh) + extra, True)
-
-    first_late = jnp.maximum(z + 1, zh)
+        late(zh, True)
 
     def partner_phase():
         def body(i, carry):
@@ -717,20 +794,13 @@
                     res_ref[n] = finished(1, n)
                     back_copy(n, n, (s, partner_x, j)).start()
 
-            @pl.when((i == 0) & (z < zh))
-            def _():
-                late(first_late, True)
-                late_across(first_late, True)
+            @pl.when((i == 0) & (z > 0) & (z < zh))
+            def _():
+                late_across(zh, True)
 
             return carry
 
         lax.fori_loop(0, pairs // 2, body, 0)
-
-        @pl.when((z > 0) & (z < zh))
-        def _():
-            for extra in range(1, zs - zh):
-                late(first_late + extra, True)
-                late_across(first_late + extra, True)
 
     def far_phase():
         for n in range(kv_heads * half_count):
@@ -739,14 +809,34 @@
                 far_recv.at[n], here,
             ).wait_recv()
 
-        for n in range(pairs):
-
-            @pl.when(n < taken)
-            def _():
-                q_arrived(pairs + n)
-                prepare(2, n, in_q[pairs + n], n // kv_heads, far_decays(n))
-
-        taken_groups(lambda at, lanes: sweep(2, at, lanes, 0, upper))
+        def body(i, carry):
+            for n in range(pairs):
+
+                @pl.when((i == n // 2) & (n < taken))
+                def _():
+                    q_arrived(pairs + n)
+                    prepare(2, n, in_q[pairs + n], n // kv_heads, far_decays(n))
+
+            @pl.when(taken >= 2 * i + 2)
+            def _():
+                sweep(2, i * 2 * span, 2 * span, 0, upper)
+
+            @pl.when(taken == 2 * i + 1)
+            def _():
+                sweep(2, i * 2 * span, span, 0, upper)
+
+            @pl.when((z == 0) & (i == 0))
+            def _():
+                late(zh, True)
+
+            @pl.when((z == 0) & (i == 1))
+            def _():
+                late_across(zh, True)
+                late(zh + 1, True)
+
+            return carry
+
+        lax.fori_loop(0, pairs // 2, body, 0)
 
     def turn(i, carry):
         @pl.when((i == 0) == (z > 0))
@@ -764,10 +854,14 @@
     @pl.when(z < zh)
     def _():
         def zone(zo, carry):
-            @pl.when((z == 0) & (zo > first_late))
+            @pl.when(zo > jnp.where(z == 0, zh + 1, zh))
             def _():
                 late(zo, True)
                 late_across(zo, True)
+
+            @pl.when((z == 0) & (zo == zh))
+            def _():
+                late_across(zh + 1, True)
 
             late_lanes(zo)
 
@@ -802,7 +896,7 @@
 
         @pl.when(pair >= my_first)
         def _():
-            out_ref[:, q_lanes(g, pair)] = finished(0, pair)
+            att_ref[:, q_lanes(g, pair)] = finished(0, pair)
 
     x_copy.wait_send()
     each_side(
@@ -824,7 +918,10 @@
         late_across(zo, False)
         return carry
 
-    lax.fori_loop(zh, zs, drain_late, 0)
+    @pl.when(z < zh)
+    def _():
+        lax.fori_loop(zh, zs, drain_late, 0)
+
 
     @pl.when(is_high)
     def _():
@@ -850,17 +947,31 @@
         def _():
             back_arrived(g, pair)
 
+    fetches[5].wait()
+
+    def output(n, carry):
+        at = pl.ds(pl.multiple_of(n * 512, 512), 512)
+        out_ref[:, at] = jnp.dot(
+            att_ref[...], wo_ref[:, at], preferred_element_type=jnp.float32
+        ).astype(jnp.bfloat16)
+        return carry
+
+    lax.fori_loop(0, wo_ref.shape[1] // 512, output, 0)
+
 
 def lines_of(sp_count):
     ys = 1 << ((sp_count.bit_length() - 1) // 2)
     return sp_count // ys, ys
 
 
-def stream(queries, kvt, decays, sizes):
+def stream(
+    inputs, in_gain, w_query, w_key, w_value, query_gain, key_gain, decay_sums, w_out, sizes
+):
     sp_count, kv_heads, half_count = sizes
-    rows = queries.shape[0]
-    heads = queries.shape[1] // 64 // kv_heads
-    local, chunk_rows = decays.shape
+    rows, model = inputs.shape
+    width = w_query.shape[1]
+    heads = width // 64 // kv_heads
+    chunk_rows, local = decay_sums.shape
     zs, ys = lines_of(sp_count)
     pairs = heads // 2
     count = sp_count * kv_heads * half_count
@@ -868,34 +979,46 @@
     per = 1 + (ys - 1) + (half_count - 1) + (ys - 1) * (half_count - 1)
     each = kv_heads + 1
     vmem = pl.BlockSpec(memory_space=pltpu.VMEM)
+    hbm = pl.BlockSpec(memory_space=pltpu.MemorySpace.HBM)
     dma = pltpu.SemaphoreType.DMA
     return pl.pallas_call(
         lambda *refs: stream_kernel(
             *refs, sizes=sizes, lines=(zs, ys), rows=rows, heads=heads
         ),
-        out_shape=jax.ShapeDtypeStruct(queries.shape, jnp.bfloat16),
-        in_specs=[vmem] * 3,
+        out_shape=jax.ShapeDtypeStruct((rows, w_out.shape[1]), jnp.bfloat16),
+        in_specs=[hbm, vmem, hbm, hbm, hbm, vmem, vmem, hbm, hbm],
         out_specs=vmem,
         scratch_shapes=[
+            pltpu.VMEM((rows, model), jnp.bfloat16),
+            pltpu.VMEM((model, 256), jnp.bfloat16),
+            pltpu.VMEM(w_query.shape, jnp.bfloat16),
+            pltpu.VMEM(decay_sums.shape, jnp.float32),
+            pltpu.VMEM(w_out.shape, jnp.bfloat16),
+            pltpu.VMEM((rows, model), jnp.bfloat16),
+            pltpu.VMEM((kv_heads, 128, rows), jnp.bfloat16),
+            pltpu.VMEM((width, rows), jnp.bfloat16),
+            pltpu.VMEM((local, chunk_rows), jnp.float32),
+            pltpu.VMEM((rows, width), jnp.bfloat16),
             pltpu.VMEM((count, 128, rows), jnp.bfloat16),
             pltpu.VMEM((members, local, chunk_rows), jnp.float32),
             pltpu.VMEM((kv_heads * half_count, local, rows), jnp.float32),
-            pltpu.VMEM((2 * pairs, rows, 128), jnp.bfloat16),
+            pltpu.VMEM((2 * pairs, 128, rows), jnp.bfloat16),
             pltpu.VMEM((3, 128, heads * rows), jnp.bfloat16),
             pltpu.VMEM((3, 80, heads * rows), jnp.float32),
             pltpu.VMEM((sp_count, chunk_rows, 128), jnp.bfloat16),
             pltpu.VMEM((sp_count, 80, chunk_rows), jnp.bfloat16),
             pltpu.VMEM((2 * pairs, rows, 128), jnp.bfloat16),
+            dma((6,)),
             dma((count,)), dma((members,)), dma, dma(((ys + half_count) * each,)),
             dma((zs * 2 * per * each,)), dma(((zs - zs // 2) * per * each,)),
             dma((kv_heads * half_count,)), dma((kv_heads * half_count,)),
             dma((2 * pairs,)), dma((2 * pairs,)), dma((2 * pairs,)), dma((2 * pairs,)),
         ],
         compiler_params=pltpu.CompilerParams(
-            has_side_effects=True, vmem_limit_bytes=44 * 1024 * 1024
+            has_side_effects=True, collective_id=0, vmem_limit_bytes=56 * 1024 * 1024
         ),
         name="stream",
-    )(kvt, queries, decays)
+    )(inputs, in_gain, w_query, w_key, w_value, query_gain, key_gain, decay_sums, w_out)
 
 
 def any_scores(queries, kv_blocks, decays, sizes):
@@ -955,9 +1078,10 @@
     )
 
 
-def per_device(inputs, in_gain, w_query, w_key, w_value, query_gain, key_gain, decay_sums, w_out):
-    kv_heads = lax.axis_size("kv")
-    sizes = (lax.axis_size("sp"), kv_heads, lax.axis_size("half"))
+def any_program(
+    inputs, in_gain, w_query, w_key, w_value, query_gain, key_gain, decay_sums, w_out, sizes
+):
+    kv_heads = sizes[1]
     head_size = query_gain.shape[0]
     rows = inputs.shape[0]
     all_heads = w_query.shape[1] // head_size
@@ -974,26 +1098,27 @@
         .astype(jnp.bfloat16)
         .reshape(rows, kv_heads, head_size)
     )
-    pairs = jnp.concatenate([keys, values], axis=2)
-    kvt = pairs.transpose(1, 2, 0)
-    decays = decay_sums.T * LOG2E
-
+    kv_blocks = jnp.concatenate([keys, values], axis=2).transpose(1, 0, 2)
     queries = rms_norm(
         jnp.dot(normed, w_query, preferred_element_type=jnp.float32).reshape(
             rows, all_heads, head_size
         ),
         query_gain * (LOG2E * head_size ** (-0.5)),
     ).astype(jnp.bfloat16).reshape(rows, all_heads * head_size)
-    bound = head_size**0.5 * LOG2E * jnp.max(query_gain) * jnp.max(key_gain)
-    whole = lax.cond(
+    whole = any_scores(queries, kv_blocks, decay_sums.T * LOG2E, sizes)
+    return jnp.dot(whole, w_out, preferred_element_type=jnp.float32).astype(jnp.bfloat16)
+
+
+def per_device(*arrays):
+    query_gain, key_gain = arrays[5:7]
+    sizes = (lax.axis_size("sp"), lax.axis_size("kv"), lax.axis_size("half"))
+    bound = query_gain.shape[0] ** 0.5 * LOG2E * jnp.max(query_gain) * jnp.max(key_gain)
+    return lax.cond(
         bound <= SMALL,
-        lambda queries, kvt, decays: stream(queries, kvt, decays, sizes),
-        lambda queries, kvt, decays: any_scores(
-            queries, kvt.transpose(0, 2, 1), decays, sizes
-        ),
-        queries, kvt, decays,
+        lambda *given: stream(*given, sizes),
+        lambda *given: any_program(*given, sizes),
+        *arrays,
     )
-    return jnp.dot(whole, w_out, preferred_element_type=jnp.float32).astype(jnp.bfloat16)
 
 
 def solution(mesh):

time: 138 us -> 138 us (level)
  no operation moved by 1% of the time
where the time goes in v3:
time: 138 us; the launch traced here: 137 us
  Pallas kernels  99.4 us (72%)
  waiting for transfers between devices  13.4 us (10%)
  matrix products  8.28 us (6%)
  other arithmetic  7.56 us (5%)
  local copies, waits for them, and re-layouts  6.61 us (5%)
    pallas_call x1, Pallas kernels, any_scores(): pl.pallas_call(lambda *refs: exchange_kernel(*refs, rows=rows, sizes=size...  51.6 us
    pallas_call x1, Pallas kernels, attend(): pl.pallas_call(lambda *refs: attend_kernel(*refs, rows=rows, heads=heads,...  47.7 us
    ppermute x1, waiting for transfers between devices, any_scores(): back = lax.ppermute(attended[1], ALL, mirror)  13.4 us
    dot_general x1, matrix products, any_program(): jnp.dot(normed, w_query, preferred_element_type=jnp.float32)  4.47 us
  transfers between devices with their start and end apart: 1, of which 1 were waited for; matrix products, arithmetic and copies ran while one was open for 0% of the time, Pallas kernels for 0%

profile of v3, /device:TPU:9, one launch (start us, length us, event | category | flops | bytes accessed | tf_op | source)
XLA Modules:
  0.0 137.2 jit_solution(16558980028315723960)
XLA Ops:
  0.0 1.3 reduce_max.19
  1.3 1.3 reduce_max.18
  3.8 132.4 %conditional.1 = (bf16[256,2048]{1,0:T(8,128)(2,1)S(1)}) conditional(s32[]{:T(128)} %convert_element_type.22, (bf16[256,2048]{1,0:T(8,128)(2,1)}, f32[2048]{0:T(1024)}, bf16[2048,1024]{1,0:T(8,128)(2,1)}, f32[64]{0:T(128)}, bf16[2048,128]{1,0:T(8,128)(2,1)}, /*index=5*/f32[64]{0:T(128)}, bf16[2048,128]{1,0:T(8,128)(2,1)}, f32[1024,4]{0,1:T(4,128)}, ...), branch_computations={%region_2.6_spmd, %region_6.7_spmd} | conditional | flops 2428711680 | bytes 68477896 | solution.py:1116
  3.9 0.8 broadcast_multiply_fusion
  4.7 1.5 %fusion = f32[256]{0:T(256)S(1)} fusion(bf16[256,2048]{1,0:T(8,128)(2,1)} %get-tuple-element.44), kind=kLoop, calls=%fused_computation.3 | loop fusion | flops 1572608 | bytes 1049600 | tf_op jit(solution)/shard_map/cond/branch_0_fun/reduce_sum | solution.py:20
  6.3 0.7 multiply_bitcast_fusion
  7.0 0.6 reshape.44.refs_2_
  7.6 1.9 %convolution_convert_fusion.1 = bf16[256,128]{0,1:T(8,128)(2,1)S(1)} fusion(bf16[2048,128]{1,0:T(8,128)(2,1)} %get-tuple-element.50, bf16[256,2048]{1,0:T(8,128)(2,1)} %get-tuple-element.44, f32[2048]{0:T(1024)} %get-tuple-element.45, f32[256]{0:T(256)S(1)} %add_rsqrt_fusion.2), kind=kOutput, calls=%fused_computation.6 | convolution fusion | flops 136347648 | bytes 1647616 | tf_op jit(solution)/shard_map/cond/branch_0_fun/dot_general | solution.py:1097
  9.7 0.6 multiply_reduce_fusion
  10.5 4.5 %fusion.15 = (f32[256,1024]{1,0:T(8,128)S(1)}, f32[256,1024]{1,0:T(8,128)}) fusion(bf16[2048,1024]{1,0:T(8,128)(2,1)} %get-tuple-element.46, bf16[256,2048]{1,0:T(8,128)(2,1)S(1)} %copy-done.3, f32[2048]{0:T(1024)S(1)} %copy-done.6, f32[256]{0:T(256)S(1)} %add_rsqrt_fusion.2), kind=kOutput, calls=%fused_computation.35 | convolution fusion | flops 1076101120 | bytes 7349248 | tf_op jit(solution)/shard_map/cond/branch_0_fun/dot_general | solution.py:1103
  14.9 0.3 copy.22
  15.5 0.3 copy.23
  15.9 0.1 multiply_convert_fusion.1
  16.1 0.8 maximum_bitcast_fusion.refs_0_
  16.8 0.2 multiply_convert_fusion
  17.0 0.7 broadcast_select_fusion
  17.8 51.6 %exchange.1 = (bf16[8192,128]{1,0:T(8,128)(2,1)}, bf16[256,512]{1,0:T(8,128)(2,1)}, f32[16,32,128]{2,1,0:T(8,128)}) custom-call(bf16[2,256,128]{2,1,0:T(8,128)(2,1)} %maximum_bitcast_fusion.refs_0_, bf16[256,512]{1,0:T(8,128)(2,1)} %get-tuple-element.95.refs_1_, f32[32,128]{1,0:T(8,128)} %reshape.44.refs_2_), custom_call_target="tpu_custom_call" | custom-call | tf_op jit(solution)/shard_map/cond/branch_0_fun/exchange/pallas_call | solution.py:1046
  69.4 1.1 reshape.45
  70.8 1.6 %copy-done = bf16[8192,128]{1,0:T(8,128)(2,1)S(1)} copy-done((bf16[8192,128]{1,0:T(8,128)(2,1)S(1)}, bf16[8192,128]{1,0:T(8,128)(2,1)}, u32[]{:S(2)}) %copy-start) | copy-done | bytes 2097176 | tf_op jit(solution)/shard_map/cond
  72.4 0.9 copy-done.1
  73.4 47.7 %attend_any.1 = bf16[2,256,512]{2,1,0:T(8,128)(2,1)S(1)} custom-call(s32[2]{0:T(128)S(1)} %pad_add_fusion.refs_0_, bf16[256,512]{1,0:T(8,128)(2,1)S(1)} %get-tuple-element.96.refs_1_, bf16[256,512]{1,0:T(8,128)(2,1)S(1)} %copy-done.1, f32[2,256,8]{2,1,0:T(8,128)S(1)} %copy.27.refs_3_, f32[16,8,512]{2,1,0:T(8,128)S(1)} %bitcast.36, bf16[8192,128]{1,0:T(8,128)(2,1)S(1)} %copy-done), custom_call_target="tpu_custom_call" | custom-call | tf_op jit(solution)/shard_map/cond/branch_0_fun/attend_any/pallas_call | solution.py:204
  121.2 13.4 %collective-permute-done = bf16[256,512]{1,0:T(8,128)(2,1)S(1)} collective-permute-done((bf16[256,512]{1,0:T(8,128)(2,1)S(1)}, bf16[256,512]{1,0:T(8,128)(2,1)S(1)}, u32[]{:S(2)}, u32[]{:S(2)}) %collective-permute-start) | collective-permute-done | bytes 262176 | tf_op jit(solution)/shard_map/cond/branch_0_fun/ppermute | solution.py:1075
  134.7 1.3 convolution_convert_fusion
  136.2 1.0 copy.32
  (30 shorter events, 1.0 us)
Async XLA Ops:
  3.8 5.9 %copy-start.3 = (bf16[256,2048]{1,0:T(8,128)(2,1)S(1)}, bf16[256,2048]{1,0:T(8,128)(2,1)}, u32[]{:S(2)}) copy-start(bf16[256,2048]{1,0:T(8,128)(2,1)} %get-tuple-element.44) | copy-start | bytes 3145732 | tf_op jit(solution)/shard_map/cond
  3.8 5.9 %copy-start.5 = (bf16[2048,128]{1,0:T(8,128)(2,1)S(1)}, bf16[2048,128]{1,0:T(8,128)(2,1)}, u32[]{:S(2)}) copy-start(bf16[2048,128]{1,0:T(8,128)(2,1)} %get-tuple-element.48) | copy-start | bytes 1572868 | tf_op jit(solution)/shard_map/cond
  3.8 5.9 %copy-start.6 = (f32[2048]{0:T(1024)S(1)}, f32[2048]{0:T(1024)}, u32[]{:S(2)}) copy-start(f32[2048]{0:T(1024)} %get-tuple-element.45) | copy-start | bytes 24580 | tf_op jit(solution)/shard_map/cond
  15.3 0.7 copy-start.7
  15.4 1.4 %copy-start.4 = (f32[256,1024]{1,0:T(8,128)S(1)}, f32[256,1024]{1,0:T(8,128)}, u32[]{:S(2)}) copy-start(f32[256,1024]{1,0:T(8,128)} %get-tuple-element.100) | copy-start | bytes 3145732 | tf_op jit(solution)/shard_map/cond
  70.8 1.6 %copy-start = (bf16[8192,128]{1,0:T(8,128)(2,1)S(1)}, bf16[8192,128]{1,0:T(8,128)(2,1)}, u32[]{:S(2)}) copy-start(bf16[8192,128]{1,0:T(8,128)(2,1)} %get-tuple-element.54.refs_5_) | copy-start | bytes 6291460 | tf_op jit(solution)/shard_map/cond
  72.4 0.9 copy-start.1
  73.4 61.3 %copy-start.2 = (bf16[1024,2048]{1,0:T(8,128)(2,1)S(1)}, bf16[1024,2048]{1,0:T(8,128)(2,1)}, u32[]{:S(2)}) copy-start(bf16[1024,2048]{1,0:T(8,128)(2,1)} %get-tuple-element.55) | copy-start | bytes 12582916 | tf_op jit(solution)/shard_map/cond
  121.2 13.5 %collective-permute-start = (bf16[256,512]{1,0:T(8,128)(2,1)S(1)}, bf16[256,512]{1,0:T(8,128)(2,1)S(1)}, u32[]{:S(2)}, u32[]{:S(2)}) collective-permute-start(bf16[256,512]{1,0:T(8,128)(2,1)S(1)} %get-tuple-element.94), channel_id=1, source_target_pairs={{0,31},{1,30},{2,29},{3,28},{4,27},{5,26},{6,25},{7,24},{8,23},{9,... | collective-permute-start | bytes 786440 | tf_op jit(solution)/shard_map/cond/branch_0_fun/ppermute | solution.py:1075

commit v4 on v3

--- a/solution.py
+++ b/solution.py
@@ -13,6 +13,7 @@
 HEADS_PER_DOT = 2
 KEY_BLOCK = 512
 SMALL = 60.0
+SPARED = 1
 
 
 def rms_norm(vector, gain_vec):
@@ -222,7 +223,7 @@
 def stream_kernel(
     x_hbm, in_gain, wq_hbm, wk_hbm, wv_hbm, query_gain, key_gain, sums_hbm, wo_hbm, out_ref,
     x_ref, wkv_ref, wq_ref, sums_ref, wo_ref, normed_ref, kvt_ref, query_ref, decay_ref, att_ref,
-    kvt_all, decay_all, far_decay, in_q, qt_ref, acc_ref, kp_all, vt_all, res_ref, loads, kv_recv,
+    kvt_all, decay_all, far_decay, in_q, qt_ref, acc_ref, kp_all, vt_all, res_ref, done_ref, loads, kv_recv,
     decay_recv, x_send, own_send, round_send, late_send, far_send, far_recv, q_send, q_recv,
     back_send, back_recv, *, sizes, lines, rows, heads
 ):
@@ -242,7 +243,8 @@
     is_high = s >= upper
 
     def share(s_):
-        return (2 * units * (2 * s_ + 1 - sp_count) + 2 * s_ + 1) // (2 * (2 * s_ + 1))
+        even = (2 * units * (2 * s_ + 1 - sp_count) + 2 * s_ + 1) // (2 * (2 * s_ + 1))
+        return jnp.maximum(even - SPARED, 0)
 
     given = jnp.where(is_high, share(jnp.maximum(s, upper)), 0)
     taken = jnp.where(is_high, 0, share(jnp.maximum(s_far, upper)))
@@ -325,38 +327,26 @@
             slot = ys + half_count - 1 + (m - 1) * (half_count - 1)
             relay(zo * ys + (y + m) % ys, to_lanes(base + slot * each), sems, go)
 
-    def near_from(z_, way):
-        return inside(z_) if way > 0 else inside(z_) & (z_ < zh)
-
     def round_of(k, go):
-        for d, way in enumerate((1, -1)):
-            base = ((k - 1) * 2 + d) * per * each
-
-            @pl.when(near_from(z - way * k, way))
-            def _():
-                spread(
-                    (z - way * k) * ys + y, base, inside(z + way), ((z + way) * ys + y, g, j),
-                    round_send, go,
-                )
-
-            reach = near_from(z - way * (k - 1), way)
-            if way < 0:
-                reach = reach & (k != 1)
-
-            @pl.when(reach)
-            def _():
-                across(z - way * (k - 1), base, round_send, go)
+        base = (k - 1) * per * each
+
+        @pl.when(inside(z - k))
+        def _():
+            spread(
+                (z - k) * ys + y, base, inside(z + 1), ((z + 1) * ys + y, g, j), round_send, go
+            )
+
+        @pl.when(inside(z - k + 1))
+        def _():
+            across(z - k + 1, base, round_send, go)
 
     def late(zo, go):
-        @pl.when(zo <= zs - 1 - z)
-        def _():
-            base = (zo - zh) * per * each
-            spread(zo * ys + y, base, z > 0, ((z - 1) * ys + y, g, j), late_send, go)
+        base = (zo - 1) * per * each
+        routes = to_rows(base + each) + to_lanes(base + ys * each)
+        relay(zo * ys + y, routes, late_send, go)
 
     def late_across(zo, go):
-        @pl.when(zo <= zs - 1 - z)
-        def _():
-            across(zo, (zo - zh) * per * each, late_send, go)
+        across(zo, (zo - 1) * per * each, late_send, go)
 
     def build(s_):
         for x_ in range(kv_heads):
@@ -389,35 +379,27 @@
             build(s_)
 
     def lanes_of(k):
-        for way in (1, -1):
-
-            @pl.when(near_from(z - way * k, way))
-            def _():
-                s_ = (z - way * k) * ys + y
+        @pl.when(inside(z - k))
+        def _():
+            s_ = (z - k) * ys + y
+            for n in range(1, half_count):
+                arrived(s_, (j + n) % half_count)
+            build_if(s_)
+
+        @pl.when(inside(z - k + 1))
+        def _():
+            for m in range(1, ys):
+                s_ = (z - k + 1) * ys + (y + m) % ys
                 for n in range(1, half_count):
                     arrived(s_, (j + n) % half_count)
                 build_if(s_)
 
-            reach = near_from(z - way * (k - 1), way)
-            if way < 0:
-                reach = reach & (k != 1)
-
-            @pl.when(reach)
-            def _():
-                for m in range(1, ys):
-                    s_ = (z - way * (k - 1)) * ys + (y + m) % ys
-                    for n in range(1, half_count):
-                        arrived(s_, (j + n) % half_count)
-                    build_if(s_)
-
     def late_lanes(zo):
-        @pl.when(zo <= zs - 1 - z)
-        def _():
-            for m in range(ys):
-                s_ = zo * ys + (y + m) % ys
-                for n in range(1, half_count):
-                    arrived(s_, (j + n) % half_count)
-                build_if(s_)
+        for m in range(ys):
+            s_ = zo * ys + (y + m) % ys
+            for n in range(1, half_count):
+                arrived(s_, (j + n) % half_count)
+            build_if(s_)
 
     def q_lanes(group, pair):
         return pl.ds(pl.multiple_of(group * width + pair * 128, 128), 128)
@@ -446,8 +428,15 @@
         greet((s, g, (j + n) % half_count))
         greeted += 1
     greet((s, partner_x, j))
-    greet(((zs - 1 - z) * ys + y, g, j))
-    greeted += 2
+    greeted += 1
+    for z_ in range(zs):
+        met = ((z_ < z) & (z_ <= zs - 1 - z)) | ((z < z_) & (z <= zs - 1 - z_))
+
+        @pl.when(met)
+        def _():
+            greet((z_ * ys + y, g, j))
+
+        greeted = greeted + jnp.where(met, 1, 0)
     for n in range(1, ys):
         greet((z * ys + (y + n) % ys, g, j))
         greeted += 1
@@ -487,7 +476,7 @@
         kvt_ref[n, 0:64] = turned_keys[n * 64 : (n + 1) * 64]
         kvt_ref[n, 64:128] = turned_values[n * 64 : (n + 1) * 64]
     fetches[3].wait()
-    decay_ref[...] = sums_ref[...].T * LOG2E
+    decay_ref[...] = sums_ref[...] * LOG2E
 
     def far_q_copy(group, pair):
         unit = kv_heads * pair + g
@@ -550,8 +539,12 @@
         targets += [(None, (z * ys + (y + n) % ys, g, j)) for n in range(1, ys)]
         return targets
 
-    down = (jnp.where(is_high, zs - 1 - z, jnp.maximum(z - 1, 0)) * ys + y, g, j)
-    down_base = (ys + half_count - 1) * each
+    def each_down(act):
+        for z_ in range(zh - 1, -1, -1):
+
+            @pl.when((z_ < z) & (z_ <= zs - 1 - z))
+            def _():
+                act((ys + half_count - 1 + z_) * each, (z_ * ys + y, g, j))
 
     def each_side(act):
         for slot, (condition, device) in enumerate(side_targets()):
@@ -577,30 +570,26 @@
     x_copy.start()
     each_side(lambda base, device: start_all(own_copies(base, device)))
 
-    @pl.when((z > 0) & jnp.logical_not(is_high))
+    @pl.when(z <= zh)
     def _():
-        start_all(own_copies(down_base, down))
+        each_down(lambda base, device: start_all(own_copies(base, device)))
 
     fetches[4].wait()
     query_columns = columns(query_gain[...] * (LOG2E * 64 ** (-0.5)))
 
     def project(n, carry):
-        at = pl.ds(pl.multiple_of(n * 256, 256), 256)
+        at = pl.ds(pl.multiple_of(n * 512, 512), 512)
         turned = jnp.dot(
             normed_ref[...], wq_ref[:, at], preferred_element_type=jnp.float32
         ).T
         query_ref[at] = per_head(turned, query_columns).astype(jnp.bfloat16)
         return carry
 
-    lax.fori_loop(0, query_ref.shape[0] // 256, project, 0)
+    lax.fori_loop(0, query_ref.shape[0] // 512, project, 0)
 
     @pl.when(z > zh)
     def _():
         far_sends(start_all)
-
-    @pl.when(is_high)
-    def _():
-        start_all(own_copies(down_base, down))
 
     near_sends(start_all)
     kvt_all[own_block] = kvt_ref[g]
@@ -725,9 +714,9 @@
     kv_copy(kvt_ref.at[g], other_block, x_send, here).wait_recv()
     each_side(lambda base, device: start_all(other_copies(base, device)))
 
-    @pl.when(z > 0)
+    @pl.when(z <= zh)
     def _():
-        start_all(other_copies(down_base, down))
+        each_down(lambda base, device: start_all(other_copies(base, device)))
 
     @pl.when(z == zh)
     def _():
@@ -745,39 +734,67 @@
     kept_groups(my_first, lambda at, lanes: diagonal(0, at, lanes, s, offset))
     round_of(1, True)
 
+    def at_step(k):
+        return s - jnp.where(y == 0, jnp.where(k == 1, ys, jnp.where(k == ys, 1, k)), k)
+
+    def comes(zo):
+        return (z < zh) & (zo > z) & (zo <= zs - 1 - z)
+
     def item(k, carry):
+        @pl.when((k == 2) & (z > zh))
+        def _():
+            each_down(
+                lambda base, device: start_all(
+                    own_copies(base, device) + other_copies(base, device)
+                )
+            )
+
         lanes_of(k)
 
+        @pl.when(k <= s)
+        def _():
+            kept_groups(my_first, lambda at, lanes: whole(0, at, lanes, at_step(k)))
+
         @pl.when(k < zs)
         def _():
             round_of(k + 1, True)
 
-        back = jnp.where(y == 0, jnp.where(k == 1, ys, jnp.where(k == ys, 1, k)), k)
-
-        @pl.when(k <= s)
-        def _():
-            kept_groups(my_first, lambda at, lanes: whole(0, at, lanes, s - back))
-
-        return carry
-
-    lax.fori_loop(1, zs + 1, item, 0)
-
-    @pl.when((z > 0) & (z < zh))
-    def _():
-        late(zh, True)
-
-    def partner_phase():
-        def body(i, carry):
+        for step, duty, zo in ((2, late, z + 1), (3, late_across, z + 1), (4, late, z + 2)):
+
+            @pl.when((k == step) & comes(zo))
+            def _():
+                duty(zo, True)
+
+        @pl.when(k == 2)
+        def _():
             for n in range(pairs):
 
-                @pl.when((i == n // 2) & (partner_first <= n))
+                @pl.when(partner_first <= n)
                 def _():
                     q_arrived(n)
                     prepare(1, n, in_q[n], n, own_decays(n, partner_x))
 
+            kept_groups(
+                partner_first, lambda at, lanes: diagonal(1, at, lanes, s, partner_offset)
+            )
+
+        @pl.when((k > 2) & (k - 2 <= s))
+        def _():
+            kept_groups(partner_first, lambda at, lanes: whole(1, at, lanes, at_step(k - 2)))
+
+        return carry
+
+    lax.fori_loop(1, zs + 1, item, 0)
+
+    def partner_phase():
+        def body(i, carry):
             def run(at, lanes):
-                diagonal(1, at, lanes, s, partner_offset)
-                sweep(1, at, lanes, 0, s)
+                def body(k, carry):
+                    whole(1, at, lanes, at_step(k))
+                    return carry
+
+                lax.fori_loop(zs - 1, jnp.minimum(s, zs) + 1, body, 0)
+                sweep(1, at, lanes, 0, jnp.maximum(s - zs, 0))
 
             @pl.when(partner_first <= 2 * i)
             def _():
@@ -793,10 +810,6 @@
                 def _():
                     res_ref[n] = finished(1, n)
                     back_copy(n, n, (s, partner_x, j)).start()
-
-            @pl.when((i == 0) & (z > 0) & (z < zh))
-            def _():
-                late_across(zh, True)
 
             return carry
 
@@ -809,71 +822,49 @@
                 far_recv.at[n], here,
             ).wait_recv()
 
-        def body(i, carry):
-            for n in range(pairs):
-
-                @pl.when((i == n // 2) & (n < taken))
+        for n in range(pairs):
+
+            @pl.when(n < taken)
+            def _():
+                q_arrived(pairs + n)
+                prepare(2, n, in_q[pairs + n], n // kv_heads, far_decays(n))
+
+        def zone(zo, carry):
+            high = jnp.minimum(zo * ys + ys, s_far)
+
+            def body(i, carry):
+                @pl.when(taken >= 2 * i + 2)
                 def _():
-                    q_arrived(pairs + n)
-                    prepare(2, n, in_q[pairs + n], n // kv_heads, far_decays(n))
-
-            @pl.when(taken >= 2 * i + 2)
+                    sweep(2, i * 2 * span, 2 * span, zo * ys, high)
+
+                @pl.when(taken == 2 * i + 1)
+                def _():
+                    sweep(2, i * 2 * span, span, zo * ys, high)
+
+                for turn, ahead, duty, zl in (
+                    (0, 0, late_across, z + 2), (1, 0, late, z + 3), (0, 1, late_across, z + 3),
+                ):
+
+                    @pl.when((i == turn) & (zo == z + ahead) & comes(zl))
+                    def _():
+                        duty(zl, True)
+
+                return carry
+
+            lax.fori_loop(0, pairs // 2, body, 0)
+
+            @pl.when(comes(zo + 1) & (zo > z + 2))
             def _():
-                sweep(2, i * 2 * span, 2 * span, 0, upper)
-
-            @pl.when(taken == 2 * i + 1)
+                late(zo + 1, True)
+                late_across(zo + 1, True)
+
+            @pl.when(comes(zo + 1))
             def _():
-                sweep(2, i * 2 * span, span, 0, upper)
-
-            @pl.when((z == 0) & (i == 0))
-            def _():
-                late(zh, True)
-
-            @pl.when((z == 0) & (i == 1))
-            def _():
-                late_across(zh, True)
-                late(zh + 1, True)
+                late_lanes(zo + 1)
 
             return carry
 
-        lax.fori_loop(0, pairs // 2, body, 0)
-
-    def turn(i, carry):
-        @pl.when((i == 0) == (z > 0))
-        def _():
-            partner_phase()
-
-        @pl.when(((i == 0) == (z == 0)) & (z < zh))
-        def _():
-            far_phase()
-
-        return carry
-
-    lax.fori_loop(0, 2, turn, 0)
-
-    @pl.when(z < zh)
-    def _():
-        def zone(zo, carry):
-            @pl.when(zo > jnp.where(z == 0, zh + 1, zh))
-            def _():
-                late(zo, True)
-                late_across(zo, True)
-
-            @pl.when((z == 0) & (zo == zh))
-            def _():
-                late_across(zh + 1, True)
-
-            late_lanes(zo)
-
-            @pl.when(zo < zs - 1 - z)
-            def _():
-                taken_groups(lambda at, lanes: sweep(2, at, lanes, zo * ys, zo * ys + ys))
-
-            return carry
-
-        lax.fori_loop(zh, zs - z, zone, 0)
-        last = (zs - 1 - z) * ys
-        taken_groups(lambda at, lanes: sweep(2, at, lanes, last, s_far))
+        lax.fori_loop(0, zs - z, zone, 0)
 
         def close(n, carry):
             unit_x = n % kv_heads
@@ -891,6 +882,12 @@
 
         lax.fori_loop(0, taken, close, 0)
 
+    partner_phase()
+
+    @pl.when(z < zh)
+    def _():
+        far_phase()
+
     kept_groups(my_first, lambda at, lanes: sweep(0, at, lanes, 0, jnp.maximum(s - zs, 0)))
     for pair in range(pairs):
 
@@ -903,9 +900,9 @@
         lambda base, device: drain_all(own_copies(base, device) + other_copies(base, device))
     )
 
-    @pl.when(z > 0)
-    def _():
-        drain_all(own_copies(down_base, down) + other_copies(down_base, down))
+    each_down(
+        lambda base, device: drain_all(own_copies(base, device) + other_copies(base, device))
+    )
 
     def drain(k, carry):
         round_of(k, False)
@@ -920,7 +917,7 @@
 
     @pl.when(z < zh)
     def _():
-        lax.fori_loop(zh, zs, drain_late, 0)
+        lax.fori_loop(z + 1, zs - z, drain_late, 0)
 
 
     @pl.when(is_high)
@@ -949,14 +946,18 @@
 
     fetches[5].wait()
 
-    def output(n, carry):
-        at = pl.ds(pl.multiple_of(n * 512, 512), 512)
-        out_ref[:, at] = jnp.dot(
+    model = wo_ref.shape[1]
+    half = model // 2
+    puts = []
+    for n in range(2):
+        at = pl.ds(n * half, half)
+        done_ref[:, at] = jnp.dot(
             att_ref[...], wo_ref[:, at], preferred_element_type=jnp.float32
         ).astype(jnp.bfloat16)
-        return carry
-
-    lax.fori_loop(0, wo_ref.shape[1] // 512, output, 0)
+        puts.append(pltpu.make_async_copy(done_ref.at[:, at], out_ref.at[:, at], loads.at[n]))
+        puts[n].start()
+    for put in puts:
+        put.wait()
 
 
 def lines_of(sp_count):
@@ -971,7 +972,7 @@
     rows, model = inputs.shape
     width = w_query.shape[1]
     heads = width // 64 // kv_heads
-    chunk_rows, local = decay_sums.shape
+    local, chunk_rows = decay_sums.shape
     zs, ys = lines_of(sp_count)
     pairs = heads // 2
     count = sp_count * kv_heads * half_count
@@ -987,7 +988,7 @@
         ),
         out_shape=jax.ShapeDtypeStruct((rows, w_out.shape[1]), jnp.bfloat16),
         in_specs=[hbm, vmem, hbm, hbm, hbm, vmem, vmem, hbm, hbm],
-        out_specs=vmem,
+        out_specs=hbm,
         scratch_shapes=[
             pltpu.VMEM((rows, model), jnp.bfloat16),
             pltpu.VMEM((model, 256), jnp.bfloat16),
@@ -1008,9 +1009,10 @@
             pltpu.VMEM((sp_count, chunk_rows, 128), jnp.bfloat16),
             pltpu.VMEM((sp_count, 80, chunk_rows), jnp.bfloat16),
             pltpu.VMEM((2 * pairs, rows, 128), jnp.bfloat16),
+            pltpu.VMEM((rows, w_out.shape[1]), jnp.bfloat16),
             dma((6,)),
-            dma((count,)), dma((members,)), dma, dma(((ys + half_count) * each,)),
-            dma((zs * 2 * per * each,)), dma(((zs - zs // 2) * per * each,)),
+            dma((count,)), dma((members,)), dma, dma(((ys + half_count + zs // 2) * each,)),
+            dma((zs * per * each,)), dma((zs * per * each,)),
             dma((kv_heads * half_count,)), dma((kv_heads * half_count,)),
             dma((2 * pairs,)), dma((2 * pairs,)), dma((2 * pairs,)), dma((2 * pairs,)),
         ],
@@ -1112,10 +1114,11 @@
 def per_device(*arrays):
     query_gain, key_gain = arrays[5:7]
     sizes = (lax.axis_size("sp"), lax.axis_size("kv"), lax.axis_size("half"))
-    bound = query_gain.shape[0] ** 0.5 * LOG2E * jnp.max(query_gain) * jnp.max(key_gain)
+    most = jnp.max(query_gain[:, None] * key_gain[None, :])
+    bound = query_gain.shape[0] ** 0.5 * LOG2E * most
     return lax.cond(
         bound <= SMALL,
-        lambda *given: stream(*given, sizes),
+        lambda *given: stream(*given[:7], given[7].T, given[8], sizes),
         lambda *given: any_program(*given, sizes),
         *arrays,
     )

time: 138 us -> 136 us (0.986)
  no operation moved by 1% of the time
where the time goes in v4:
time: 136 us
  Pallas kernels  99.4 us (73%)
  waiting for transfers between devices  13.4 us (10%)
  matrix products  8.24 us (6%)
  local copies, waits for them, and re-layouts  6.61 us (5%)
  other arithmetic  6.38 us (5%)
    pallas_call x1, Pallas kernels, any_scores(): pl.pallas_call(lambda *refs: exchange_kernel(*refs, rows=rows, sizes=size...  51.7 us
    pallas_call x1, Pallas kernels, attend(): pl.pallas_call(lambda *refs: attend_kernel(*refs, rows=rows, heads=heads,...  47.7 us
    ppermute x1, waiting for transfers between devices, any_scores(): back = lax.ppermute(attended[1], ALL, mirror)  13.4 us
    dot_general x1, matrix products, any_program(): jnp.dot(normed, w_query, preferred_element_type=jnp.float32)  4.46 us
  transfers between devices with their start and end apart: 1, of which 1 were waited for; matrix products, arithmetic and copies ran while one was open for 0% of the time, Pallas kernels for 0%

profile of v4, /device:TPU:9, one launch (start us, length us, event | category | flops | bytes accessed | tf_op | source)
XLA Modules:
  0.0 135.7 jit_solution(10857188095584231758)
XLA Ops:
  0.0 1.4 multiply_reduce_fusion.1
  2.0 132.7 %conditional.1 = (bf16[256,2048]{1,0:T(8,128)(2,1)S(1)}) conditional(s32[]{:T(128)} %convert_element_type.22, (bf16[256,2048]{1,0:T(8,128)(2,1)}, f32[2048]{0:T(1024)}, bf16[2048,1024]{1,0:T(8,128)(2,1)}, f32[64]{0:T(128)}, bf16[2048,128]{1,0:T(8,128)(2,1)}, /*index=5*/f32[64]{0:T(128)}, bf16[2048,128]{1,0:T(8,128)(2,1)}, f32[1024,4]{0,1:T(4,128)}, ...), branch_computations={%region_1.5_spmd, %region_5.6_spmd} | conditional | flops 2428711680 | bytes 68477896 | solution.py:1119
  2.1 0.8 broadcast_multiply_fusion
  2.9 1.5 %fusion = f32[256]{0:T(256)S(1)} fusion(bf16[256,2048]{1,0:T(8,128)(2,1)} %get-tuple-element.44), kind=kLoop, calls=%fused_computation.3 | loop fusion | flops 1572608 | bytes 1049600 | tf_op jit(solution)/shard_map/cond/branch_0_fun/reduce_sum | solution.py:21
  4.5 0.7 multiply_bitcast_fusion
  5.2 0.6 reshape.46.refs_2_
  5.8 1.9 %convolution_convert_fusion.1 = bf16[256,128]{0,1:T(8,128)(2,1)S(1)} fusion(bf16[2048,128]{1,0:T(8,128)(2,1)} %get-tuple-element.50, bf16[256,2048]{1,0:T(8,128)(2,1)} %get-tuple-element.44, f32[2048]{0:T(1024)} %get-tuple-element.45, f32[256]{0:T(256)S(1)} %add_rsqrt_fusion.2), kind=kOutput, calls=%fused_computation.6 | convolution fusion | flops 136347648 | bytes 1647616 | tf_op jit(solution)/shard_map/cond/branch_0_fun/dot_general | solution.py:1099
  7.9 0.6 multiply_reduce_fusion
  8.5 0.1 copy.28
  8.6 4.5 %fusion.15 = (f32[256,1024]{1,0:T(8,128)S(1)}, f32[256,1024]{1,0:T(8,128)}) fusion(bf16[2048,1024]{1,0:T(8,128)(2,1)} %get-tuple-element.46, bf16[256,2048]{1,0:T(8,128)(2,1)S(1)} %copy-done.3, f32[2048]{0:T(1024)S(1)} %copy-done.6, f32[256]{0:T(256)S(1)} %add_rsqrt_fusion.2), kind=kOutput, calls=%fused_computation.36 | convolution fusion | flops 1076101120 | bytes 7349248 | tf_op jit(solution)/shard_map/cond/branch_0_fun/dot_general | solution.py:1105
  13.1 0.3 copy.26
  13.7 0.3 copy.27
  14.1 0.1 multiply_convert_fusion.1
  14.2 0.8 maximum_bitcast_fusion.refs_0_
  15.0 0.2 multiply_convert_fusion
  15.2 0.7 broadcast_select_fusion
  16.0 51.7 %exchange.1 = (bf16[8192,128]{1,0:T(8,128)(2,1)}, bf16[256,512]{1,0:T(8,128)(2,1)}, f32[16,32,128]{2,1,0:T(8,128)}) custom-call(bf16[2,256,128]{2,1,0:T(8,128)(2,1)} %maximum_bitcast_fusion.refs_0_, bf16[256,512]{1,0:T(8,128)(2,1)} %get-tuple-element.68.refs_1_, f32[32,128]{1,0:T(8,128)} %reshape.46.refs_2_), custom_call_target="tpu_custom_call" | custom-call | tf_op jit(solution)/shard_map/cond/branch_0_fun/exchange/pallas_call | solution.py:1048
  67.6 1.1 reshape.47
  69.1 1.6 %copy-done = bf16[8192,128]{1,0:T(8,128)(2,1)S(1)} copy-done((bf16[8192,128]{1,0:T(8,128)(2,1)S(1)}, bf16[8192,128]{1,0:T(8,128)(2,1)}, u32[]{:S(2)}) %copy-start) | copy-done | bytes 2097176 | tf_op jit(solution)/shard_map/cond
  70.6 0.9 copy-done.1
  71.6 47.7 %attend_any.1 = bf16[2,256,512]{2,1,0:T(8,128)(2,1)S(1)} custom-call(s32[2]{0:T(128)S(1)} %pad_add_fusion.refs_0_, bf16[256,512]{1,0:T(8,128)(2,1)S(1)} %get-tuple-element.69.refs_1_, bf16[256,512]{1,0:T(8,128)(2,1)S(1)} %copy-done.1, f32[2,256,8]{2,1,0:T(8,128)S(1)} %copy.31.refs_3_, f32[16,8,512]{2,1,0:T(8,128)S(1)} %bitcast.37, bf16[8192,128]{1,0:T(8,128)(2,1)S(1)} %copy-done), custom_call_target="tpu_custom_call" | custom-call | tf_op jit(solution)/shard_map/cond/branch_0_fun/attend_any/pallas_call | solution.py:205
  119.5 13.4 %collective-permute-done = bf16[256,512]{1,0:T(8,128)(2,1)S(1)} collective-permute-done((bf16[256,512]{1,0:T(8,128)(2,1)S(1)}, bf16[256,512]{1,0:T(8,128)(2,1)S(1)}, u32[]{:S(2)}, u32[]{:S(2)}) %collective-permute-start) | collective-permute-done | bytes 262176 | tf_op jit(solution)/shard_map/cond/branch_0_fun/ppermute | solution.py:1077
  132.9 1.3 convolution_convert_fusion
  134.7 1.0 copy.35
  (29 shorter events, 0.9 us)
Async XLA Ops:
  2.0 5.9 %copy-start.3 = (bf16[256,2048]{1,0:T(8,128)(2,1)S(1)}, bf16[256,2048]{1,0:T(8,128)(2,1)}, u32[]{:S(2)}) copy-start(bf16[256,2048]{1,0:T(8,128)(2,1)} %get-tuple-element.44) | copy-start | bytes 3145732 | tf_op jit(solution)/shard_map/cond
  2.0 5.9 %copy-start.5 = (bf16[2048,128]{1,0:T(8,128)(2,1)S(1)}, bf16[2048,128]{1,0:T(8,128)(2,1)}, u32[]{:S(2)}) copy-start(bf16[2048,128]{1,0:T(8,128)(2,1)} %get-tuple-element.48) | copy-start | bytes 1572868 | tf_op jit(solution)/shard_map/cond
  2.0 5.9 %copy-start.6 = (f32[2048]{0:T(1024)S(1)}, f32[2048]{0:T(1024)}, u32[]{:S(2)}) copy-start(f32[2048]{0:T(1024)} %get-tuple-element.45) | copy-start | bytes 24580 | tf_op jit(solution)/shard_map/cond
  13.4 0.7 copy-start.7
  13.6 1.5 %copy-start.4 = (f32[256,1024]{1,0:T(8,128)S(1)}, f32[256,1024]{1,0:T(8,128)}, u32[]{:S(2)}) copy-start(f32[256,1024]{1,0:T(8,128)} %get-tuple-element.73) | copy-start | bytes 3145732 | tf_op jit(solution)/shard_map/cond
  69.0 1.6 %copy-start = (bf16[8192,128]{1,0:T(8,128)(2,1)S(1)}, bf16[8192,128]{1,0:T(8,128)(2,1)}, u32[]{:S(2)}) copy-start(bf16[8192,128]{1,0:T(8,128)(2,1)} %get-tuple-element.54.refs_5_) | copy-start | bytes 6291460 | tf_op jit(solution)/shard_map/cond
  70.6 0.9 copy-start.1
  71.6 61.3 %copy-start.2 = (bf16[1024,2048]{1,0:T(8,128)(2,1)S(1)}, bf16[1024,2048]{1,0:T(8,128)(2,1)}, u32[]{:S(2)}) copy-start(bf16[1024,2048]{1,0:T(8,128)(2,1)} %get-tuple-element.55) | copy-start | bytes 12582916 | tf_op jit(solution)/shard_map/cond
  119.4 13.5 %collective-permute-start = (bf16[256,512]{1,0:T(8,128)(2,1)S(1)}, bf16[256,512]{1,0:T(8,128)(2,1)S(1)}, u32[]{:S(2)}, u32[]{:S(2)}) collective-permute-start(bf16[256,512]{1,0:T(8,128)(2,1)S(1)} %get-tuple-element.67), channel_id=1, source_target_pairs={{0,31},{1,30},{2,29},{3,28},{4,27},{5,26},{6,25},{7,24},{8,23},{9,... | collective-permute-start | bytes 786440 | tf_op jit(solution)/shard_map/cond/branch_0_fun/ppermute | solution.py:1077

commit v5 on v4

--- a/solution.py
+++ b/solution.py
@@ -13,7 +13,7 @@
 HEADS_PER_DOT = 2
 KEY_BLOCK = 512
 SMALL = 60.0
-SPARED = 1
+MOVED = (7, 10)
 
 
 def rms_norm(vector, gain_vec):
@@ -223,7 +223,7 @@
 def stream_kernel(
     x_hbm, in_gain, wq_hbm, wk_hbm, wv_hbm, query_gain, key_gain, sums_hbm, wo_hbm, out_ref,
     x_ref, wkv_ref, wq_ref, sums_ref, wo_ref, normed_ref, kvt_ref, query_ref, decay_ref, att_ref,
-    kvt_all, decay_all, far_decay, in_q, qt_ref, acc_ref, kp_all, vt_all, res_ref, done_ref, loads, kv_recv,
+    kvt_all, decay_all, far_decay, in_q, qt_ref, acc_ref, kp_all, vt_all, res_ref, done_ref, sum_ref, loads, kv_recv,
     decay_recv, x_send, own_send, round_send, late_send, far_send, far_recv, q_send, q_recv,
     back_send, back_recv, *, sizes, lines, rows, heads
 ):
@@ -244,7 +244,7 @@
 
     def share(s_):
         even = (2 * units * (2 * s_ + 1 - sp_count) + 2 * s_ + 1) // (2 * (2 * s_ + 1))
-        return jnp.maximum(even - SPARED, 0)
+        return even * MOVED[0] // MOVED[1]
 
     given = jnp.where(is_high, share(jnp.maximum(s, upper)), 0)
     taken = jnp.where(is_high, 0, share(jnp.maximum(s_far, upper)))
@@ -634,7 +634,7 @@
             if limit is not None:
                 key = lax.broadcasted_iota(jnp.int32, (step, lanes), 0)
                 row = lax.broadcasted_iota(jnp.int32, (step, lanes), 1) % rows
-                scores = jnp.where(key <= row, scores, -1e30)
+                scores = jnp.where(key <= row + limit, scores, -1e30)
             weights = jnp.exp2(scores).astype(jnp.bfloat16)
             total = total + jnp.dot(
                 vt_all[chunk, :, where], weights, preferred_element_type=jnp.float32
@@ -652,12 +652,14 @@
         lax.fori_loop(low, high, body, 0)
 
     def diagonal(t, at, lanes, chunk, offset):
+        full = offset // span
+
         def body(i, carry):
-            work(t, at, lanes, chunk, i * rows, rows, rows)
+            work(t, at, lanes, chunk, i * span, span, span)
             return carry
 
-        lax.fori_loop(0, offset // rows, body, 0)
-        work(t, at, lanes, chunk, offset, rows, rows, True)
+        lax.fori_loop(0, full, body, 0)
+        work(t, at, lanes, chunk, full * span, span, span, offset - full * span)
 
     def finished(t, slot):
         out = []
@@ -750,22 +752,24 @@
             )
 
         lanes_of(k)
-
-        @pl.when(k <= s)
-        def _():
-            kept_groups(my_first, lambda at, lanes: whole(0, at, lanes, at_step(k)))
-
-        @pl.when(k < zs)
-        def _():
-            round_of(k + 1, True)
-
-        for step, duty, zo in ((2, late, z + 1), (3, late_across, z + 1), (4, late, z + 2)):
-
-            @pl.when((k == step) & comes(zo))
+        for here_too, step, duty, zo in (
+            (z == 0, 1, late, z + 1), (z == 0, 3, late, z + 2),
+            (z > 0, 2, late, z + 1), (z > 0, 4, late_across, z + 1),
+        ):
+
+            @pl.when(here_too & (k == step) & comes(zo))
             def _():
                 duty(zo, True)
 
-        @pl.when(k == 2)
+        @pl.when(k <= s)
+        def _():
+            kept_groups(my_first, lambda at, lanes: whole(0, at, lanes, at_step(k)))
+
+        @pl.when(k < zs)
+        def _():
+            round_of(k + 1, True)
+
+        @pl.when(k == 1)
         def _():
             for n in range(pairs):
 
@@ -778,9 +782,9 @@
                 partner_first, lambda at, lanes: diagonal(1, at, lanes, s, partner_offset)
             )
 
-        @pl.when((k > 2) & (k - 2 <= s))
-        def _():
-            kept_groups(partner_first, lambda at, lanes: whole(1, at, lanes, at_step(k - 2)))
+        @pl.when((k > 1) & (k - 1 <= s))
+        def _():
+            kept_groups(partner_first, lambda at, lanes: whole(1, at, lanes, at_step(k - 1)))
 
         return carry
 
@@ -793,7 +797,7 @@
                     whole(1, at, lanes, at_step(k))
                     return carry
 
-                lax.fori_loop(zs - 1, jnp.minimum(s, zs) + 1, body, 0)
+                lax.fori_loop(zs, jnp.minimum(s, zs) + 1, body, 0)
                 sweep(1, at, lanes, 0, jnp.maximum(s - zs, 0))
 
             @pl.when(partner_first <= 2 * i)
@@ -842,10 +846,11 @@
                     sweep(2, i * 2 * span, span, zo * ys, high)
 
                 for turn, ahead, duty, zl in (
-                    (0, 0, late_across, z + 2), (1, 0, late, z + 3), (0, 1, late_across, z + 3),
+                    (0, 0, late_across, z + 1), (0, 1, late, z + 3), (1, 1, late_across, z + 2),
+                    (0, 2, late_across, z + 3),
                 ):
 
-                    @pl.when((i == turn) & (zo == z + ahead) & comes(zl))
+                    @pl.when((z == 0) & (i == turn) & (zo == ahead) & comes(zl))
                     def _():
                         duty(zl, True)
 
@@ -853,7 +858,7 @@
 
             lax.fori_loop(0, pairs // 2, body, 0)
 
-            @pl.when(comes(zo + 1) & (zo > z + 2))
+            @pl.when(comes(zo + 1) & (zo > jnp.where(z == 0, 2, z)))
             def _():
                 late(zo + 1, True)
                 late_across(zo + 1, True)
@@ -895,6 +900,33 @@
         def _():
             att_ref[:, q_lanes(g, pair)] = finished(0, pair)
 
+    fetches[5].wait()
+    for pair in range(pairs):
+
+        @pl.when(pair < my_first)
+        def _():
+            back_arrived(g, pair)
+
+    mine = pl.ds(pl.multiple_of(g * width, width), width)
+    theirs = pl.ds(pl.multiple_of(partner_x * width, width), width)
+    model = wo_ref.shape[1]
+    half = model // 2
+    for n in range(2):
+        at = pl.ds(n * half, half)
+        sum_ref[:, at] = jnp.dot(
+            att_ref[:, mine], wo_ref[mine, at], preferred_element_type=jnp.float32
+        )
+    for pair in range(pairs):
+        back_arrived(partner_x, pair)
+    puts = []
+    for n in range(2):
+        at = pl.ds(n * half, half)
+        done_ref[:, at] = (
+            sum_ref[:, at]
+            + jnp.dot(att_ref[:, theirs], wo_ref[theirs, at], preferred_element_type=jnp.float32)
+        ).astype(jnp.bfloat16)
+        puts.append(pltpu.make_async_copy(done_ref.at[:, at], out_ref.at[:, at], loads.at[n]))
+        puts[n].start()
     x_copy.wait_send()
     each_side(
         lambda base, device: drain_all(own_copies(base, device) + other_copies(base, device))
@@ -937,25 +969,6 @@
             back_copy(
                 pairs + pair, pair // kv_heads, (s_far, pair % kv_heads, j)
             ).wait_send()
-
-        back_arrived(partner_x, pair)
-
-        @pl.when(pair < my_first)
-        def _():
-            back_arrived(g, pair)
-
-    fetches[5].wait()
-
-    model = wo_ref.shape[1]
-    half = model // 2
-    puts = []
-    for n in range(2):
-        at = pl.ds(n * half, half)
-        done_ref[:, at] = jnp.dot(
-            att_ref[...], wo_ref[:, at], preferred_element_type=jnp.float32
-        ).astype(jnp.bfloat16)
-        puts.append(pltpu.make_async_copy(done_ref.at[:, at], out_ref.at[:, at], loads.at[n]))
-        puts[n].start()
     for put in puts:
         put.wait()
 
@@ -1010,6 +1023,7 @@
             pltpu.VMEM((sp_count, 80, chunk_rows), jnp.bfloat16),
             pltpu.VMEM((2 * pairs, rows, 128), jnp.bfloat16),
             pltpu.VMEM((rows, w_out.shape[1]), jnp.bfloat16),
+            pltpu.VMEM((rows, w_out.shape[1]), jnp.float32),
             dma((6,)),
             dma((count,)), dma((members,)), dma, dma(((ys + half_count + zs // 2) * each,)),
             dma((zs * per * each,)), dma((zs * per * each,)),

time: 136 us -> 136 us (level)
  no operation moved by 1% of the time
where the time goes in v5:
time: 136 us
  Pallas kernels  99.4 us (73%)
  waiting for transfers between devices  13.4 us (10%)
  matrix products  8.24 us (6%)
  local copies, waits for them, and re-layouts  6.61 us (5%)
  other arithmetic  6.38 us (5%)
    pallas_call x1, Pallas kernels, any_scores(): pl.pallas_call(lambda *refs: exchange_kernel(*refs, rows=rows, sizes=size...  51.7 us
    pallas_call x1, Pallas kernels, attend(): pl.pallas_call(lambda *refs: attend_kernel(*refs, rows=rows, heads=heads,...  47.7 us
    ppermute x1, waiting for transfers between devices, any_scores(): back = lax.ppermute(attended[1], ALL, mirror)  13.4 us
    dot_general x1, matrix products, any_program(): jnp.dot(normed, w_query, preferred_element_type=jnp.float32)  4.46 us
  transfers between devices with their start and end apart: 1, of which 1 were waited for; matrix products, arithmetic and copies ran while one was open for 0% of the time, Pallas kernels for 0%

profile of v5, /device:TPU:9, one launch (start us, length us, event | category | flops | bytes accessed | tf_op | source)
XLA Modules:
  0.0 135.7 jit_solution(7647333040377334563)
XLA Ops:
  0.0 1.4 multiply_reduce_fusion.1
  2.0 132.7 %conditional.1 = (bf16[256,2048]{1,0:T(8,128)(2,1)S(1)}) conditional(s32[]{:T(128)} %convert_element_type.22, (bf16[256,2048]{1,0:T(8,128)(2,1)}, f32[2048]{0:T(1024)}, bf16[2048,1024]{1,0:T(8,128)(2,1)}, f32[64]{0:T(128)}, bf16[2048,128]{1,0:T(8,128)(2,1)}, /*index=5*/f32[64]{0:T(128)}, bf16[2048,128]{1,0:T(8,128)(2,1)}, f32[1024,4]{0,1:T(4,128)}, ...), branch_computations={%region_1.5_spmd, %region_5.6_spmd} | conditional | flops 2428711680 | bytes 68477896 | solution.py:1133
  2.1 0.8 broadcast_multiply_fusion
  2.9 1.5 %fusion = f32[256]{0:T(256)S(1)} fusion(bf16[256,2048]{1,0:T(8,128)(2,1)} %get-tuple-element.44), kind=kLoop, calls=%fused_computation.3 | loop fusion | flops 1572608 | bytes 1049600 | tf_op jit(solution)/shard_map/cond/branch_0_fun/reduce_sum | solution.py:21
  4.5 0.7 multiply_bitcast_fusion
  5.2 0.6 reshape.46.refs_2_
  5.8 1.9 %convolution_convert_fusion.1 = bf16[256,128]{0,1:T(8,128)(2,1)S(1)} fusion(bf16[2048,128]{1,0:T(8,128)(2,1)} %get-tuple-element.50, bf16[256,2048]{1,0:T(8,128)(2,1)} %get-tuple-element.44, f32[2048]{0:T(1024)} %get-tuple-element.45, f32[256]{0:T(256)S(1)} %add_rsqrt_fusion.2), kind=kOutput, calls=%fused_computation.6 | convolution fusion | flops 136347648 | bytes 1647616 | tf_op jit(solution)/shard_map/cond/branch_0_fun/dot_general | solution.py:1113
  7.9 0.6 multiply_reduce_fusion
  8.5 0.1 copy.28
  8.6 4.5 %fusion.15 = (f32[256,1024]{1,0:T(8,128)S(1)}, f32[256,1024]{1,0:T(8,128)}) fusion(bf16[2048,1024]{1,0:T(8,128)(2,1)} %get-tuple-element.46, bf16[256,2048]{1,0:T(8,128)(2,1)S(1)} %copy-done.3, f32[2048]{0:T(1024)S(1)} %copy-done.6, f32[256]{0:T(256)S(1)} %add_rsqrt_fusion.2), kind=kOutput, calls=%fused_computation.36 | convolution fusion | flops 1076101120 | bytes 7349248 | tf_op jit(solution)/shard_map/cond/branch_0_fun/dot_general | solution.py:1119
  13.1 0.3 copy.26
  13.7 0.3 copy.27
  14.1 0.1 multiply_convert_fusion.1
  14.2 0.8 maximum_bitcast_fusion.refs_0_
  15.0 0.2 multiply_convert_fusion
  15.2 0.7 broadcast_select_fusion
  16.0 51.7 %exchange.1 = (bf16[8192,128]{1,0:T(8,128)(2,1)}, bf16[256,512]{1,0:T(8,128)(2,1)}, f32[16,32,128]{2,1,0:T(8,128)}) custom-call(bf16[2,256,128]{2,1,0:T(8,128)(2,1)} %maximum_bitcast_fusion.refs_0_, bf16[256,512]{1,0:T(8,128)(2,1)} %get-tuple-element.68.refs_1_, f32[32,128]{1,0:T(8,128)} %reshape.46.refs_2_), custom_call_target="tpu_custom_call" | custom-call | tf_op jit(solution)/shard_map/cond/branch_0_fun/exchange/pallas_call | solution.py:1062
  67.6 1.1 reshape.47
  69.1 1.6 %copy-done = bf16[8192,128]{1,0:T(8,128)(2,1)S(1)} copy-done((bf16[8192,128]{1,0:T(8,128)(2,1)S(1)}, bf16[8192,128]{1,0:T(8,128)(2,1)}, u32[]{:S(2)}) %copy-start) | copy-done | bytes 2097176 | tf_op jit(solution)/shard_map/cond
  70.6 0.9 copy-done.1
  71.6 47.7 %attend_any.1 = bf16[2,256,512]{2,1,0:T(8,128)(2,1)S(1)} custom-call(s32[2]{0:T(128)S(1)} %pad_add_fusion.refs_0_, bf16[256,512]{1,0:T(8,128)(2,1)S(1)} %get-tuple-element.69.refs_1_, bf16[256,512]{1,0:T(8,128)(2,1)S(1)} %copy-done.1, f32[2,256,8]{2,1,0:T(8,128)S(1)} %copy.31.refs_3_, f32[16,8,512]{2,1,0:T(8,128)S(1)} %bitcast.37, bf16[8192,128]{1,0:T(8,128)(2,1)S(1)} %copy-done), custom_call_target="tpu_custom_call" | custom-call | tf_op jit(solution)/shard_map/cond/branch_0_fun/attend_any/pallas_call | solution.py:205
  119.5 13.4 %collective-permute-done = bf16[256,512]{1,0:T(8,128)(2,1)S(1)} collective-permute-done((bf16[256,512]{1,0:T(8,128)(2,1)S(1)}, bf16[256,512]{1,0:T(8,128)(2,1)S(1)}, u32[]{:S(2)}, u32[]{:S(2)}) %collective-permute-start) | collective-permute-done | bytes 262176 | tf_op jit(solution)/shard_map/cond/branch_0_fun/ppermute | solution.py:1091
  132.9 1.3 convolution_convert_fusion
  134.7 1.0 copy.35
  (29 shorter events, 0.9 us)
Async XLA Ops:
  2.0 5.9 %copy-start.3 = (bf16[256,2048]{1,0:T(8,128)(2,1)S(1)}, bf16[256,2048]{1,0:T(8,128)(2,1)}, u32[]{:S(2)}) copy-start(bf16[256,2048]{1,0:T(8,128)(2,1)} %get-tuple-element.44) | copy-start | bytes 3145732 | tf_op jit(solution)/shard_map/cond
  2.0 5.9 %copy-start.5 = (bf16[2048,128]{1,0:T(8,128)(2,1)S(1)}, bf16[2048,128]{1,0:T(8,128)(2,1)}, u32[]{:S(2)}) copy-start(bf16[2048,128]{1,0:T(8,128)(2,1)} %get-tuple-element.48) | copy-start | bytes 1572868 | tf_op jit(solution)/shard_map/cond
  2.0 5.9 %copy-start.6 = (f32[2048]{0:T(1024)S(1)}, f32[2048]{0:T(1024)}, u32[]{:S(2)}) copy-start(f32[2048]{0:T(1024)} %get-tuple-element.45) | copy-start | bytes 24580 | tf_op jit(solution)/shard_map/cond
  13.4 0.7 copy-start.7
  13.6 1.5 %copy-start.4 = (f32[256,1024]{1,0:T(8,128)S(1)}, f32[256,1024]{1,0:T(8,128)}, u32[]{:S(2)}) copy-start(f32[256,1024]{1,0:T(8,128)} %get-tuple-element.73) | copy-start | bytes 3145732 | tf_op jit(solution)/shard_map/cond
  69.0 1.6 %copy-start = (bf16[8192,128]{1,0:T(8,128)(2,1)S(1)}, bf16[8192,128]{1,0:T(8,128)(2,1)}, u32[]{:S(2)}) copy-start(bf16[8192,128]{1,0:T(8,128)(2,1)} %get-tuple-element.54.refs_5_) | copy-start | bytes 6291460 | tf_op jit(solution)/shard_map/cond
  70.6 0.9 copy-start.1
  71.6 61.3 %copy-start.2 = (bf16[1024,2048]{1,0:T(8,128)(2,1)S(1)}, bf16[1024,2048]{1,0:T(8,128)(2,1)}, u32[]{:S(2)}) copy-start(bf16[1024,2048]{1,0:T(8,128)(2,1)} %get-tuple-element.55) | copy-start | bytes 12582916 | tf_op jit(solution)/shard_map/cond
  119.4 13.5 %collective-permute-start = (bf16[256,512]{1,0:T(8,128)(2,1)S(1)}, bf16[256,512]{1,0:T(8,128)(2,1)S(1)}, u32[]{:S(2)}, u32[]{:S(2)}) collective-permute-start(bf16[256,512]{1,0:T(8,128)(2,1)S(1)} %get-tuple-element.67), channel_id=1, source_target_pairs={{0,31},{1,30},{2,29},{3,28},{4,27},{5,26},{6,25},{7,24},{8,23},{9,... | collective-permute-start | bytes 786440 | tf_op jit(solution)/shard_map/cond/branch_0_fun/ppermute | solution.py:1091

commit v6 on v5

--- a/solution.py
+++ b/solution.py
@@ -577,15 +577,12 @@
     fetches[4].wait()
     query_columns = columns(query_gain[...] * (LOG2E * 64 ** (-0.5)))
 
-    def project(n, carry):
-        at = pl.ds(pl.multiple_of(n * 512, 512), 512)
+    for n in range(query_ref.shape[0] // 256):
+        at = pl.ds(n * 256, 256)
         turned = jnp.dot(
             normed_ref[...], wq_ref[:, at], preferred_element_type=jnp.float32
         ).T
         query_ref[at] = per_head(turned, query_columns).astype(jnp.bfloat16)
-        return carry
-
-    lax.fori_loop(0, query_ref.shape[0] // 512, project, 0)
 
     @pl.when(z > zh)
     def _():
@@ -644,22 +641,12 @@
     def whole(t, at, lanes, chunk):
         work(t, at, lanes, chunk, 0, chunk_rows, chunk_rows if lanes == span else chunk_rows // 2)
 
-    def sweep(t, at, lanes, low, high):
-        def body(chunk, carry):
-            whole(t, at, lanes, chunk)
+    def diagonal(t, at, lanes, chunk, offset):
+        def body(i, carry):
+            work(t, at, lanes, chunk, i * span, span, span, offset - i * span)
             return carry
 
-        lax.fori_loop(low, high, body, 0)
-
-    def diagonal(t, at, lanes, chunk, offset):
-        full = offset // span
-
-        def body(i, carry):
-            work(t, at, lanes, chunk, i * span, span, span)
-            return carry
-
-        lax.fori_loop(0, full, body, 0)
-        work(t, at, lanes, chunk, full * span, span, span, offset - full * span)
+        lax.fori_loop(0, offset // span + 1, body, 0)
 
     def finished(t, slot):
         out = []
@@ -680,33 +667,25 @@
             back_recv.at[group * pairs + pair], here,
         ).wait_recv()
 
+    assert MOVED[0] * pairs // MOVED[1] <= kv_heads
+
     def kept_groups(first, act):
-        def body(i, carry):
-            @pl.when(first <= 2 * i)
-            def _():
-                act(i * 2 * span, 2 * span)
-
-            @pl.when(first == 2 * i + 1)
-            def _():
-                act((2 * i + 1) * span, span)
-
-            return carry
-
-        lax.fori_loop(0, pairs // 2, body, 0)
+        @pl.when(first == 0)
+        def _():
+            act(0, pairs * span)
+
+        @pl.when(first > 0)
+        def _():
+            act(span, (pairs - 1) * span)
 
     def taken_groups(act):
-        def body(i, carry):
-            @pl.when(taken >= 2 * i + 2)
-            def _():
-                act(i * 2 * span, 2 * span)
-
-            @pl.when(taken == 2 * i + 1)
-            def _():
-                act(i * 2 * span, span)
-
-            return carry
-
-        lax.fori_loop(0, pairs // 2, body, 0)
+        @pl.when(taken == 2)
+        def _():
+            act(0, 2 * span)
+
+        @pl.when(taken == 1)
+        def _():
+            act(0, span)
 
     my_first = kept_from(g)
     partner_first = kept_from(partner_x)
@@ -733,91 +712,91 @@
     build(s)
     for pair in range(pairs):
         prepare(0, pair, query_ref[q_lanes(g, pair)], pair, own_decays(pair, g))
-    kept_groups(my_first, lambda at, lanes: diagonal(0, at, lanes, s, offset))
-    round_of(1, True)
-
     def at_step(k):
         return s - jnp.where(y == 0, jnp.where(k == 1, ys, jnp.where(k == ys, 1, k)), k)
 
     def comes(zo):
         return (z < zh) & (zo > z) & (zo <= zs - 1 - z)
 
-    def item(k, carry):
-        @pl.when((k == 2) & (z > zh))
-        def _():
-            each_down(
-                lambda base, device: start_all(
-                    own_copies(base, device) + other_copies(base, device)
+    first_steps = 2 * (zs + 1)
+    left = jnp.maximum(s - zs + 1, 0)
+
+    def item(f, carry):
+        early = f < first_steps
+        late_f = f - first_steps
+        k = f // 2
+        turn = jnp.where(early, f % 2, jnp.where(late_f < left, 1, 0))
+        step = jnp.where(
+            early, k - turn, jnp.where(late_f < left, zs + late_f, zs + late_f - left)
+        )
+        idle = early & (turn == 0) & (k == zs) & (s >= zs)
+
+        @pl.when(early & (turn == 0) & (k > 0))
+        def _():
+            @pl.when((k == 2) & (z > zh))
+            def _():
+                each_down(
+                    lambda base, device: start_all(
+                        own_copies(base, device) + other_copies(base, device)
+                    )
                 )
-            )
-
-        lanes_of(k)
-        for here_too, step, duty, zo in (
-            (z == 0, 1, late, z + 1), (z == 0, 3, late, z + 2),
-            (z > 0, 2, late, z + 1), (z > 0, 4, late_across, z + 1),
-        ):
-
-            @pl.when(here_too & (k == step) & comes(zo))
+
+            lanes_of(k)
+            for here_too, when, duty, zo in (
+                (z == 0, 1, late, z + 1), (z == 0, 3, late, z + 2),
+                (z > 0, 2, late, z + 1), (z > 0, 4, late_across, z + 1),
+            ):
+
+                @pl.when(here_too & (k == when) & comes(zo))
+                def _():
+                    duty(zo, True)
+
+        @pl.when(early & (turn == 1))
+        def _():
+            @pl.when(k < zs)
             def _():
-                duty(zo, True)
-
-        @pl.when(k <= s)
-        def _():
-            kept_groups(my_first, lambda at, lanes: whole(0, at, lanes, at_step(k)))
-
-        @pl.when(k < zs)
-        def _():
-            round_of(k + 1, True)
-
-        @pl.when(k == 1)
+                round_of(k + 1, True)
+
+            @pl.when(k == 1)
+            def _():
+                for n in range(pairs):
+
+                    @pl.when(partner_first <= n)
+                    def _():
+                        q_arrived(n)
+                        prepare(1, n, in_q[n], n, own_decays(n, partner_x))
+
+        kept = jnp.where(turn == 0, my_first, partner_first)
+        start = jnp.where(turn == 0, offset, partner_offset)
+
+        @pl.when(step == 0)
+        def _():
+            kept_groups(kept, lambda at, lanes: diagonal(turn, at, lanes, s, start))
+
+        @pl.when((step > 0) & (step <= s) & jnp.logical_not(idle))
+        def _():
+            kept_groups(kept, lambda at, lanes: whole(turn, at, lanes, at_step(step)))
+
+        @pl.when((step == s) & (turn == 0) & jnp.logical_not(idle))
+        def _():
+            for pair in range(pairs):
+
+                @pl.when(pair >= my_first)
+                def _():
+                    att_ref[:, q_lanes(g, pair)] = finished(0, pair)
+
+        @pl.when((step == s) & (turn == 1))
         def _():
             for n in range(pairs):
 
                 @pl.when(partner_first <= n)
-                def _():
-                    q_arrived(n)
-                    prepare(1, n, in_q[n], n, own_decays(n, partner_x))
-
-            kept_groups(
-                partner_first, lambda at, lanes: diagonal(1, at, lanes, s, partner_offset)
-            )
-
-        @pl.when((k > 1) & (k - 1 <= s))
-        def _():
-            kept_groups(partner_first, lambda at, lanes: whole(1, at, lanes, at_step(k - 1)))
-
-        return carry
-
-    lax.fori_loop(1, zs + 1, item, 0)
-
-    def partner_phase():
-        def body(i, carry):
-            def run(at, lanes):
-                def body(k, carry):
-                    whole(1, at, lanes, at_step(k))
-                    return carry
-
-                lax.fori_loop(zs, jnp.minimum(s, zs) + 1, body, 0)
-                sweep(1, at, lanes, 0, jnp.maximum(s - zs, 0))
-
-            @pl.when(partner_first <= 2 * i)
-            def _():
-                run(i * 2 * span, 2 * span)
-
-            @pl.when(partner_first == 2 * i + 1)
-            def _():
-                run((2 * i + 1) * span, span)
-
-            for n in range(pairs):
-
-                @pl.when((i == n // 2) & (partner_first <= n))
                 def _():
                     res_ref[n] = finished(1, n)
                     back_copy(n, n, (s, partner_x, j)).start()
 
-            return carry
-
-        lax.fori_loop(0, pairs // 2, body, 0)
+        return carry
+
+    lax.fori_loop(0, first_steps + 2 * left, item, 0)
 
     def far_phase():
         for n in range(kv_heads * half_count):
@@ -834,29 +813,25 @@
                 prepare(2, n, in_q[pairs + n], n // kv_heads, far_decays(n))
 
         def zone(zo, carry):
-            high = jnp.minimum(zo * ys + ys, s_far)
-
             def body(i, carry):
-                @pl.when(taken >= 2 * i + 2)
+                chunk = zo * ys + i
+
+                @pl.when(chunk < s_far)
                 def _():
-                    sweep(2, i * 2 * span, 2 * span, zo * ys, high)
-
-                @pl.when(taken == 2 * i + 1)
-                def _():
-                    sweep(2, i * 2 * span, span, zo * ys, high)
-
-                for turn, ahead, duty, zl in (
-                    (0, 0, late_across, z + 1), (0, 1, late, z + 3), (1, 1, late_across, z + 2),
+                    taken_groups(lambda at, lanes: whole(2, at, lanes, chunk))
+
+                for place, ahead, duty, zl in (
+                    (0, 0, late_across, z + 1), (0, 1, late, z + 3), (ys - 1, 1, late_across, z + 2),
                     (0, 2, late_across, z + 3),
                 ):
 
-                    @pl.when((z == 0) & (i == turn) & (zo == ahead) & comes(zl))
+                    @pl.when((z == 0) & (i == place) & (zo == ahead) & comes(zl))
                     def _():
                         duty(zl, True)
 
                 return carry
 
-            lax.fori_loop(0, pairs // 2, body, 0)
+            lax.fori_loop(0, ys, body, 0)
 
             @pl.when(comes(zo + 1) & (zo > jnp.where(z == 0, 2, z)))
             def _():
@@ -887,44 +862,36 @@
 
         lax.fori_loop(0, taken, close, 0)
 
-    partner_phase()
-
     @pl.when(z < zh)
     def _():
         far_phase()
 
-    kept_groups(my_first, lambda at, lanes: sweep(0, at, lanes, 0, jnp.maximum(s - zs, 0)))
-    for pair in range(pairs):
-
-        @pl.when(pair >= my_first)
-        def _():
-            att_ref[:, q_lanes(g, pair)] = finished(0, pair)
-
     fetches[5].wait()
-    for pair in range(pairs):
-
-        @pl.when(pair < my_first)
-        def _():
-            back_arrived(g, pair)
-
-    mine = pl.ds(pl.multiple_of(g * width, width), width)
-    theirs = pl.ds(pl.multiple_of(partner_x * width, width), width)
-    model = wo_ref.shape[1]
-    half = model // 2
-    for n in range(2):
-        at = pl.ds(n * half, half)
-        sum_ref[:, at] = jnp.dot(
-            att_ref[:, mine], wo_ref[mine, at], preferred_element_type=jnp.float32
-        )
-    for pair in range(pairs):
+    for pair in range(1, pairs):
         back_arrived(partner_x, pair)
+
+    firsts = [pl.ds(n * width, 128) for n in range(kv_heads)]
+    others = [pl.ds(n * width + 128, width - 128) for n in range(kv_heads)]
+    quarter = wo_ref.shape[1] // 4
+
+    def output(parts, at):
+        rows_in = jnp.concatenate([att_ref[:, part] for part in parts], axis=1)
+        weights_in = jnp.concatenate([wo_ref[part, at] for part in parts], axis=0)
+        return jnp.dot(rows_in, weights_in, preferred_element_type=jnp.float32)
+
+    for n in range(4):
+        at = pl.ds(n * quarter, quarter)
+        sum_ref[:, at] = output(others, at)
+
+    @pl.when(my_first > 0)
+    def _():
+        back_arrived(g, 0)
+
+    back_arrived(partner_x, 0)
     puts = []
-    for n in range(2):
-        at = pl.ds(n * half, half)
-        done_ref[:, at] = (
-            sum_ref[:, at]
-            + jnp.dot(att_ref[:, theirs], wo_ref[theirs, at], preferred_element_type=jnp.float32)
-        ).astype(jnp.bfloat16)
+    for n in range(4):
+        at = pl.ds(n * quarter, quarter)
+        done_ref[:, at] = (sum_ref[:, at] + output(firsts, at)).astype(jnp.bfloat16)
         puts.append(pltpu.make_async_copy(done_ref.at[:, at], out_ref.at[:, at], loads.at[n]))
         puts[n].start()
     x_copy.wait_send()

time: 136 us -> 136 us (level)
  no operation moved by 1% of the time
where the time goes in v6:
time: 136 us; the launch traced here: 135 us
  Pallas kernels  99.4 us (73%)
  waiting for transfers between devices  13.4 us (10%)
  matrix products  8.24 us (6%)
  local copies, waits for them, and re-layouts  6.61 us (5%)
  other arithmetic  6.38 us (5%)
    pallas_call x1, Pallas kernels, any_scores(): pl.pallas_call(lambda *refs: exchange_kernel(*refs, rows=rows, sizes=size...  51.7 us
    pallas_call x1, Pallas kernels, attend(): pl.pallas_call(lambda *refs: attend_kernel(*refs, rows=rows, heads=heads,...  47.7 us
    ppermute x1, waiting for transfers between devices, any_scores(): back = lax.ppermute(attended[1], ALL, mirror)  13.4 us
    dot_general x1, matrix products, any_program(): jnp.dot(normed, w_query, preferred_element_type=jnp.float32)  4.46 us
  transfers between devices with their start and end apart: 1, of which 1 were waited for; matrix products, arithmetic and copies ran while one was open for 0% of the time, Pallas kernels for 0%

profile of v6, /device:TPU:9, one launch (start us, length us, event | category | flops | bytes accessed | tf_op | source)
XLA Modules:
  0.0 135.4 jit_solution(16547191690507168246)
XLA Ops:
  0.0 1.4 multiply_reduce_fusion.1
  2.0 132.4 %conditional.1 = (bf16[256,2048]{1,0:T(8,128)(2,1)S(1)}) conditional(s32[]{:T(128)} %convert_element_type.22, (bf16[256,2048]{1,0:T(8,128)(2,1)}, f32[2048]{0:T(1024)}, bf16[2048,1024]{1,0:T(8,128)(2,1)}, f32[64]{0:T(128)}, bf16[2048,128]{1,0:T(8,128)(2,1)}, /*index=5*/f32[64]{0:T(128)}, bf16[2048,128]{1,0:T(8,128)(2,1)}, f32[1024,4]{0,1:T(4,128)}, ...), branch_computations={%region_1.5_spmd, %region_5.6_spmd} | conditional | flops 2428711680 | bytes 68477896 | solution.py:1100
  2.1 0.8 broadcast_multiply_fusion
  2.9 1.5 %fusion = f32[256]{0:T(256)S(1)} fusion(bf16[256,2048]{1,0:T(8,128)(2,1)} %get-tuple-element.44), kind=kLoop, calls=%fused_computation.3 | loop fusion | flops 1572608 | bytes 1049600 | tf_op jit(solution)/shard_map/cond/branch_0_fun/reduce_sum | solution.py:21
  4.5 0.7 multiply_bitcast_fusion
  5.2 0.6 reshape.46.refs_2_
  5.8 1.9 %convolution_convert_fusion.1 = bf16[256,128]{0,1:T(8,128)(2,1)S(1)} fusion(bf16[2048,128]{1,0:T(8,128)(2,1)} %get-tuple-element.50, bf16[256,2048]{1,0:T(8,128)(2,1)} %get-tuple-element.44, f32[2048]{0:T(1024)} %get-tuple-element.45, f32[256]{0:T(256)S(1)} %add_rsqrt_fusion.2), kind=kOutput, calls=%fused_computation.6 | convolution fusion | flops 136347648 | bytes 1647616 | tf_op jit(solution)/shard_map/cond/branch_0_fun/dot_general | solution.py:1080
  7.9 0.6 multiply_reduce_fusion
  8.5 0.1 copy.28
  8.6 4.5 %fusion.15 = (f32[256,1024]{1,0:T(8,128)S(1)}, f32[256,1024]{1,0:T(8,128)}) fusion(bf16[2048,1024]{1,0:T(8,128)(2,1)} %get-tuple-element.46, bf16[256,2048]{1,0:T(8,128)(2,1)S(1)} %copy-done.3, f32[2048]{0:T(1024)S(1)} %copy-done.6, f32[256]{0:T(256)S(1)} %add_rsqrt_fusion.2), kind=kOutput, calls=%fused_computation.36 | convolution fusion | flops 1076101120 | bytes 7349248 | tf_op jit(solution)/shard_map/cond/branch_0_fun/dot_general | solution.py:1086
  13.1 0.3 copy.26
  13.7 0.3 copy.27
  14.1 0.1 multiply_convert_fusion.1
  14.2 0.8 maximum_bitcast_fusion.refs_0_
  15.0 0.2 multiply_convert_fusion
  15.2 0.7 broadcast_select_fusion
  16.0 51.7 %exchange.1 = (bf16[8192,128]{1,0:T(8,128)(2,1)}, bf16[256,512]{1,0:T(8,128)(2,1)}, f32[16,32,128]{2,1,0:T(8,128)}) custom-call(bf16[2,256,128]{2,1,0:T(8,128)(2,1)} %maximum_bitcast_fusion.refs_0_, bf16[256,512]{1,0:T(8,128)(2,1)} %get-tuple-element.68.refs_1_, f32[32,128]{1,0:T(8,128)} %reshape.46.refs_2_), custom_call_target="tpu_custom_call" | custom-call | tf_op jit(solution)/shard_map/cond/branch_0_fun/exchange/pallas_call | solution.py:1029
  67.6 1.1 reshape.47
  69.1 1.6 %copy-done = bf16[8192,128]{1,0:T(8,128)(2,1)S(1)} copy-done((bf16[8192,128]{1,0:T(8,128)(2,1)S(1)}, bf16[8192,128]{1,0:T(8,128)(2,1)}, u32[]{:S(2)}) %copy-start) | copy-done | bytes 2097176 | tf_op jit(solution)/shard_map/cond
  70.6 0.9 copy-done.1
  71.6 47.7 %attend_any.1 = bf16[2,256,512]{2,1,0:T(8,128)(2,1)S(1)} custom-call(s32[2]{0:T(128)S(1)} %pad_add_fusion.refs_0_, bf16[256,512]{1,0:T(8,128)(2,1)S(1)} %get-tuple-element.69.refs_1_, bf16[256,512]{1,0:T(8,128)(2,1)S(1)} %copy-done.1, f32[2,256,8]{2,1,0:T(8,128)S(1)} %copy.31.refs_3_, f32[16,8,512]{2,1,0:T(8,128)S(1)} %bitcast.37, bf16[8192,128]{1,0:T(8,128)(2,1)S(1)} %copy-done), custom_call_target="tpu_custom_call" | custom-call | tf_op jit(solution)/shard_map/cond/branch_0_fun/attend_any/pallas_call | solution.py:205
  119.5 13.4 %collective-permute-done = bf16[256,512]{1,0:T(8,128)(2,1)S(1)} collective-permute-done((bf16[256,512]{1,0:T(8,128)(2,1)S(1)}, bf16[256,512]{1,0:T(8,128)(2,1)S(1)}, u32[]{:S(2)}, u32[]{:S(2)}) %collective-permute-start) | collective-permute-done | bytes 262176 | tf_op jit(solution)/shard_map/cond/branch_0_fun/ppermute | solution.py:1058
  132.9 1.3 convolution_convert_fusion
  134.4 1.0 copy.35
  (29 shorter events, 0.9 us)
Async XLA Ops:
  2.0 5.9 %copy-start.3 = (bf16[256,2048]{1,0:T(8,128)(2,1)S(1)}, bf16[256,2048]{1,0:T(8,128)(2,1)}, u32[]{:S(2)}) copy-start(bf16[256,2048]{1,0:T(8,128)(2,1)} %get-tuple-element.44) | copy-start | bytes 3145732 | tf_op jit(solution)/shard_map/cond
  2.0 5.9 %copy-start.5 = (bf16[2048,128]{1,0:T(8,128)(2,1)S(1)}, bf16[2048,128]{1,0:T(8,128)(2,1)}, u32[]{:S(2)}) copy-start(bf16[2048,128]{1,0:T(8,128)(2,1)} %get-tuple-element.48) | copy-start | bytes 1572868 | tf_op jit(solution)/shard_map/cond
  2.0 5.9 %copy-start.6 = (f32[2048]{0:T(1024)S(1)}, f32[2048]{0:T(1024)}, u32[]{:S(2)}) copy-start(f32[2048]{0:T(1024)} %get-tuple-element.45) | copy-start | bytes 24580 | tf_op jit(solution)/shard_map/cond
  13.4 0.7 copy-start.7
  13.6 1.5 %copy-start.4 = (f32[256,1024]{1,0:T(8,128)S(1)}, f32[256,1024]{1,0:T(8,128)}, u32[]{:S(2)}) copy-start(f32[256,1024]{1,0:T(8,128)} %get-tuple-element.73) | copy-start | bytes 3145732 | tf_op jit(solution)/shard_map/cond
  69.0 1.6 %copy-start = (bf16[8192,128]{1,0:T(8,128)(2,1)S(1)}, bf16[8192,128]{1,0:T(8,128)(2,1)}, u32[]{:S(2)}) copy-start(bf16[8192,128]{1,0:T(8,128)(2,1)} %get-tuple-element.54.refs_5_) | copy-start | bytes 6291460 | tf_op jit(solution)/shard_map/cond
  70.6 0.9 copy-start.1
  71.6 61.3 %copy-start.2 = (bf16[1024,2048]{1,0:T(8,128)(2,1)S(1)}, bf16[1024,2048]{1,0:T(8,128)(2,1)}, u32[]{:S(2)}) copy-start(bf16[1024,2048]{1,0:T(8,128)(2,1)} %get-tuple-element.55) | copy-start | bytes 12582916 | tf_op jit(solution)/shard_map/cond
  119.4 13.5 %collective-permute-start = (bf16[256,512]{1,0:T(8,128)(2,1)S(1)}, bf16[256,512]{1,0:T(8,128)(2,1)S(1)}, u32[]{:S(2)}, u32[]{:S(2)}) collective-permute-start(bf16[256,512]{1,0:T(8,128)(2,1)S(1)} %get-tuple-element.67), channel_id=1, source_target_pairs={{0,31},{1,30},{2,29},{3,28},{4,27},{5,26},{6,25},{7,24},{8,23},{9,... | collective-permute-start | bytes 786440 | tf_op jit(solution)/shard_map/cond/branch_0_fun/ppermute | solution.py:1058

commit v7 on v6

--- a/solution.py
+++ b/solution.py
@@ -741,7 +741,10 @@
                     )
                 )
 
-            lanes_of(k)
+            @pl.when(k < zs)
+            def _():
+                lanes_of(k)
+
             for here_too, when, duty, zo in (
                 (z == 0, 1, late, z + 1), (z == 0, 3, late, z + 2),
                 (z > 0, 2, late, z + 1), (z > 0, 4, late_across, z + 1),
@@ -753,7 +756,7 @@
 
         @pl.when(early & (turn == 1))
         def _():
-            @pl.when(k < zs)
+            @pl.when(k < zs - 1)
             def _():
                 round_of(k + 1, True)
 
@@ -779,20 +782,32 @@
 
         @pl.when((step == s) & (turn == 0) & jnp.logical_not(idle))
         def _():
-            for pair in range(pairs):
-
-                @pl.when(pair >= my_first)
-                def _():
-                    att_ref[:, q_lanes(g, pair)] = finished(0, pair)
+            for pair in range(1, pairs):
+                att_ref[:, q_lanes(g, pair)] = finished(0, pair)
+
+            @pl.when(my_first == 0)
+            def _():
+                att_ref[:, q_lanes(g, 0)] = finished(0, 0)
 
         @pl.when((step == s) & (turn == 1))
         def _():
-            for n in range(pairs):
-
-                @pl.when(partner_first <= n)
-                def _():
-                    res_ref[n] = finished(1, n)
-                    back_copy(n, n, (s, partner_x, j)).start()
+            for n in range(1, pairs):
+                res_ref[n] = finished(1, n)
+            for n in range(1, pairs):
+                back_copy(n, n, (s, partner_x, j)).start()
+
+            @pl.when(partner_first == 0)
+            def _():
+                res_ref[0] = finished(1, 0)
+                back_copy(0, 0, (s, partner_x, j)).start()
+
+        @pl.when(early & (turn == 1) & (k == zs - 1))
+        def _():
+            round_of(zs, True)
+
+        @pl.when(early & (turn == 1) & (k == zs))
+        def _():
+            lanes_of(zs)
 
         return carry
 

time: 136 us -> 136 us (level)
  no operation moved by 1% of the time
where the time goes in v7:
time: 136 us; the launch traced here: 135 us
  Pallas kernels  99.4 us (73%)
  waiting for transfers between devices  13.4 us (10%)
  matrix products  8.24 us (6%)
  local copies, waits for them, and re-layouts  6.61 us (5%)
  other arithmetic  6.38 us (5%)
    pallas_call x1, Pallas kernels, any_scores(): pl.pallas_call(lambda *refs: exchange_kernel(*refs, rows=rows, sizes=size...  51.7 us
    pallas_call x1, Pallas kernels, attend(): pl.pallas_call(lambda *refs: attend_kernel(*refs, rows=rows, heads=heads,...  47.7 us
    ppermute x1, waiting for transfers between devices, any_scores(): back = lax.ppermute(attended[1], ALL, mirror)  13.4 us
    dot_general x1, matrix products, any_program(): jnp.dot(normed, w_query, preferred_element_type=jnp.float32)  4.46 us
  transfers between devices with their start and end apart: 1, of which 1 were waited for; matrix products, arithmetic and copies ran while one was open for 0% of the time, Pallas kernels for 0%

profile of v7, /device:TPU:9, one launch (start us, length us, event | category | flops | bytes accessed | tf_op | source)
XLA Modules:
  0.0 135.4 jit_solution(5048005743721283918)
XLA Ops:
  0.0 1.4 multiply_reduce_fusion.1
  2.0 132.4 %conditional.1 = (bf16[256,2048]{1,0:T(8,128)(2,1)S(1)}) conditional(s32[]{:T(128)} %convert_element_type.22, (bf16[256,2048]{1,0:T(8,128)(2,1)}, f32[2048]{0:T(1024)}, bf16[2048,1024]{1,0:T(8,128)(2,1)}, f32[64]{0:T(128)}, bf16[2048,128]{1,0:T(8,128)(2,1)}, /*index=5*/f32[64]{0:T(128)}, bf16[2048,128]{1,0:T(8,128)(2,1)}, f32[1024,4]{0,1:T(4,128)}, ...), branch_computations={%region_1.5_spmd, %region_5.6_spmd} | conditional | flops 2428711680 | bytes 68477896 | solution.py:1115
  2.1 0.8 broadcast_multiply_fusion
  2.9 1.5 %fusion = f32[256]{0:T(256)S(1)} fusion(bf16[256,2048]{1,0:T(8,128)(2,1)} %get-tuple-element.44), kind=kLoop, calls=%fused_computation.3 | loop fusion | flops 1572608 | bytes 1049600 | tf_op jit(solution)/shard_map/cond/branch_0_fun/reduce_sum | solution.py:21
  4.5 0.7 multiply_bitcast_fusion
  5.2 0.6 reshape.46.refs_2_
  5.8 1.9 %convolution_convert_fusion.1 = bf16[256,128]{0,1:T(8,128)(2,1)S(1)} fusion(bf16[2048,128]{1,0:T(8,128)(2,1)} %get-tuple-element.50, bf16[256,2048]{1,0:T(8,128)(2,1)} %get-tuple-element.44, f32[2048]{0:T(1024)} %get-tuple-element.45, f32[256]{0:T(256)S(1)} %add_rsqrt_fusion.2), kind=kOutput, calls=%fused_computation.6 | convolution fusion | flops 136347648 | bytes 1647616 | tf_op jit(solution)/shard_map/cond/branch_0_fun/dot_general | solution.py:1095
  7.9 0.6 multiply_reduce_fusion
  8.5 0.1 copy.28
  8.6 4.5 %fusion.15 = (f32[256,1024]{1,0:T(8,128)S(1)}, f32[256,1024]{1,0:T(8,128)}) fusion(bf16[2048,1024]{1,0:T(8,128)(2,1)} %get-tuple-element.46, bf16[256,2048]{1,0:T(8,128)(2,1)S(1)} %copy-done.3, f32[2048]{0:T(1024)S(1)} %copy-done.6, f32[256]{0:T(256)S(1)} %add_rsqrt_fusion.2), kind=kOutput, calls=%fused_computation.36 | convolution fusion | flops 1076101120 | bytes 7349248 | tf_op jit(solution)/shard_map/cond/branch_0_fun/dot_general | solution.py:1101
  13.1 0.3 copy.26
  13.7 0.3 copy.27
  14.1 0.1 multiply_convert_fusion.1
  14.2 0.8 maximum_bitcast_fusion.refs_0_
  15.0 0.2 multiply_convert_fusion
  15.2 0.7 broadcast_select_fusion
  16.0 51.7 %exchange.1 = (bf16[8192,128]{1,0:T(8,128)(2,1)}, bf16[256,512]{1,0:T(8,128)(2,1)}, f32[16,32,128]{2,1,0:T(8,128)}) custom-call(bf16[2,256,128]{2,1,0:T(8,128)(2,1)} %maximum_bitcast_fusion.refs_0_, bf16[256,512]{1,0:T(8,128)(2,1)} %get-tuple-element.68.refs_1_, f32[32,128]{1,0:T(8,128)} %reshape.46.refs_2_), custom_call_target="tpu_custom_call" | custom-call | tf_op jit(solution)/shard_map/cond/branch_0_fun/exchange/pallas_call | solution.py:1044
  67.6 1.1 reshape.47
  69.1 1.6 %copy-done = bf16[8192,128]{1,0:T(8,128)(2,1)S(1)} copy-done((bf16[8192,128]{1,0:T(8,128)(2,1)S(1)}, bf16[8192,128]{1,0:T(8,128)(2,1)}, u32[]{:S(2)}) %copy-start) | copy-done | bytes 2097176 | tf_op jit(solution)/shard_map/cond
  70.6 0.9 copy-done.1
  71.6 47.7 %attend_any.1 = bf16[2,256,512]{2,1,0:T(8,128)(2,1)S(1)} custom-call(s32[2]{0:T(128)S(1)} %pad_add_fusion.refs_0_, bf16[256,512]{1,0:T(8,128)(2,1)S(1)} %get-tuple-element.69.refs_1_, bf16[256,512]{1,0:T(8,128)(2,1)S(1)} %copy-done.1, f32[2,256,8]{2,1,0:T(8,128)S(1)} %copy.31.refs_3_, f32[16,8,512]{2,1,0:T(8,128)S(1)} %bitcast.37, bf16[8192,128]{1,0:T(8,128)(2,1)S(1)} %copy-done), custom_call_target="tpu_custom_call" | custom-call | tf_op jit(solution)/shard_map/cond/branch_0_fun/attend_any/pallas_call | solution.py:205
  119.5 13.4 %collective-permute-done = bf16[256,512]{1,0:T(8,128)(2,1)S(1)} collective-permute-done((bf16[256,512]{1,0:T(8,128)(2,1)S(1)}, bf16[256,512]{1,0:T(8,128)(2,1)S(1)}, u32[]{:S(2)}, u32[]{:S(2)}) %collective-permute-start) | collective-permute-done | bytes 262176 | tf_op jit(solution)/shard_map/cond/branch_0_fun/ppermute | solution.py:1073
  132.9 1.3 convolution_convert_fusion
  134.4 1.0 copy.35
  (29 shorter events, 0.9 us)
Async XLA Ops:
  2.0 5.9 %copy-start.3 = (bf16[256,2048]{1,0:T(8,128)(2,1)S(1)}, bf16[256,2048]{1,0:T(8,128)(2,1)}, u32[]{:S(2)}) copy-start(bf16[256,2048]{1,0:T(8,128)(2,1)} %get-tuple-element.44) | copy-start | bytes 3145732 | tf_op jit(solution)/shard_map/cond
  2.0 5.9 %copy-start.5 = (bf16[2048,128]{1,0:T(8,128)(2,1)S(1)}, bf16[2048,128]{1,0:T(8,128)(2,1)}, u32[]{:S(2)}) copy-start(bf16[2048,128]{1,0:T(8,128)(2,1)} %get-tuple-element.48) | copy-start | bytes 1572868 | tf_op jit(solution)/shard_map/cond
  2.0 5.9 %copy-start.6 = (f32[2048]{0:T(1024)S(1)}, f32[2048]{0:T(1024)}, u32[]{:S(2)}) copy-start(f32[2048]{0:T(1024)} %get-tuple-element.45) | copy-start | bytes 24580 | tf_op jit(solution)/shard_map/cond
  13.4 0.7 copy-start.7
  13.6 1.5 %copy-start.4 = (f32[256,1024]{1,0:T(8,128)S(1)}, f32[256,1024]{1,0:T(8,128)}, u32[]{:S(2)}) copy-start(f32[256,1024]{1,0:T(8,128)} %get-tuple-element.73) | copy-start | bytes 3145732 | tf_op jit(solution)/shard_map/cond
  69.0 1.6 %copy-start = (bf16[8192,128]{1,0:T(8,128)(2,1)S(1)}, bf16[8192,128]{1,0:T(8,128)(2,1)}, u32[]{:S(2)}) copy-start(bf16[8192,128]{1,0:T(8,128)(2,1)} %get-tuple-element.54.refs_5_) | copy-start | bytes 6291460 | tf_op jit(solution)/shard_map/cond
  70.6 0.9 copy-start.1
  71.6 61.3 %copy-start.2 = (bf16[1024,2048]{1,0:T(8,128)(2,1)S(1)}, bf16[1024,2048]{1,0:T(8,128)(2,1)}, u32[]{:S(2)}) copy-start(bf16[1024,2048]{1,0:T(8,128)(2,1)} %get-tuple-element.55) | copy-start | bytes 12582916 | tf_op jit(solution)/shard_map/cond
  119.4 13.5 %collective-permute-start = (bf16[256,512]{1,0:T(8,128)(2,1)S(1)}, bf16[256,512]{1,0:T(8,128)(2,1)S(1)}, u32[]{:S(2)}, u32[]{:S(2)}) collective-permute-start(bf16[256,512]{1,0:T(8,128)(2,1)S(1)} %get-tuple-element.67), channel_id=1, source_target_pairs={{0,31},{1,30},{2,29},{3,28},{4,27},{5,26},{6,25},{7,24},{8,23},{9,... | collective-permute-start | bytes 786440 | tf_op jit(solution)/shard_map/cond/branch_0_fun/ppermute | solution.py:1073
